TPU v7x, 512 devices: a whole 4x4x16 slice. The times are simulated.
512 devices in a mesh: sp: 64 (over z, y), tp: 8 (over x, core).
Axes of the slice: x: 4, y: 4, z: 16, core: 2. Of those that a mesh axis runs over, the one named last changes fastest.
Arguments:
- tokens: bfloat16 [16384, 2048], P('sp', 'tp'), may hold values from -64 to 64
- input_norm_gain: float32 [2048], replicated, may hold values from 0.1 to 1.9
- attention_query_weight: bfloat16 [2048, 512], P(None, 'tp'), may hold values from -0.21875 to 0.21875
- attention_key_weight: bfloat16 [2048, 512], P(None, 'tp'), may hold values from -0.21875 to 0.21875
- attention_value_weight: bfloat16 [2048, 512], P(None, 'tp'), may hold values from -0.125 to 0.125
- attention_score_bias: float32 [8], P('tp'), may hold values from -18 to -7
- recurrence_query_weight: bfloat16 [2048, 1024], P(None, 'tp'), may hold values from -0.125 to 0.125
- forget_weight: bfloat16 [2048, 1024], P(None, 'tp'), may hold values from -0.125 to 0.125
- input_weight: bfloat16 [2048, 512], P(None, 'tp'), may hold values from -0.125 to 0.125
- output_gate_weight: bfloat16 [2048, 512], P(None, 'tp'), may hold values from -0.125 to 0.125
- forget_minimum: float32 [8, 128], P('tp'), may hold values from 0.9 to 1
- decay_spikes: float32 [16384, 8], P('sp', 'tp'), may hold values from -2.2 to 0
- head_norm_gain: float32 [64], replicated, may hold values from 0.1 to 1.9
- attention_output_weight: bfloat16 [512, 2048], P('tp'), may hold values from -0.25 to 0.25
- recurrence_output_weight: bfloat16 [512, 2048], P('tp'), may hold values from -0.25 to 0.25
Outputs:
- mixed: bfloat16 [16384, 2048], P('sp', 'tp')
All inputs are finite; a program needn't handle non-finite values.
Results may differ from a plain program's by a relative error of at most 0.018.
Values may be sent and summed in bfloat16 or wider, within the bound.
A program may use at most 64 MiB of HBM per device.

v0:
```python
import jax
import jax.numpy as jnp
from jax import lax
from jax.sharding import Mesh
from jax.sharding import PartitionSpec as P

D = 2048
HEAD = 64
REC_KEY = 128
REC_VAL = 64
KEY_SPAN = 1024
REC_SPAN = 64
SP = ("sp_0", "sp_1")


epsilon = 1e-06


def copy_for_each(array, axis):
    copies = jnp.broadcast_to(array, (lax.axis_size(axis), *array.shape))
    return lax.all_to_all(copies, axis, split_axis=0, concat_axis=0, tiled=True)


def laid_out(pieces, dim):
    lengths = list(pieces.shape[1:])
    lengths[dim] *= pieces.shape[0]
    return jnp.moveaxis(pieces, 0, dim).reshape(lengths)


def gathered_copies(array, axis, dim):
    pieces = copy_for_each(array, axis)
    return laid_out(pieces, dim)


def side_by_side(arrays, axis, dim, along):
    ends, at = ([], 0)
    for a in arrays[:-1]:
        at += a.shape[along]
        ends.append(at)
    both = jnp.concatenate(arrays, axis=along)
    return tuple(jnp.split(lax.all_gather(both, axis, axis=dim, tiled=True), ends, axis=along))


def neutral_like(array, identity):
    return jax.tree.map(
        lambda a, e: jnp.broadcast_to(jnp.asarray(e, a.dtype), a.shape), array, identity
    )


def entering(array, axes, combine, identity):
    before = start = neutral_like(array, identity)
    running = array
    for axis in reversed(axes):
        size, here = (lax.axis_size(axis), lax.axis_index(axis))
        pieces = jax.tree.map(lambda part: lax.all_gather(part, axis), running)
        inside, running = (start, start)
        for k in range(size):
            passed = k < here
            running = combine(running, jax.tree.map(lambda part: part[k], pieces))
            inside = jax.tree.map(lambda new, old: jnp.where(passed, new, old), running, inside)
        before = combine(inside, before)
    return before


def cut_along(array, dim, size):
    lengths = array.shape
    pieces = array.reshape(*lengths[:dim], size, lengths[dim] // size, *lengths[dim + 1 :])
    return jnp.moveaxis(pieces, dim, 0)


def summed_on_arrival(array, axis, dim):
    pieces = cut_along(array, dim, lax.axis_size(axis))
    arrived = lax.all_to_all(pieces, axis, split_axis=0, concat_axis=0, tiled=True)
    return arrived.astype(jnp.float32).sum(axis=0)


def shards(
    tokens,
    input_norm_gain,
    attention_query_weight,
    attention_key_weight,
    attention_value_weight,
    attention_score_bias,
    recurrence_query_weight,
    forget_weight,
    input_weight,
    output_gate_weight,
    forget_minimum,
    decay_spikes,
    head_norm_gain,
    attention_output_weight,
    recurrence_output_weight,
):
    row_count = tokens.shape[0]
    weights = (
        attention_query_weight,
        attention_key_weight,
        attention_value_weight,
        recurrence_query_weight,
        forget_weight,
        input_weight,
        output_gate_weight,
    )
    values = gathered_copies(tokens, "tp", 1).astype(jnp.float32)
    scaled = (values * input_norm_gain[None, :]).astype(jnp.bfloat16)
    partials = tuple(
        (jnp.dot(scaled, weight, preferred_element_type=jnp.float32) for weight in weights)
    )
    partials, squares = (partials, jnp.sum(values * values, axis=1))
    inverse = lax.rsqrt(squares / D + epsilon)[:, None]
    query_stick, key_stick, value_stick, query_rows, forget_rows, input_rows, gate_rows = tuple(
        ((running_total * inverse).astype(jnp.bfloat16) for running_total in partials)
    )
    position = lax.axis_index(SP)
    first_row = position * row_count
    end_row = first_row + row_count
    keys_all, values_all = side_by_side((key_stick, value_stick), SP, 0, 1)
    heads_here = attention_score_bias.shape[0]
    query_heads = query_stick.reshape(row_count, heads_here, HEAD)
    query_pos = first_row + jnp.arange(row_count, dtype=jnp.int32)
    block_rows = min(KEY_SPAN, keys_all.shape[0])
    block_count = (end_row + block_rows - 1) // block_rows

    def key_block(block_number, state_carry):
        totals, carried = state_carry
        upper_row = end_row - block_number * block_rows
        lower_row = jnp.maximum(upper_row - block_rows, 0)
        key_rows = lax.dynamic_slice_in_dim(keys_all, lower_row, block_rows, 0).reshape(
            block_rows, heads_here, HEAD
        )
        value_rows = lax.dynamic_slice_in_dim(values_all, lower_row, block_rows, 0).reshape(
            block_rows, heads_here, HEAD
        )
        key_pos = lower_row + jnp.arange(block_rows, dtype=jnp.int32)
        scores = jnp.einsum(
            "qhd,khd->hqk", query_heads, key_rows, preferred_element_type=jnp.float32
        ) * HEAD ** (-0.5)
        scores = scores + attention_score_bias[:, None, None]
        before = ((key_pos[None, :] < query_pos[:, None]) & (key_pos[None, :] < upper_row))[None]
        log_rest = jnp.where(before, jax.nn.log_sigmoid(-scores), 0.0)
        later_sum = lax.cumsum(log_rest, axis=2, reverse=True) - log_rest + carried[:, :, None]
        weights_here = jnp.where(
            before, jnp.exp(jax.nn.log_sigmoid(scores) + later_sum), 0.0
        ).astype(jnp.bfloat16)
        totals = totals + jnp.einsum(
            "hqk,khd->qhd", weights_here, value_rows, preferred_element_type=jnp.float32
        )
        return (totals, carried + jnp.sum(log_rest, axis=2))

    start_carry = (
        jnp.zeros((row_count, heads_here, HEAD), jnp.float32),
        jnp.zeros((heads_here, row_count), jnp.float32),
    )
    totals, carried = lax.fori_loop(0, block_count, key_block, start_carry)
    stick_heads = totals.reshape(row_count, heads_here * HEAD).astype(jnp.bfloat16)
    state_heads_here = forget_minimum.shape[0]
    raised_values = jax.nn.silu(query_rows.astype(jnp.float32)).reshape(
        row_count, state_heads_here, REC_KEY
    )
    admitted_input = (1.0 - forget_minimum)[None] * jax.nn.sigmoid(
        -forget_rows.astype(jnp.float32).reshape(row_count, state_heads_here, REC_KEY)
    )
    forget_logarithm = jnp.log1p(-admitted_input) + decay_spikes[:, :, None]
    inputs = input_rows.astype(jnp.float32).reshape(row_count, state_heads_here, REC_VAL)
    span_count = row_count // REC_SPAN
    causal = jnp.tril(jnp.ones((REC_SPAN, REC_SPAN), jnp.bool_))[:, :, None, None]

    def to_spans(array):
        return array.reshape(span_count, REC_SPAN, state_heads_here, array.shape[-1])

    def advance(state_carry, pieces):
        recurrent_memory, offset = state_carry
        window_query, window_admitted, window_input, span_log = pieces
        running_total = jnp.cumsum(span_log, axis=0)
        log_gaps = running_total[:, None] - running_total[None, :]
        decay_table = jnp.where(causal, jnp.exp(jnp.where(causal, log_gaps, 0.0)), 0.0)
        inner_scores = jnp.einsum("thk,shk,tshk->hts", window_query, window_admitted, decay_table)
        final_output = jnp.einsum("hts,shv->thv", inner_scores, window_input)
        final_output = final_output + jnp.einsum(
            "zbg,bgp->zbp", window_query * jnp.exp(running_total), recurrent_memory
        )
        window_total = running_total[-1]
        recurrent_memory = recurrent_memory * jnp.exp(window_total)[:, :, None] + jnp.einsum(
            "rof,roi->ofi",
            window_admitted * jnp.exp(window_total[None] - running_total),
            window_input,
        )
        return (
            (recurrent_memory, offset + window_total),
            (final_output, running_total + offset[None]),
        )

    start_state = (
        jnp.zeros((state_heads_here, REC_KEY, REC_VAL), jnp.float32),
        jnp.zeros((state_heads_here, REC_KEY), jnp.float32),
    )
    (memory_end, offset_end), (local_out, prefix_total) = lax.scan(
        advance,
        start_state,
        (
            to_spans(raised_values),
            to_spans(admitted_input),
            to_spans(inputs),
            to_spans(forget_logarithm),
        ),
    )
    local_out = local_out.reshape(row_count, state_heads_here, REC_VAL)
    prefix_total = prefix_total.reshape(row_count, state_heads_here, REC_KEY)
    decay_all = jnp.exp(offset_end)

    def chain_combine(earlier, later_part):
        return (earlier[0] * later_part[0], earlier[1] * later_part[0][:, :, None] + later_part[1])

    identity = (jnp.ones_like(decay_all), jnp.zeros_like(memory_end))
    decay_before, incoming_state = entering((decay_all, memory_end), SP, chain_combine, identity)
    outputs = local_out + jnp.einsum(
        "zbg,bgp->zbp", raised_values * jnp.exp(prefix_total), incoming_state
    )
    normed = (
        outputs
        * lax.rsqrt(jnp.mean(outputs * outputs, axis=2, keepdims=True) + epsilon)
        * head_norm_gain
    )
    gated_out = normed * jax.nn.silu(
        gate_rows.astype(jnp.float32).reshape(row_count, state_heads_here, REC_VAL)
    )
    recurrence_heads = gated_out.reshape(row_count, state_heads_here * REC_VAL).astype(jnp.bfloat16)
    partial_out = jnp.dot(stick_heads, attention_output_weight, preferred_element_type=jnp.float32)
    partial_out = partial_out + jnp.dot(
        recurrence_heads, recurrence_output_weight, preferred_element_type=jnp.float32
    )
    mixed_out = summed_on_arrival(partial_out.astype(jnp.bfloat16), "tp", 1).astype(jnp.bfloat16)
    return mixed_out


def solution(mesh):
    torus = Mesh(mesh.devices.reshape(16, 4, mesh.shape["tp"]), ("sp_0", "sp_1", "tp"))
    placed = (
        P(SP, "tp"),
        P(),
        P(None, "tp"),
        P(None, "tp"),
        P(None, "tp"),
        P("tp"),
        P(None, "tp"),
        P(None, "tp"),
        P(None, "tp"),
        P(None, "tp"),
        P("tp", None),
        P(SP, "tp"),
        P(),
        P("tp", None),
        P("tp", None),
    )
    return jax.shard_map(
        shards, mesh=torus, in_specs=placed, out_specs=P(SP, "tp"), check_vma=False
    )
```

profile of v0, /device:TPU:480, one launch (start us, length us, event | category | flops | bytes accessed | tf_op | source)
XLA Modules:
  0.0 368.8 jit_solution(13854328306392518044)
XLA Ops:
  8.7 4.3 %all-to-all-start = ((bf16[8,256,256]{1,2,0:T(8,128)(2,1)}), bf16[8,256,256]{1,2,0:T(8,128)(2,1)S(1)}, u32[]{:S(2)}, u32[]{:S(2)}) async-start(bf16[8,256,256]{1,2,0:T(8,128)(2,1)} %broadcast_in_dim.72), calls=%async_computation | async-start | bytes 2097152 | tf_op jit(solution)/shard_map/all_to_all | solution.py:21
  13.2 15.8 %all-to-all-done = bf16[8,256,256]{1,2,0:T(8,128)(2,1)S(1)} async-done(((bf16[8,256,256]{1,2,0:T(8,128)(2,1)}), bf16[8,256,256]{1,2,0:T(8,128)(2,1)S(1)}, u32[]{:S(2)}, u32[]{:S(2)}) %all-to-all-start) | async-done | bytes 1048608 | tf_op jit(solution)/shard_map/all_to_all | solution.py:21
  33.5 12.9 %while.34 = (s32[]{:T(128)}, f32[1,128,64]{1,2,0:T(8,128)S(1)}, f32[1,128]{1,0:T(1,128)S(1)}, f32[4,64,1,64]{1,0,3,2:T(4,128)S(1)}, f32[4,64,1,128]{3,1,2,0:T(8,...) while((s32[]{:T(128)}, f32[1,128,64]{1,2,0:T(8,128)S(1)}, ...), condition=%wide.region_8.9_spmd.clone.clone, body=%wide.region_6.8_spmd.clone.clone.sunk | while | flops 6353155 | bytes 5060253 | solution.py:197
  46.6 10.0 %all-gather.2 = f32[4,1,128]{2,1,0:T(1,128)S(1)} all-gather(f32[1,1,128]{2,1,0:T(1,128)S(1)} %exponential_bitcast_fusion), channel_id=2, replica_groups=mesh['sp_0'=16,'sp_1'=4,'tp'=8] {'sp_1'}, dimensions={0}, use_global_device_ids=true | all-gather | bytes 2560 | tf_op jit(solution)/shard_map/all_gather | solution.py:55
  56.6 25.7 %all_gather.26 = f32[16,1,128]{2,1,0:T(1,128)S(1)} all-gather(f32[1,1,128]{2,1,0:T(1,128)S(1)} %get-tuple-element.415), channel_id=1, replica_groups=mesh['sp_0'=16,'sp_1'=4,'tp'=8] {'sp_0'}, dimensions={0}, use_global_device_ids=true | all-gather | bytes 8704 | tf_op jit(solution)/shard_map/all_gather | solution.py:55
  82.3 12.0 %all-gather.1 = f32[4,128,64]{1,2,0:T(8,128)S(1)} all-gather(f32[1,128,64]{1,2,0:T(8,128)S(1)} %get-tuple-element.194), channel_id=3, replica_groups=mesh['sp_0'=16,'sp_1'=4,'tp'=8] {'sp_1'}, dimensions={0}, use_global_device_ids=true | all-gather | bytes 163840 | tf_op jit(solution)/shard_map/all_gather | solution.py:55
  94.7 32.1 %all_gather.29 = f32[16,1,128,64]{2,3,1,0:T(8,128)S(1)} all-gather(f32[1,1,128,64]{2,3,1,0:T(8,128)S(1)} %bitcast_add_fusion.6), channel_id=1, replica_groups=mesh['sp_0'=16,'sp_1'=4,'tp'=8] {'sp_0'}, dimensions={0}, use_global_device_ids=true | all-gather | bytes 557056 | tf_op jit(solution)/shard_map/all_gather | solution.py:55
  127.6 44.5 %all-gather.5.cloned.1.call-done = bf16[16384,128]{0,1:T(8,128)(2,1)} async-done(((bf16[256,128]{0,1:T(8,128)(2,1)}), bf16[16384,128]{0,1:T(8,128)(2,1)}) %all-gather.5.cloned.1.call-update) | async-done | bytes 4194320 | tf_op jit(solution)/shard_map/all_gather | solution.py:41
  172.1 4.6 %fusion.203 = (bf16[16384,64]{0,1:T(8,128)(2,1)}, bf16[16384,64]{0,1:T(8,128)(2,1)}) fusion(bf16[16384,128]{0,1:T(8,128)(2,1)} %all-gather.5.cloned.1.call-done), kind=kLoop, calls=%fused_computation.279 | loop fusion | bytes 8388608 | tf_op jit(solution)/shard_map/split | solution.py:41
  176.7 159.5 %while.33 = (s32[]{:T(128)}, f32[256,1,64]{0,2,1:T(8,128)S(1)}, f32[1,256]{1,0:T(1,128)S(1)}, s32[]{:T(128)}, s32[]{:T(128)}, /*index=5*/bf16[16384,64]{0,1:T(8,...) while((s32[]{:T(128)}, f32[256,1,64]{0,2,1:T(8,128)S(1)}, ...), condition=%wide.region_5.6_spmd.clone, body=%wide.region_1.5_spmd.clone.sunk | while | flops 108039168 | bytes 10994401 | solution.py:154
  176.8 3.4 fusion.253
  180.2 2.5 fusion.254
  186.8 3.4 fusion.253
  196.8 3.4 fusion.253
  200.2 2.5 fusion.254
  206.7 3.4 fusion.253
  210.1 2.5 fusion.254
  216.7 3.4 fusion.253
  220.1 2.5 fusion.254
  226.7 3.4 fusion.253
  236.6 3.4 fusion.253
  246.6 3.4 fusion.253
  256.6 3.4 fusion.253
  266.6 3.4 fusion.253
  276.5 3.4 fusion.253
  286.5 3.4 fusion.253
  296.5 3.4 fusion.253
  306.4 3.4 fusion.253
  316.4 3.4 fusion.253
  326.4 3.4 fusion.253
  338.2 2.7 fusion.46
  340.9 20.3 %all_to_all.10 = bf16[8,256,256]{2,1,0:T(8,128)(2,1)S(1)} all-to-all(bf16[8,256,256]{2,1,0:T(8,128)(2,1)S(1)} %bitcast.481), channel_id=1, replica_groups=mesh['sp_0'=16,'sp_1'=4,'tp'=8] {'tp'}, dimensions={0} | all-to-all | bytes 2097152 | tf_op jit(solution)/shard_map/all_to_all | solution.py:73
  (299 shorter events, 116.8 us)
Async XLA Ops:
  6.5 26.4 %copy-start = (bf16[2048,128]{1,0:T(8,128)(2,1)S(1)}, bf16[2048,128]{1,0:T(8,128)(2,1)}, u32[]{:S(2)}) copy-start(bf16[2048,128]{1,0:T(8,128)(2,1)} %param.26) | copy-start | bytes 1572868
  6.5 6.6 %copy-start.15 = (f32[1,128]{1,0:T(1,128)S(1)}, f32[1,128]{1,0:T(1,128)}, u32[]{:S(2)}) copy-start(f32[1,128]{1,0:T(1,128)} %param.29) | copy-start | bytes 1540
  7.6 21.6 %copy-start.12 = (f32[2048]{0:T(1024)S(1)}, f32[2048]{0:T(1024)}, u32[]{:S(2)}) copy-start(f32[2048]{0:T(1024)} %param.20) | copy-start | bytes 24580
  8.7 20.2 %all-to-all-start = ((bf16[8,256,256]{1,2,0:T(8,128)(2,1)}), bf16[8,256,256]{1,2,0:T(8,128)(2,1)S(1)}, u32[]{:S(2)}, u32[]{:S(2)}) async-start(bf16[8,256,256]{1,2,0:T(8,128)(2,1)} %broadcast_in_dim.72), calls=%async_computation | async-start | bytes 2097152 | tf_op jit(solution)/shard_map/all_to_all | solution.py:21
  13.0 16.6 %copy-start.6 = (bf16[2048,64]{0,1:T(8,128)(2,1)S(1)}, bf16[2048,64]{0,1:T(8,128)(2,1)}, u32[]{:S(2)}) copy-start(bf16[2048,64]{0,1:T(8,128)(2,1)} %param.23) | copy-start | bytes 786436
  13.0 159.2 %all-gather.5.cloned.1.call-start = ((), (), s32[]{:S(2)}) async-start(), calls=%async_computation.2 | async-start | bytes 4259840 | tf_op jit(solution)/shard_map/all_gather | solution.py:41
  13.1 16.8 %copy-start.7 = (bf16[2048,64]{0,1:T(8,128)(2,1)S(1)}, bf16[2048,64]{0,1:T(8,128)(2,1)}, u32[]{:S(2)}) copy-start(bf16[2048,64]{0,1:T(8,128)(2,1)} %param.22) | copy-start | bytes 786436
  29.2 1.7 copy-start.8
  29.6 64.7 %copy-start.1 = (bf16[256,2048]{0,1:T(8,128)(2,1)}, bf16[256,2048]{0,1:T(8,128)(2,1)S(1)}, u32[]{:S(2)}) copy-start(bf16[256,2048]{0,1:T(8,128)(2,1)S(1)} %fusion.47) | copy-start | bytes 3145732
  30.2 2.7 copy-start.14
  31.3 2.1 copy-start.10
  31.3 2.1 copy-start.11
  33.4 60.8 %copy-start.9 = (bf16[2048,64]{0,1:T(8,128)(2,1)S(1)}, bf16[2048,64]{0,1:T(8,128)(2,1)}, u32[]{:S(2)}) copy-start(bf16[2048,64]{0,1:T(8,128)(2,1)} %param.21) | copy-start | bytes 786436
  176.7 159.6 %copy-start.3 = (bf16[64,2048]{1,0:T(8,128)(2,1)S(1)}, bf16[64,2048]{1,0:T(8,128)(2,1)}, u32[]{:S(2)}) copy-start(bf16[64,2048]{1,0:T(8,128)(2,1)} %param.32) | copy-start | bytes 786436
  336.3 1.9 copy-start.2
  336.3 1.9 copy-start.4
  336.3 1.8 copy-start.5
  336.3 1.8 copy-start.13
Sparse Core Ops, SparseCore 0:
  31.0 141.0 all-gather.4
where the time goes:
time: 370 us; the launch traced here: 369 us
  blocking collectives  100 us (27%)
  other arithmetic  91.1 us (25%)
  matrix products  84 us (23%)
  waiting for transfers between devices  60.3 us (16%)
  between operations  13.8 us (4%)
  local copies, waits for them, and re-layouts  13.6 us (4%)
  starting transfers between devices  4.34 us (1%)
    all_gather x4, blocking collectives, entering(): pieces = jax.tree.map(lambda part: lax.all_gather(part, axis), running)  79.7 us
    dot_general x16, matrix products, key_block(): jnp.einsum('qhd,khd->hqk', query_heads, key_rows, preferred_element_type=...  54.6 us
    all_gather x1, waiting for transfers between devices, side_by_side(): lax.all_gather(both, axis, axis=dim, tiled=True)  44.5 us
    another operation x36, other arithmetic  40.7 us
    convert_element_type x16, other arithmetic, key_block(): weights_here = jnp.where(before, jnp.exp(jax.nn.log_sigmoid(scores) + lat...  38.1 us
    all_to_all x1, blocking collectives, summed_on_arrival(): lax.all_to_all(pieces, axis, split_axis=0, concat_axis=0, tiled=True)  20.3 us
    dot_general x16, matrix products, key_block(): jnp.einsum('hqk,khd->qhd', weights_here, value_rows, preferred_element_ty...  18.7 us
    all_to_all x1, waiting for transfers between devices, copy_for_each(): return lax.all_to_all(copies, axis, split_axis=0, concat_axis=0, tiled=True)  15.8 us
  transfers between devices with their start and end apart: 2, of which 2 were waited for; matrix products, arithmetic and copies ran while one was open for 4% of the time, Pallas kernels for 0%

commit v1 on v0

v1 whole, which is shorter than its diff:
```python
import functools

import jax
import jax.numpy as jnp
from jax import lax
from jax.experimental import pallas as pl
from jax.experimental.pallas import tpu as pltpu
from jax.sharding import Mesh
from jax.sharding import PartitionSpec as P

LOG2E = 1.4426950408889634
KB = 256

D = 2048
HEAD = 64
REC_KEY = 128
REC_VAL = 64
REC_SPAN = 64
SP = ("sp_0", "sp_1")


epsilon = 1e-06


def copy_for_each(array, axis):
    copies = jnp.broadcast_to(array, (lax.axis_size(axis), *array.shape))
    return lax.all_to_all(copies, axis, split_axis=0, concat_axis=0, tiled=True)


def laid_out(pieces, dim):
    lengths = list(pieces.shape[1:])
    lengths[dim] *= pieces.shape[0]
    return jnp.moveaxis(pieces, 0, dim).reshape(lengths)


def gathered_copies(array, axis, dim):
    pieces = copy_for_each(array, axis)
    return laid_out(pieces, dim)


def side_by_side(arrays, axis, dim, along):
    ends, at = ([], 0)
    for a in arrays[:-1]:
        at += a.shape[along]
        ends.append(at)
    both = jnp.concatenate(arrays, axis=along)
    return tuple(jnp.split(lax.all_gather(both, axis, axis=dim, tiled=True), ends, axis=along))


def neutral_like(array, identity):
    return jax.tree.map(
        lambda a, e: jnp.broadcast_to(jnp.asarray(e, a.dtype), a.shape), array, identity
    )


def entering(array, axes, combine, identity):
    before = start = neutral_like(array, identity)
    running = array
    for axis in reversed(axes):
        size, here = (lax.axis_size(axis), lax.axis_index(axis))
        pieces = jax.tree.map(lambda part: lax.all_gather(part, axis), running)
        inside, running = (start, start)
        for k in range(size):
            passed = k < here
            running = combine(running, jax.tree.map(lambda part: part[k], pieces))
            inside = jax.tree.map(lambda new, old: jnp.where(passed, new, old), running, inside)
        before = combine(inside, before)
    return before


def cut_along(array, dim, size):
    lengths = array.shape
    pieces = array.reshape(*lengths[:dim], size, lengths[dim] // size, *lengths[dim + 1 :])
    return jnp.moveaxis(pieces, dim, 0)


def summed_on_arrival(array, axis, dim):
    pieces = cut_along(array, dim, lax.axis_size(axis))
    arrived = lax.all_to_all(pieces, axis, split_axis=0, concat_axis=0, tiled=True)
    return arrived.astype(jnp.float32).sum(axis=0)


def dot(a, b, ta=False, tb=False):
    dims = (((0 if ta else 1,), (1 if tb else 0,)), ((), ()))
    return lax.dot_general(a, b, dims, preferred_element_type=jnp.float32)


def stick_tile(q, kv, tri, bias2, carry, keep=None):
    z = dot(q, kv, tb=True) * (LOG2E / 8.0) + bias2
    soft = jnp.maximum(z, jnp.log(1.0 + jnp.exp2(jnp.minimum(z, 30.0))) * LOG2E)
    if keep is not None:
        soft = jnp.where(keep, soft, 0.0)
    later = dot(soft.astype(jnp.bfloat16), tri)
    weight = jnp.exp2((z - soft) + (later + carry))
    if keep is not None:
        weight = jnp.where(keep, weight, 0.0)
    part = dot(weight.astype(jnp.bfloat16), kv)
    return part, carry + (later[:, 0:1] - soft[:, 0:1])


def stick_kernel(pos_ref, bias_ref, q_ref, kv_ref, out_ref, tri_ref, acc_ref, carry_ref):
    pos = pos_ref[0]
    bias2 = bias_ref[0] * LOG2E
    rows = lax.broadcasted_iota(jnp.int32, (KB, KB), 0)
    cols = lax.broadcasted_iota(jnp.int32, (KB, KB), 1)
    tri_ref[...] = jnp.where(rows > cols, -1.0, 0.0).astype(jnp.bfloat16)
    q = q_ref[...]
    zero = jnp.zeros((KB, 1), jnp.float32)
    part, carry = stick_tile(
        q, kv_ref[pl.ds(pl.multiple_of(pos * KB, KB), KB), :], tri_ref[...], bias2, zero, cols < rows
    )
    acc_ref[...] = part
    carry_ref[...] = jnp.broadcast_to(carry, carry_ref.shape)

    def block(i, _):
        at = pl.multiple_of((pos - 1 - i) * KB, KB)
        part, carry = stick_tile(
            q, kv_ref[pl.ds(at, KB), :], tri_ref[...], bias2, carry_ref[:, 0:1]
        )
        acc_ref[...] += part
        carry_ref[...] = jnp.broadcast_to(carry, carry_ref.shape)
        return 0

    lax.fori_loop(0, pos, block, 0)
    out_ref[...] = acc_ref[...].astype(jnp.bfloat16)


def stick(pos, bias, q, kv):
    return pl.pallas_call(
        stick_kernel,
        out_shape=jax.ShapeDtypeStruct((KB, 2 * HEAD), jnp.bfloat16),
        in_specs=[
            pl.BlockSpec(memory_space=pltpu.SMEM),
            pl.BlockSpec(memory_space=pltpu.SMEM),
            pl.BlockSpec(memory_space=pltpu.VMEM),
            pl.BlockSpec(memory_space=pltpu.VMEM),
        ],
        out_specs=pl.BlockSpec(memory_space=pltpu.VMEM),
        scratch_shapes=[
            pltpu.VMEM((KB, KB), jnp.bfloat16),
            pltpu.VMEM((KB, 2 * HEAD), jnp.float32),
            pltpu.VMEM((KB, 128), jnp.float32),
        ],
        name="stick",
    )(pos, bias, q, kv)


def scan_kernel(query_ref, forget_ref, input_ref, low_ref, spike_ref, out_ref, lift_ref, state_ref, total_ref):
    span = REC_SPAN
    rows = lax.broadcasted_iota(jnp.int32, (span, span), 0)
    cols = lax.broadcasted_iota(jnp.int32, (span, span), 1)
    causal = cols <= rows
    ones = jnp.where(causal, 1.0, 0.0)
    state = jnp.zeros((REC_VAL, REC_KEY), jnp.float32)
    offset = jnp.zeros((1, REC_KEY), jnp.float32)
    for n in range(query_ref.shape[0] // span):
        at = slice(n * span, (n + 1) * span)
        query = query_ref[at, :].astype(jnp.float32)
        lifted = query * jax.nn.sigmoid(query)
        intake = (1.0 - low_ref[...]) * jax.nn.sigmoid(-forget_ref[at, :].astype(jnp.float32))
        log_forget = jnp.log1p(-intake) + spike_ref[at, :]
        running = lax.dot_general(
            ones, log_forget, (((1,), (0,)), ((), ())),
            precision=lax.Precision.HIGHEST, preferred_element_type=jnp.float32,
        )
        total = running[span - 1 : span, :]
        middle = running[span // 2 - 1 : span // 2, :]
        value = input_ref[at, :]
        grown = (lifted * jnp.exp(running - middle)).astype(jnp.bfloat16)
        shrunk = (intake * jnp.exp(middle - running)).astype(jnp.bfloat16)
        inner = jnp.where(causal, dot(grown, shrunk, tb=True), 0.0)
        faded = (lifted * jnp.exp(running)).astype(jnp.bfloat16)
        out = dot(inner.astype(jnp.bfloat16), value) + dot(faded, state.astype(jnp.bfloat16), tb=True)
        out_ref[at, :] = out
        lift_ref[at, :] = (lifted * jnp.exp(running + offset)).astype(jnp.bfloat16)
        kept = (intake * jnp.exp(total - running)).astype(jnp.bfloat16)
        state = state * jnp.exp(total) + dot(value, kept, ta=True)
        offset = offset + total
    state_ref[...] = state
    total_ref[...] = offset


def local_scan(query, forget, inputs, low, spikes):
    n = query.shape[0]
    f32, bf16 = jnp.float32, jnp.bfloat16
    vmem = pl.BlockSpec(memory_space=pltpu.VMEM)
    return pl.pallas_call(
        scan_kernel,
        out_shape=(
            jax.ShapeDtypeStruct((n, REC_VAL), f32),
            jax.ShapeDtypeStruct((n, REC_KEY), bf16),
            jax.ShapeDtypeStruct((REC_VAL, REC_KEY), f32),
            jax.ShapeDtypeStruct((1, REC_KEY), f32),
        ),
        in_specs=[vmem] * 5,
        out_specs=(vmem,) * 4,
        name="local_scan",
    )(query, forget, inputs, low, spikes)


def shards(
    tokens,
    input_norm_gain,
    attention_query_weight,
    attention_key_weight,
    attention_value_weight,
    attention_score_bias,
    recurrence_query_weight,
    forget_weight,
    input_weight,
    output_gate_weight,
    forget_minimum,
    decay_spikes,
    head_norm_gain,
    attention_output_weight,
    recurrence_output_weight,
):
    row_count = tokens.shape[0]
    weights = (
        attention_query_weight,
        attention_key_weight,
        attention_value_weight,
        recurrence_query_weight,
        forget_weight,
        input_weight,
        output_gate_weight,
    )
    values = gathered_copies(tokens, "tp", 1).astype(jnp.float32)
    scaled = (values * input_norm_gain[None, :]).astype(jnp.bfloat16)
    partials = tuple(
        (jnp.dot(scaled, weight, preferred_element_type=jnp.float32) for weight in weights)
    )
    partials, squares = (partials, jnp.sum(values * values, axis=1))
    inverse = lax.rsqrt(squares / D + epsilon)[:, None]
    query_stick, key_stick, value_stick, query_rows, forget_rows, input_rows, gate_rows = tuple(
        ((running_total * inverse).astype(jnp.bfloat16) for running_total in partials)
    )
    position = lax.axis_index(SP)
    kv = jnp.concatenate([key_stick, value_stick], axis=1)
    kv_all = lax.all_gather(kv, SP, axis=0, tiled=True)
    padded = jnp.pad(query_stick, ((0, 0), (0, HEAD)))
    pos = position.astype(jnp.int32).reshape(1)
    stick_heads = stick(pos, attention_score_bias, padded, kv_all)[:, HEAD:]
    local_out, faded, memory_end, offset_end = local_scan(
        query_rows, forget_rows, input_rows, forget_minimum, decay_spikes
    )
    decay_all = jnp.exp(offset_end)

    def chain_combine(earlier, later_part):
        return (earlier[0] * later_part[0], earlier[1] * later_part[0] + later_part[1])

    identity = (jnp.ones_like(decay_all), jnp.zeros_like(memory_end))
    decay_before, incoming_state = entering((decay_all, memory_end), SP, chain_combine, identity)
    outputs = local_out + dot(faded, incoming_state.astype(jnp.bfloat16), tb=True)
    normed = (
        outputs
        * lax.rsqrt(jnp.mean(outputs * outputs, axis=1, keepdims=True) + epsilon)
        * head_norm_gain
    )
    recurrence_heads = (normed * jax.nn.silu(gate_rows.astype(jnp.float32))).astype(jnp.bfloat16)
    partial_out = jnp.dot(stick_heads, attention_output_weight, preferred_element_type=jnp.float32)
    partial_out = partial_out + jnp.dot(
        recurrence_heads, recurrence_output_weight, preferred_element_type=jnp.float32
    )
    mixed_out = summed_on_arrival(partial_out.astype(jnp.bfloat16), "tp", 1).astype(jnp.bfloat16)
    return mixed_out


def solution(mesh):
    torus = Mesh(mesh.devices.reshape(16, 4, mesh.shape["tp"]), ("sp_0", "sp_1", "tp"))
    placed = (
        P(SP, "tp"),
        P(),
        P(None, "tp"),
        P(None, "tp"),
        P(None, "tp"),
        P("tp"),
        P(None, "tp"),
        P(None, "tp"),
        P(None, "tp"),
        P(None, "tp"),
        P("tp", None),
        P(SP, "tp"),
        P(),
        P("tp", None),
        P("tp", None),
    )
    return jax.shard_map(
        shards, mesh=torus, in_specs=placed, out_specs=P(SP, "tp"), check_vma=False
    )
```

time: 370 us -> 240 us (0.65)
  other arithmetic: 91.1 us -> 2.22 us
  matrix products: 84 us -> 11.7 us
  Pallas kernels: 0 us -> 37.1 us
  blocking collectives: 100 us -> 120 us
  local copies, waits for them, and re-layouts: 13.6 us -> 3.62 us
  waiting for transfers between devices: 60.3 us -> 51.1 us
  starting transfers between devices: 4.34 us -> 0.01 us
    dot_general x45 -> x1, matrix products: 76.2 us -> 1.29 us  [dot(): return lax.dot_general(a, b, dims, preferred_element_type=jnp.float32)]
    another operation x41 -> x1, other arithmetic: 41 us -> 0.01 us  [chain_combine(): earlier[1] * later_part[0] + later_part[1]]
    convert_element_type x16 -> x0, other arithmetic: 38.1 us -> none  [key_block(): weights_here = jnp.where(before, jnp.exp(jax.nn.log_sigmoid(scores) + lat...]
    pallas_call x0 -> x2, Pallas kernels: none -> 37.1 us  [the longest x1 34.2 us: stick(): pl.pallas_call(stick_kernel, out_shape=jax.ShapeDtypeStruct((KB, 2 * HEAD...]
    all_to_all x0 -> x1, blocking collectives: none -> 20.1 us  [copy_for_each(): return lax.all_to_all(copies, axis, split_axis=0, concat_axis=0, tiled=True)]
    all_to_all x1 -> x0, waiting for transfers between devices: 15.8 us -> none  [copy_for_each(): return lax.all_to_all(copies, axis, split_axis=0, concat_axis=0, tiled=True)]
    dot_general x4 -> x0, other arithmetic: 6.84 us -> none  [advance(): jnp.einsum('thk,shk,tshk->hts', window_query, window_admitted, decay_table)]
    all_gather x1, waiting for transfers between devices: 44.5 us -> 51.1 us  [shards(): kv_all = lax.all_gather(kv, SP, axis=0, tiled=True)]
  transfers between devices with their start and end apart: 2 -> 1, of which waited for: 2 -> 1; matrix products, arithmetic and copies ran while one was open for 4% -> 3% of each run, Pallas kernels for 0% -> 1%
where the time goes in v1:
time: 240 us
  blocking collectives  120 us (50%)
  waiting for transfers between devices  51.1 us (21%)
  Pallas kernels  37.1 us (15%)
  between operations  14.2 us (6%)
  matrix products  11.7 us (5%)
  local copies, waits for them, and re-layouts  3.62 us (2%)
    all_gather x4, blocking collectives, entering(): pieces = jax.tree.map(lambda part: lax.all_gather(part, axis), running)  79.8 us
    all_gather x1, waiting for transfers between devices, shards(): kv_all = lax.all_gather(kv, SP, axis=0, tiled=True)  51.1 us
    pallas_call x1, Pallas kernels, stick(): pl.pallas_call(stick_kernel, out_shape=jax.ShapeDtypeStruct((KB, 2 * HEAD...  34.2 us
    all_to_all x1, blocking collectives, copy_for_each(): return lax.all_to_all(copies, axis, split_axis=0, concat_axis=0, tiled=True)  20.1 us
    all_to_all x1, blocking collectives, summed_on_arrival(): lax.all_to_all(pieces, axis, split_axis=0, concat_axis=0, tiled=True)  20 us
  transfers between devices with their start and end apart: 1, of which 1 were waited for; matrix products, arithmetic and copies ran while one was open for 3% of the time, Pallas kernels for 1%

profile of v1, /device:TPU:480, one launch (start us, length us, event | category | flops | bytes accessed | tf_op | source)
XLA Modules:
  0.0 239.7 jit_solution(10346250943630144603)
XLA Ops:
  6.5 1.1 copy.34
  7.6 0.0 copy-start.5
  7.6 0.1 broadcast_in_dim.17
  7.7 20.1 %all_to_all.10 = bf16[8,256,256]{1,2,0:T(8,128)(2,1)S(1)} all-to-all(bf16[8,256,256]{1,2,0:T(8,128)(2,1)S(1)} %broadcast_in_dim.17), channel_id=1, replica_groups=mesh['sp_0'=16,'sp_1'=4,'tp'=8] {'tp'}, dimensions={0} | all-to-all | bytes 2097152 | tf_op jit(solution)/shard_map/all_to_all | solution.py:27
  27.8 0.3 multiply_reduce_fusion
  28.1 0.0 copy-start.6
  28.1 0.3 fusion.1
  28.4 0.3 copy-done.8
  28.7 0.5 fusion.4
  29.2 0.5 fusion.3
  29.7 0.7 pad_maximum_fusion
  30.4 0.0 all-gather.5.cloned.1.call-update
  31.1 0.8 copy.43.spike_ref
  31.9 0.5 fusion.2
  32.4 0.6 pad.4.q_ref
  33.1 1.1 fusion.7.input_ref
  34.2 1.1 fusion.5.query_ref
  35.3 1.1 fusion.6.forget_ref
  36.4 2.8 %local_scan.1 = (f32[256,64]{1,0:T(8,128)}, bf16[256,128]{1,0:T(8,128)(2,1)}, f32[64,128]{1,0:T(8,128)}, f32[1,128]{1,0:T(1,128)}) custom-call(bf16[256,128]{1,0:T(8,128)(2,1)} %fusion.5.query_ref, bf16[256,128]{1,0:T(8,128)(2,1)} %fusion.6.forget_ref, bf16[256,64]{1,0:T(8,128)(2,1)} %fusion.7.input_ref, f32[1,128]{1,0:T(1,128)} %low_ref.1, ...), custom_call_target="tpu_custom_call" | custom-call | tf_op jit(solution)/shard_map/local_scan/pallas_call | solution.py:187
  39.2 0.7 exponential_bitcast_fusion
  39.9 10.0 %all-gather.2 = f32[4,1,128]{2,1,0:T(1,128)S(1)} all-gather(f32[1,1,128]{2,1,0:T(1,128)S(1)} %exponential_bitcast_fusion), channel_id=2, replica_groups=mesh['sp_0'=16,'sp_1'=4,'tp'=8] {'sp_1'}, dimensions={0}, use_global_device_ids=true | all-gather | bytes 2560 | tf_op jit(solution)/shard_map/all_gather | solution.py:61
  49.9 25.7 %all_gather.26 = f32[16,1,128]{2,1,0:T(1,128)S(1)} all-gather(f32[1,1,128]{2,1,0:T(1,128)S(1)} %get-tuple-element.29), channel_id=1, replica_groups=mesh['sp_0'=16,'sp_1'=4,'tp'=8] {'sp_0'}, dimensions={0}, use_global_device_ids=true | all-gather | bytes 8704 | tf_op jit(solution)/shard_map/all_gather | solution.py:61
  75.6 12.2 %all-gather.1 = f32[256,128]{1,0:T(8,128)S(1)} all-gather(f32[64,128]{1,0:T(8,128)} %get-tuple-element.12), channel_id=3, replica_groups=mesh['sp_0'=16,'sp_1'=4,'tp'=8] {'sp_1'}, dimensions={0}, use_global_device_ids=true | all-gather | bytes 163840 | tf_op jit(solution)/shard_map/all_gather | solution.py:61
  87.9 31.9 %all_gather.29 = f32[16,64,128]{2,1,0:T(8,128)S(1)} all-gather(f32[1,64,128]{2,1,0:T(8,128)S(1)} %bitcast_add_fusion), channel_id=1, replica_groups=mesh['sp_0'=16,'sp_1'=4,'tp'=8] {'sp_0'}, dimensions={0}, use_global_device_ids=true | all-gather | bytes 557056 | tf_op jit(solution)/shard_map/all_gather | solution.py:61
  119.8 1.3 multiply_reduce_fusion.1
  121.1 51.1 %all-gather.5.cloned.1.call-done.kv_ref = bf16[16384,128]{1,0:T(8,128)(2,1)} async-done(((bf16[256,128]{1,0:T(8,128)(2,1)}), bf16[16384,128]{1,0:T(8,128)(2,1)}) %all-gather.5.cloned.1.call-update) | async-done | bytes 4194320 | tf_op jit(solution)/shard_map/all_gather | solution.py:240
  172.2 34.2 %stick.1 = bf16[256,128]{1,0:T(8,128)(2,1)} custom-call(s32[1]{0:T(128)} %bitcast.pos_ref, f32[1]{0:T(128)S(6)} %copy.57.bias_ref, bf16[256,128]{1,0:T(8,128)(2,1)} %pad.4.q_ref, bf16[16384,128]{1,0:T(8,128)(2,1)} %all-gather.5.cloned.1.call-done.kv_ref), custom_call_target="tpu_custom_call" | custom-call | tf_op jit(solution)/shard_map/stick/pallas_call | solution.py:129
  206.4 2.7 %fusion.12 = f32[256,2048]{1,0:T(8,128)} fusion(bf16[64,2048]{1,0:T(8,128)(2,1)S(1)} %copy-done.2, bf16[256,128]{1,0:T(8,128)(2,1)} %stick.1), kind=kOutput, calls=%fused_computation.26 | convolution fusion | flops 67108864 | bytes 2424832 | tf_op jit(solution)/shard_map/dot_general | solution.py:261
  209.1 2.9 %fusion = bf16[256,2048]{1,0:T(8,128)(2,1)S(1)} fusion(f32[256,2048]{1,0:T(8,128)} %fusion.12, bf16[64,2048]{1,0:T(8,128)(2,1)S(1)} %copy-done.3, bf16[256,2048]{0,1:T(8,128)(2,1)S(1)} %fusion.1, bf16[2048,64]{0,1:T(8,128)(2,1)S(1)} %copy-done.4, f32[256,64]{1,0:T(8,128)S(1)} %get-tuple-element.36, f32[256]{0:T(256)S(1)} %add_rsqrt_fusion.1, ...), kind=kOutput, calls=%fused_computation.1 | convolution fusion | flops 135446528 | bytes 4786432 | tf_op jit(solution)/shard_map/dot_general | solution.py:262
  212.1 0.1 copy.56
  212.1 20.0 %all_to_all.11 = bf16[8,256,256]{2,1,0:T(8,128)(2,1)S(1)} all-to-all(bf16[8,256,256]{2,1,0:T(8,128)(2,1)S(1)} %bitcast.253), channel_id=1, replica_groups=mesh['sp_0'=16,'sp_1'=4,'tp'=8] {'tp'}, dimensions={0} | all-to-all | bytes 2097152 | tf_op jit(solution)/shard_map/all_to_all | solution.py:79
  232.1 0.8 reduce_sum.32
  (28 shorter events, 0.1 us)
Async XLA Ops:
  6.5 27.7 %copy-start = (bf16[2048,128]{1,0:T(8,128)(2,1)S(1)}, bf16[2048,128]{1,0:T(8,128)(2,1)}, u32[]{:S(2)}) copy-start(bf16[2048,128]{1,0:T(8,128)(2,1)} %param.21) | copy-start | bytes 1572868
  6.5 165.6 %all-gather.5.cloned.1.call-start = ((), (), s32[]{:S(2)}) async-start(), calls=%async_computation.2 | async-start | bytes 4259840 | tf_op jit(solution)/shard_map/all_gather | solution.py:240
  7.6 20.5 %copy-start.5 = (f32[2048]{0:T(1024)S(1)}, f32[2048]{0:T(1024)}, u32[]{:S(2)}) copy-start(f32[2048]{0:T(1024)} %param.16) | copy-start | bytes 24580
  27.8 1.0 copy-start.8
  27.8 1.4 copy-start.9
  28.1 3.0 %copy-start.6 = (f32[256,1]{0,1:T(1,128)S(1)}, f32[256,1]{0,1:T(1,128)}, u32[]{:S(2)}) copy-start(f32[256,1]{0,1:T(1,128)} %param.26) | copy-start | bytes 3076
  28.7 3.2 %copy-start.10 = (bf16[2048,64]{0,1:T(8,128)(2,1)S(1)}, bf16[2048,64]{0,1:T(8,128)(2,1)}, u32[]{:S(2)}) copy-start(bf16[2048,64]{0,1:T(8,128)(2,1)} %param.17) | copy-start | bytes 786436
  28.7 4.4 %copy-start.11 = (bf16[2048,64]{0,1:T(8,128)(2,1)S(1)}, bf16[2048,64]{0,1:T(8,128)(2,1)}, u32[]{:S(2)}) copy-start(bf16[2048,64]{0,1:T(8,128)(2,1)} %param.23) | copy-start | bytes 786436
  31.9 3.3 %copy-start.1 = (bf16[2048,128]{1,0:T(8,128)(2,1)S(1)}, bf16[2048,128]{1,0:T(8,128)(2,1)}, u32[]{:S(2)}) copy-start(bf16[2048,128]{1,0:T(8,128)(2,1)} %param.22) | copy-start | bytes 1572868
  172.2 34.2 %copy-start.2 = (bf16[64,2048]{1,0:T(8,128)(2,1)S(1)}, bf16[64,2048]{1,0:T(8,128)(2,1)}, u32[]{:S(2)}) copy-start(bf16[64,2048]{1,0:T(8,128)(2,1)} %param.28) | copy-start | bytes 786436
  206.4 2.7 %copy-start.3 = (bf16[64,2048]{1,0:T(8,128)(2,1)S(1)}, bf16[64,2048]{1,0:T(8,128)(2,1)}, u32[]{:S(2)}) copy-start(bf16[64,2048]{1,0:T(8,128)(2,1)} %param.29) | copy-start | bytes 786436
  206.4 2.7 %copy-start.4 = (bf16[2048,64]{0,1:T(8,128)(2,1)S(1)}, bf16[2048,64]{0,1:T(8,128)(2,1)}, u32[]{:S(2)}) copy-start(bf16[2048,64]{0,1:T(8,128)(2,1)} %param.24) | copy-start | bytes 786436
  206.4 2.7 %copy-start.7 = (f32[64]{0:T(128)S(1)}, f32[64]{0:T(128)}, u32[]{:S(2)}) copy-start(f32[64]{0:T(128)} %param.27) | copy-start | bytes 772
Sparse Core Ops, SparseCore 0:
  30.6 141.5 all-gather.4

commit v2 on v1

v2 whole, which is shorter than its diff:
```python
import functools

import jax
import jax.numpy as jnp
from jax import lax
from jax.experimental import pallas as pl
from jax.experimental.pallas import tpu as pltpu
from jax.sharding import PartitionSpec as P

D = 2048
HEAD = 64
REC_KEY = 128
REC_VAL = 64
REC_SPAN = 64
TOK = 256
LOG2E = 1.4426950408889634
EARLY = 192
STATE_ROWS = REC_VAL + 8
epsilon = 1e-06
F32, BF16 = jnp.float32, jnp.bfloat16
VMEM = pl.BlockSpec(memory_space=pltpu.VMEM)
SMEM = pl.BlockSpec(memory_space=pltpu.SMEM)
ANY = pl.BlockSpec(memory_space=pl.ANY)
MESH = pl.DeviceIdType.MESH


def dot(a, b, ta=False, tb=False):
    dims = (((0 if ta else 1,), (1 if tb else 0,)), ((), ()))
    return lax.dot_general(a, b, dims, preferred_element_type=F32)


def to(src, dst, send, recv, sp):
    return pltpu.make_async_remote_copy(
        src_ref=src, dst_ref=dst, send_sem=send, recv_sem=recv,
        device_id={"sp": sp}, device_id_type=MESH,
    )


def place():
    sp = lax.axis_index("sp")
    return sp, sp // 16, (sp // 4) % 4, sp % 4


def greet(peers):
    barrier = pltpu.get_barrier_semaphore()
    for peer in peers:
        pl.semaphore_signal(barrier, inc=1, device_id={"sp": peer}, device_id_type=MESH)
    pl.semaphore_wait(barrier, len(peers))


def share_kernel(
    kv_ref, kv_hbm, query_ref, state_ref,
    early_ref, late_ref, queries_ref, before_ref, group_ref,
    rows_ref, planes_ref, send, recv, query_send, query_recv, own_sem,
):
    sp, c, zl, y = place()
    base = c * 16
    in_row = [base + zl * 4 + (y + d) % 4 for d in (1, 2, 3)]
    in_line = [base + ((zl + d) % 4) * 4 + y for d in (1, 2, 3)]
    far = [(sp + 16 * d) % 64 for d in (1, 2, 3)]
    own_early = pltpu.make_async_copy(kv_hbm.at[0:EARLY], early_ref.at[y, zl], own_sem.at[0])
    own_late = pltpu.make_async_copy(kv_hbm.at[EARLY:TOK], late_ref.at[zl, y], own_sem.at[1])
    own_early.start()
    own_late.start()
    rows_ref[y] = state_ref[...]
    greet(in_row + in_line + far)

    def step(n, src, dst, peers):
        return [to(src, dst, send.at[n, d], recv.at[n, d], peers[d]) for d in range(3)]

    first = (
        step(0, kv_ref.at[0:EARLY], early_ref.at[y, zl], in_line)
        + step(1, kv_ref.at[EARLY:TOK], late_ref.at[zl, y], in_row)
        + step(2, state_ref, rows_ref.at[y], in_row)
    )
    for copy in first:
        copy.start()
    for d in (1, 2, 3):

        @pl.when(c >= d)
        def _():
            to(
                query_ref, queries_ref.at[c - 1], query_send.at[d - 1], query_recv.at[c - 1], sp - 16 * d
            ).start()

    own_early.wait()
    own_late.wait()
    for copy in first:
        copy.wait_recv()
    second = step(3, early_ref.at[y], early_ref.at[y], in_row) + step(
        4, late_ref.at[zl], late_ref.at[zl], in_line
    )
    for copy in second:
        copy.start()
    state = rows_ref[0, 0:REC_VAL, :]
    total = rows_ref[0, REC_VAL : REC_VAL + 1, :]
    ahead = jnp.zeros_like(state)
    ahead_total = jnp.zeros_like(total)
    for n in range(1, 4):
        ahead = jnp.where(n <= y, state, ahead)
        ahead_total = jnp.where(n <= y, total, ahead_total)
        more = rows_ref[n, REC_VAL : REC_VAL + 1, :]
        state = state * jnp.exp(more) + rows_ref[n, 0:REC_VAL, :]
        total = total + more
    planes_ref[zl, 0:REC_VAL, :] = state
    planes_ref[zl, REC_VAL:STATE_ROWS, :] = jnp.broadcast_to(total, (8, REC_KEY))
    third = step(5, planes_ref.at[zl], planes_ref.at[zl], in_line)
    for copy in third:
        copy.start()
    for copy in third:
        copy.wait_recv()
    state = planes_ref[0, 0:REC_VAL, :]
    total = planes_ref[0, REC_VAL : REC_VAL + 1, :]
    low = jnp.zeros_like(state)
    low_total = jnp.zeros_like(total)
    for n in range(1, 4):
        low = jnp.where(n <= zl, state, low)
        low_total = jnp.where(n <= zl, total, low_total)
        more = planes_ref[n, REC_VAL : REC_VAL + 1, :]
        state = state * jnp.exp(more) + planes_ref[n, 0:REC_VAL, :]
        total = total + more
    group_ref[0:REC_VAL, :] = state
    group_ref[REC_VAL:STATE_ROWS, :] = jnp.broadcast_to(total, (8, REC_KEY))
    before_ref[0:REC_VAL, :] = low * jnp.exp(ahead_total) + ahead
    before_ref[REC_VAL:STATE_ROWS, :] = jnp.broadcast_to(low_total + ahead_total, (8, REC_KEY))
    for copy in second:
        copy.wait_recv()
    for n in (1, 2, 3):

        @pl.when(c < n)
        def _():
            to(
                query_ref, queries_ref.at[n - 1], query_send.at[0], query_recv.at[n - 1], sp
            ).wait_recv()

    for copy in first + second + third:
        copy.wait_send()
    for d in (1, 2, 3):

        @pl.when(c >= d)
        def _():
            to(
                query_ref, queries_ref.at[c - 1], query_send.at[d - 1], query_recv.at[c - 1], sp - 16 * d
            ).wait_send()


def share(kv, query, state):
    dma = pltpu.SemaphoreType.DMA
    return pl.pallas_call(
        share_kernel,
        out_shape=(
            jax.ShapeDtypeStruct((4, 4, EARLY, 128), BF16),
            jax.ShapeDtypeStruct((4, 4, TOK - EARLY, 128), BF16),
            jax.ShapeDtypeStruct((3, 128, 128), BF16),
            jax.ShapeDtypeStruct((STATE_ROWS, REC_KEY), F32),
            jax.ShapeDtypeStruct((STATE_ROWS, REC_KEY), F32),
        ),
        in_specs=[VMEM, ANY, VMEM, VMEM],
        out_specs=(VMEM,) * 5,
        scratch_shapes=[
            pltpu.VMEM((4, STATE_ROWS, REC_KEY), F32),
            pltpu.VMEM((4, STATE_ROWS, REC_KEY), F32),
            dma((6, 3)), dma((6, 3)), dma((3,)), dma((3,)), dma((2,)),
        ],
        compiler_params=pltpu.CompilerParams(collective_id=0, has_side_effects=True),
        name="share",
    )(kv, kv, query, state)


def stick_tile(q, kv, tri, bias2, keep=None):
    z = dot(q, kv, tb=True) * (LOG2E / 8.0) + bias2
    soft = jnp.maximum(z, jnp.log(1.0 + jnp.exp2(jnp.minimum(z, 30.0))) * LOG2E)
    if keep is not None:
        soft = jnp.where(keep, soft, 0.0)
    later = dot(soft.astype(BF16), tri)
    return z, soft, later


def stick_kernel(
    bias_ref, query_ref, queries_ref, early_ref, late_ref,
    own_ref, own_left_ref, far_ref, far_left_ref,
    q_ref, tri_ref, acc_ref, left_ref,
):
    sp, c, zl, y = place()
    here = zl * 4 + y
    bias2 = bias_ref[0] * LOG2E
    rows = lax.broadcasted_iota(jnp.int32, (TOK, TOK), 0)
    cols = lax.broadcasted_iota(jnp.int32, (TOK, TOK), 1)
    tri_ref[...] = jnp.where(rows > cols, -1.0, 0.0).astype(BF16)
    acc_ref[...] = jnp.zeros_like(acc_ref)
    left_ref[...] = jnp.zeros_like(left_ref)
    lane = lax.broadcasted_iota(jnp.int32, (128, 128), 1)
    for n in range(4):
        packed = (query_ref[...] if n == 0 else queries_ref[n - 1]).astype(F32)
        for half in range(2):
            part = packed if half == 0 else pltpu.roll(packed, 64, 1)
            at = n * TOK + half * 128
            q_ref[at : at + 128, :] = jnp.where(lane < HEAD, part, 0.0).astype(BF16)

    def pair(i, _):
        tri = tri_ref[...]
        q_own, q_far = q_ref[0:TOK, :], q_ref[TOK:, :]
        kvs, own, far = [], [], []
        for u in range(2):
            m = 15 - 2 * i - u
            kv = jnp.concatenate([early_ref[m % 4, m // 4], late_ref[m // 4, m % 4]], axis=0)
            keep = cols - rows < (here - m) * TOK
            kvs.append(kv)
            own.append(stick_tile(q_own, kv, tri, bias2, keep) + (keep,))
            far.append(stick_tile(q_far, kv, tri, bias2))
        left_own, left_far = left_ref[0:TOK, 0:1], left_ref[TOK:, 0:1]
        acc_own, acc_far = acc_ref[0:TOK, :], acc_ref[TOK:, :]
        for u in range(2):
            z, soft, later, keep = own[u]
            weight = jnp.where(keep, jnp.exp2((z - soft) + (later + left_own)), 0.0)
            acc_own = acc_own + dot(weight.astype(BF16), kvs[u])
            left_own = left_own + (later[:, 0:1] - soft[:, 0:1])
            z, soft, later = far[u]
            weight = jnp.exp2((z - soft) + (later + left_far))
            acc_far = acc_far + dot(weight.astype(BF16), kvs[u])
            left_far = left_far + (later[:, 0:1] - soft[:, 0:1])
        acc_ref[0:TOK, :] = acc_own
        acc_ref[TOK:, :] = acc_far
        left_ref[0:TOK, :] = jnp.broadcast_to(left_own, (TOK, 128))
        left_ref[TOK:, :] = jnp.broadcast_to(left_far, (3 * TOK, 128))
        return 0

    lax.fori_loop(0, 8, pair, 0)
    own_ref[...] = acc_ref[0:TOK, :]
    own_left_ref[...] = left_ref[0:TOK, :]
    for n in range(3):
        at = (n + 1) * TOK
        top = acc_ref[at : at + 128, :]
        low = pltpu.roll(acc_ref[at + 128 : at + 256, :], 64, 1)
        far_ref[n] = jnp.where(lane < HEAD, low, top).astype(BF16)
        for half in range(2):
            turned = jnp.transpose(left_ref[at + half * 128 : at + half * 128 + 128, :])
            far_left_ref[n, :, half * 128 : half * 128 + 128] = turned[0:8, :]


def stick(bias, query, queries, early, late):
    return pl.pallas_call(
        stick_kernel,
        out_shape=(
            jax.ShapeDtypeStruct((TOK, 128), F32),
            jax.ShapeDtypeStruct((TOK, 128), F32),
            jax.ShapeDtypeStruct((3, 128, 128), BF16),
            jax.ShapeDtypeStruct((3, 8, TOK), F32),
        ),
        in_specs=[SMEM, VMEM, VMEM, VMEM, VMEM],
        out_specs=(VMEM,) * 4,
        scratch_shapes=[
            pltpu.VMEM((4 * TOK, 128), BF16),
            pltpu.VMEM((TOK, TOK), BF16),
            pltpu.VMEM((4 * TOK, 128), F32),
            pltpu.VMEM((4 * TOK, 128), F32),
        ],
        name="stick",
    )(bias, query, queries, early, late)


def finish_kernel(
    own_ref, own_left_ref, far_ref, far_left_ref, before_ref, group_ref,
    local_ref, faded_ref, gate_ref, gain_ref,
    heads_ref,
    part_ref, part_left_ref, states_ref, acc_ref, left_ref, in_ref, send, recv,
):
    sp, c, zl, y = place()
    greet([(sp + 16 * d) % 64 for d in (1, 2, 3)])

    def copies(n, there, to_sp):
        pairs = (
            (far_ref.at[there - 1], part_ref.at[c]),
            (far_left_ref.at[there - 1], part_left_ref.at[c]),
            (group_ref, states_ref.at[c]),
        )
        return [
            to(src, dst, send.at[k, n], recv.at[k, c], to_sp) for k, (src, dst) in enumerate(pairs)
        ]

    def arrivals(source):
        pairs = ((far_ref.at[0], part_ref), (far_left_ref.at[0], part_left_ref), (group_ref, states_ref))
        return [
            to(src, dst.at[source], send.at[k, 0], recv.at[k, source], sp)
            for k, (src, dst) in enumerate(pairs)
        ]

    for d in (1, 2, 3):

        @pl.when(c + d < 4)
        def _():
            for copy in copies(d - 1, c + d, sp + 16 * d):
                copy.start()

    acc_ref[...] = own_ref[...]
    left_ref[...] = own_left_ref[...]
    in_ref[...] = jnp.zeros_like(in_ref)
    for g in (2, 1, 0):

        @pl.when(g < c)
        def _():
            for copy in arrivals(g)[0:2]:
                copy.wait_recv()
            packed = part_ref[g].astype(F32)
            scale = jnp.exp2(left_ref[...])
            acc_ref[0:128, :] += packed * scale[0:128, :]
            acc_ref[128:256, :] += pltpu.roll(packed, 64, 1) * scale[128:256, :]
            for half in range(2):
                at = slice(half * 128, half * 128 + 128)
                flat = jnp.broadcast_to(part_left_ref[g, 0:1, at], (128, 128))
                left_ref[at, :] += jnp.transpose(flat)

    for g in (0, 1, 2):

        @pl.when(g < c)
        def _():
            arrivals(g)[2].wait_recv()
            in_ref[...] = in_ref[...] * jnp.exp(states_ref[g, REC_VAL : REC_VAL + 1, :]) + states_ref[
                g, 0:REC_VAL, :
            ]

    state = in_ref[...] * jnp.exp(before_ref[REC_VAL : REC_VAL + 1, :]) + before_ref[0:REC_VAL, :]
    raw = local_ref[...] + dot(faded_ref[...], state.astype(BF16), tb=True)
    normed = raw * lax.rsqrt(jnp.mean(raw * raw, axis=1, keepdims=True) + epsilon) * gain_ref[...]
    gate = gate_ref[...].astype(F32)
    state_heads = normed * (gate * jax.nn.sigmoid(gate))
    heads_ref[:, 0:REC_VAL] = state_heads.astype(BF16)
    heads_ref[:, REC_VAL:] = acc_ref[:, HEAD:].astype(BF16)
    for d in (1, 2, 3):

        @pl.when(c + d < 4)
        def _():
            for copy in copies(d - 1, c + d, sp + 16 * d):
                copy.wait_send()


def finish(*operands):
    dma = pltpu.SemaphoreType.DMA
    return pl.pallas_call(
        finish_kernel,
        out_shape=jax.ShapeDtypeStruct((TOK, 128), BF16),
        in_specs=[VMEM] * 10,
        out_specs=VMEM,
        scratch_shapes=[
            pltpu.VMEM((3, 128, 128), BF16),
            pltpu.VMEM((3, 8, TOK), F32),
            pltpu.VMEM((3, STATE_ROWS, REC_KEY), F32),
            pltpu.VMEM((TOK, 128), F32),
            pltpu.VMEM((TOK, 128), F32),
            pltpu.VMEM((REC_VAL, REC_KEY), F32),
            dma((3, 3)), dma((3, 3)),
        ],
        compiler_params=pltpu.CompilerParams(collective_id=1, has_side_effects=True),
        name="finish",
    )(*operands)


def scan_kernel(query_ref, forget_ref, input_ref, low_ref, spike_ref, out_ref, lift_ref, state_ref):
    span = REC_SPAN
    rows = lax.broadcasted_iota(jnp.int32, (span, span), 0)
    cols = lax.broadcasted_iota(jnp.int32, (span, span), 1)
    causal = cols <= rows
    ones = jnp.where(causal, 1.0, 0.0)
    state = jnp.zeros((REC_VAL, REC_KEY), F32)
    offset = jnp.zeros((1, REC_KEY), F32)
    for n in range(query_ref.shape[0] // span):
        at = slice(n * span, (n + 1) * span)
        query = query_ref[at, :].astype(F32)
        lifted = query * jax.nn.sigmoid(query)
        intake = (1.0 - low_ref[...]) * jax.nn.sigmoid(-forget_ref[at, :].astype(F32))
        log_forget = jnp.log1p(-intake) + spike_ref[at, :]
        running = lax.dot_general(
            ones, log_forget, (((1,), (0,)), ((), ())),
            precision=lax.Precision.HIGHEST, preferred_element_type=F32,
        )
        total = running[span - 1 : span, :]
        middle = running[span // 2 - 1 : span // 2, :]
        value = input_ref[at, :]
        grown = (lifted * jnp.exp(running - middle)).astype(BF16)
        shrunk = (intake * jnp.exp(middle - running)).astype(BF16)
        inner = jnp.where(causal, dot(grown, shrunk, tb=True), 0.0)
        faded = (lifted * jnp.exp(running)).astype(BF16)
        out_ref[at, :] = dot(inner.astype(BF16), value) + dot(faded, state.astype(BF16), tb=True)
        lift_ref[at, :] = (lifted * jnp.exp(running + offset)).astype(BF16)
        kept = (intake * jnp.exp(total - running)).astype(BF16)
        state = state * jnp.exp(total) + dot(value, kept, ta=True)
        offset = offset + total
    state_ref[0:REC_VAL, :] = state
    state_ref[REC_VAL:STATE_ROWS, :] = jnp.broadcast_to(offset, (8, REC_KEY))


def local_scan(query, forget, inputs, low, spikes):
    n = query.shape[0]
    return pl.pallas_call(
        scan_kernel,
        out_shape=(
            jax.ShapeDtypeStruct((n, REC_VAL), F32),
            jax.ShapeDtypeStruct((n, REC_KEY), BF16),
            jax.ShapeDtypeStruct((STATE_ROWS, REC_KEY), F32),
        ),
        in_specs=[VMEM] * 5,
        out_specs=(VMEM,) * 3,
        name="local_scan",
    )(query, forget, inputs, low, spikes)


def gathered_copies(array, axis, dim):
    copies = jnp.broadcast_to(array, (lax.axis_size(axis), *array.shape))
    pieces = lax.all_to_all(copies, axis, split_axis=0, concat_axis=0, tiled=True)
    lengths = list(array.shape)
    lengths[dim] *= pieces.shape[0]
    return jnp.moveaxis(pieces, 0, dim).reshape(lengths)


def summed_on_arrival(array, axis, dim):
    size, lengths = lax.axis_size(axis), array.shape
    pieces = array.reshape(*lengths[:dim], size, lengths[dim] // size, *lengths[dim + 1 :])
    pieces = jnp.moveaxis(pieces, dim, 0)
    arrived = lax.all_to_all(pieces, axis, split_axis=0, concat_axis=0, tiled=True)
    return arrived.astype(F32).sum(axis=0)


def shards(
    tokens,
    input_norm_gain,
    attention_query_weight,
    attention_key_weight,
    attention_value_weight,
    attention_score_bias,
    recurrence_query_weight,
    forget_weight,
    input_weight,
    output_gate_weight,
    forget_minimum,
    decay_spikes,
    head_norm_gain,
    attention_output_weight,
    recurrence_output_weight,
):
    values = gathered_copies(tokens, "tp", 1).astype(F32)
    scaled = (values * input_norm_gain[None, :]).astype(BF16)
    weights = (
        attention_query_weight,
        attention_key_weight,
        attention_value_weight,
        recurrence_query_weight,
        forget_weight,
        input_weight,
        output_gate_weight,
    )
    inverse = lax.rsqrt(jnp.sum(values * values, axis=1) / D + epsilon)[:, None]
    query_stick, key_stick, value_stick, query_rows, forget_rows, input_rows, gate_rows = (
        (jnp.dot(scaled, weight, preferred_element_type=F32) * inverse).astype(BF16)
        for weight in weights
    )
    kv = jnp.concatenate([key_stick, value_stick], axis=1)
    query = jnp.concatenate([query_stick[0:128], query_stick[128:256]], axis=1)
    local_out, faded, state = local_scan(
        query_rows, forget_rows, input_rows, forget_minimum, decay_spikes
    )
    early, late, queries, before, group = share(kv, query, state)
    own, own_left, far, far_left = stick(attention_score_bias, query, queries, early, late)
    heads = finish(
        own, own_left, far, far_left, before, group, local_out, faded, gate_rows, head_norm_gain[None, :]
    )
    output_weight = jnp.concatenate([recurrence_output_weight, attention_output_weight], axis=0)
    partial_out = jnp.dot(heads, output_weight, preferred_element_type=F32)
    return summed_on_arrival(partial_out.astype(BF16), "tp", 1).astype(BF16)


def solution(mesh):
    placed = (
        P("sp", "tp"),
        P(),
        P(None, "tp"),
        P(None, "tp"),
        P(None, "tp"),
        P("tp"),
        P(None, "tp"),
        P(None, "tp"),
        P(None, "tp"),
        P(None, "tp"),
        P("tp", None),
        P("sp", "tp"),
        P(),
        P("tp", None),
        P("tp", None),
    )
    return jax.shard_map(
        shards, mesh=mesh, in_specs=placed, out_specs=P("sp", "tp"), check_vma=False
    )
```

time: 240 us -> 126 us (0.53)
  the two profiles are of different devices: /device:TPU:480 before, /device:TPU:1 now
where the time goes in v2:
time: 126 us
  Pallas kernels  58.2 us (46%)
  blocking collectives  29.5 us (23%)
  waiting for transfers between devices  13.5 us (11%)
  starting transfers between devices  10.4 us (8%)
  matrix products  7.15 us (6%)
  local copies, waits for them, and re-layouts  3.47 us (3%)
  other arithmetic  2.86 us (2%)
    all_to_all x1, blocking collectives, summed_on_arrival(): lax.all_to_all(pieces, axis, split_axis=0, concat_axis=0, tiled=True)  29.5 us
    pallas_call x1, Pallas kernels, share(): pl.pallas_call(share_kernel, out_shape=(jax.ShapeDtypeStruct((4, 4, EARLY...  27.6 us
    pallas_call x1, Pallas kernels, stick(): pl.pallas_call(stick_kernel, out_shape=(jax.ShapeDtypeStruct((TOK, 128),...  16.7 us
    all_to_all x1, waiting for transfers between devices, gathered_copies(): lax.all_to_all(copies, axis, split_axis=0, concat_axis=0, tiled=True)  13.5 us
    pallas_call x1, Pallas kernels, finish(): pl.pallas_call(finish_kernel, out_shape=jax.ShapeDtypeStruct((TOK, 128),...  11 us
    all_to_all x1, starting transfers between devices, gathered_copies(): lax.all_to_all(copies, axis, split_axis=0, concat_axis=0, tiled=True)  10.4 us
    dot_general x7, matrix products, shards(): jnp.dot(scaled, weight, preferred_element_type=F32) * inverse  5.89 us
    pallas_call x1, Pallas kernels, local_scan(): pl.pallas_call(scan_kernel, out_shape=(jax.ShapeDtypeStruct((n, REC_VAL),...  2.85 us
  transfers between devices with their start and end apart: 1, of which 1 were waited for; matrix products, arithmetic and copies ran while one was open for 1% of the time, Pallas kernels for 0%

profile of v2, /device:TPU:1, one launch (start us, length us, event | category | flops | bytes accessed | tf_op | source)
XLA Modules:
  0.0 125.9 jit_solution(12620367474044030851)
XLA Ops:
  0.0 0.0 copy-start
  0.0 1.1 copy.35
  1.1 1.0 broadcast_in_dim.8
  2.1 10.4 %all-to-all-start = ((bf16[8,256,256]{1,2,0:T(8,128)(2,1)}), bf16[8,256,256]{1,2,0:T(8,128)(2,1)S(1)}, u32[]{:S(2)}, u32[]{:S(2)}) async-start(bf16[8,256,256]{1,2,0:T(8,128)(2,1)} %broadcast_in_dim.8), calls=%async_computation | async-start | bytes 2097152 | tf_op jit(solution)/shard_map/all_to_all | solution.py:409
  13.2 0.0 copy-done.5
  13.2 0.8 copy.44.spike_ref
  14.0 13.5 %all-to-all-done = bf16[8,256,256]{1,2,0:T(8,128)(2,1)S(1)} async-done(((bf16[8,256,256]{1,2,0:T(8,128)(2,1)}), bf16[8,256,256]{1,2,0:T(8,128)(2,1)S(1)}, u32[]{:S(2)}, u32[]{:S(2)}) %all-to-all-start) | async-done | bytes 1048608 | tf_op jit(solution)/shard_map/all_to_all | solution.py:409
  27.5 0.3 multiply_reduce_fusion
  27.9 0.0 copy-done.4
  27.9 0.3 fusion
  28.2 0.0 copy-done
  28.2 0.0 copy-start.6
  28.2 1.1 fusion.5.forget_ref
  29.3 0.0 copy-done.6
  29.3 0.5 fusion.2
  29.8 0.5 copy-done.7
  30.3 0.5 fusion.3
  30.8 0.0 copy-start.1
  30.8 1.1 fusion.6.input_ref
  31.9 1.1 fusion.7.gate_ref
  33.0 1.1 fusion.4.query_ref
  34.1 0.5 fusion.1
  34.6 0.7 pad_maximum_fusion.kv_ref.kv_hbm
  35.4 0.7 pad_maximum_fusion.1.query_ref
  36.0 2.9 %local_scan.1 = (f32[256,64]{1,0:T(8,128)}, bf16[256,128]{1,0:T(8,128)(2,1)}, f32[72,128]{1,0:T(8,128)}) custom-call(bf16[256,128]{1,0:T(8,128)(2,1)} %fusion.4.query_ref, bf16[256,128]{1,0:T(8,128)(2,1)} %fusion.5.forget_ref, bf16[256,64]{1,0:T(8,128)(2,1)} %fusion.6.input_ref, f32[1,128]{1,0:T(1,128)} %low_ref.1, f32[256,1]{1,0:T(8,128)} %copy.44.spike_ref), custom_call_target="tpu_custom_call" | custom-call | tf_op jit(solution)/shard_map/local_scan/pallas_call | solution.py:394
  38.9 27.6 %share.1 = (bf16[4,4,192,128]{3,2,1,0:T(8,128)(2,1)}, bf16[4,4,64,128]{3,2,1,0:T(8,128)(2,1)}, bf16[3,128,128]{2,1,0:T(8,128)(2,1)}, f32[72,128]{1,0:T(8,128)}, f32[72,128]{1,0:T(8,128)}) custom-call(bf16[256,128]{1,0:T(8,128)(2,1)} %pad_maximum_fusion.kv_ref.kv_hbm, bf16[256,128]{1,0:T(8,128)(2,1)} %pad_maximum_fusion.kv_ref.kv_hbm, ...), custom_call_target="tpu_custom_call" | custom-call | tf_op jit(solution)/shard_map/share/pallas_call | solution.py:149
  66.5 16.7 %stick.1 = (f32[256,128]{1,0:T(8,128)}, f32[256,128]{1,0:T(8,128)}, bf16[3,128,128]{2,1,0:T(8,128)(2,1)}, f32[3,8,256]{2,1,0:T(8,128)}) custom-call(f32[1]{0:T(128)S(6)} %copy.56.bias_ref, bf16[128,128]{1,0:T(8,128)(2,1)} %pad_maximum_fusion.1.query_ref, bf16[3,128,128]{2,1,0:T(8,128)(2,1)} %get-tuple-element.18.queries_ref, ...), custom_call_target="tpu_custom_call" | custom-call | tf_op jit(solution)/shard_map/stick/pallas_call | solution.py:242
  83.2 11.0 %finish.1 = bf16[256,128]{1,0:T(8,128)(2,1)} custom-call(f32[256,128]{1,0:T(8,128)} %get-tuple-element.21.own_ref, f32[256,128]{1,0:T(8,128)} %get-tuple-element.22.own_left_ref, bf16[3,128,128]{2,1,0:T(8,128)(2,1)} %get-tuple-element.23.far_ref, f32[3,8,256]{2,1,0:T(8,128)} %get-tuple-element.24.far_left_ref, f32[72,128]{1,0:T(8,128)} %get-tuple-element.25.before_ref, ...), custom_call_target="tpu_custom_call" | custom-call | tf_op jit(solution)/shard_map/finish/pallas_call | solution.py:339
  94.3 1.3 %convolution_convert_fusion = bf16[256,2048]{1,0:T(8,128)(2,1)S(1)} fusion(bf16[256,128]{1,0:T(8,128)(2,1)} %finish.1, bf16[64,2048]{1,0:T(8,128)(2,1)S(1)} %copy-done.2, bf16[64,2048]{1,0:T(8,128)(2,1)S(1)} %copy-done.3), kind=kOutput, calls=%fused_computation | convolution fusion | flops 135790592 | bytes 1638400 | tf_op jit(solution)/shard_map/dot_general | solution.py:467
  95.5 0.1 copy.55
  95.6 29.5 %all_to_all.10 = bf16[8,256,256]{2,1,0:T(8,128)(2,1)S(1)} all-to-all(bf16[8,256,256]{2,1,0:T(8,128)(2,1)S(1)} %bitcast.30), channel_id=1, replica_groups=mesh['sp'=64,'tp'=8] {'tp'}, dimensions={0} | all-to-all | bytes 2097152 | tf_op jit(solution)/shard_map/all_to_all | solution.py:419
  125.1 0.8 reduce_sum.22
  (16 shorter events, 0.0 us)
Async XLA Ops:
  0.0 28.2 %copy-start = (bf16[2048,128]{1,0:T(8,128)(2,1)S(1)}, bf16[2048,128]{1,0:T(8,128)(2,1)}, u32[]{:S(2)}) copy-start(bf16[2048,128]{1,0:T(8,128)(2,1)} %param.22) | copy-start | bytes 1572868
  2.1 11.1 %copy-start.5 = (f32[256,1]{0,1:T(1,128)S(1)}, f32[256,1]{0,1:T(1,128)}, u32[]{:S(2)}) copy-start(f32[256,1]{0,1:T(1,128)} %param.26) | copy-start | bytes 3076
  2.1 25.4 %all-to-all-start = ((bf16[8,256,256]{1,2,0:T(8,128)(2,1)}), bf16[8,256,256]{1,2,0:T(8,128)(2,1)S(1)}, u32[]{:S(2)}, u32[]{:S(2)}) async-start(bf16[8,256,256]{1,2,0:T(8,128)(2,1)} %broadcast_in_dim.8), calls=%async_computation | async-start | bytes 2097152 | tf_op jit(solution)/shard_map/all_to_all | solution.py:409
  12.5 15.3 %copy-start.4 = (f32[2048]{0:T(1024)S(1)}, f32[2048]{0:T(1024)}, u32[]{:S(2)}) copy-start(f32[2048]{0:T(1024)} %param.16) | copy-start | bytes 24580
  28.2 1.1 copy-start.6
  29.3 1.0 copy-start.7
  29.3 1.4 %copy-start.8 = (bf16[2048,64]{0,1:T(8,128)(2,1)S(1)}, bf16[2048,64]{0,1:T(8,128)(2,1)}, u32[]{:S(2)}) copy-start(bf16[2048,64]{0,1:T(8,128)(2,1)} %param.23) | copy-start | bytes 786436
  30.3 1.6 %copy-start.9 = (bf16[2048,64]{0,1:T(8,128)(2,1)S(1)}, bf16[2048,64]{0,1:T(8,128)(2,1)}, u32[]{:S(2)}) copy-start(bf16[2048,64]{0,1:T(8,128)(2,1)} %param.24) | copy-start | bytes 786436
  30.8 2.2 %copy-start.1 = (bf16[2048,128]{1,0:T(8,128)(2,1)S(1)}, bf16[2048,128]{1,0:T(8,128)(2,1)}, u32[]{:S(2)}) copy-start(bf16[2048,128]{1,0:T(8,128)(2,1)} %param.21) | copy-start | bytes 1572868
  33.0 1.1 copy-start.10
  38.9 55.3 %copy-start.2 = (bf16[64,2048]{1,0:T(8,128)(2,1)S(1)}, bf16[64,2048]{1,0:T(8,128)(2,1)}, u32[]{:S(2)}) copy-start(bf16[64,2048]{1,0:T(8,128)(2,1)} %param.28) | copy-start | bytes 786436
  38.9 55.4 %copy-start.3 = (bf16[64,2048]{1,0:T(8,128)(2,1)S(1)}, bf16[64,2048]{1,0:T(8,128)(2,1)}, u32[]{:S(2)}) copy-start(bf16[64,2048]{1,0:T(8,128)(2,1)} %param.29) | copy-start | bytes 786436

commit v3 on v2

--- a/solution.py
+++ b/solution.py
@@ -41,17 +41,225 @@
     return sp, sp // 16, (sp // 4) % 4, sp % 4
 
 
-def greet(peers):
+def greet(peers, lane_peers=(), meanwhile=lambda: None):
     barrier = pltpu.get_barrier_semaphore()
     for peer in peers:
         pl.semaphore_signal(barrier, inc=1, device_id={"sp": peer}, device_id_type=MESH)
-    pl.semaphore_wait(barrier, len(peers))
+    for peer in lane_peers:
+        pl.semaphore_signal(barrier, inc=1, device_id={"tp": peer}, device_id_type=MESH)
+    meanwhile()
+    pl.semaphore_wait(barrier, len(peers) + len(lane_peers))
+
+
+def lanes():
+    tp = lax.axis_index("tp")
+    x, core = tp // 2, tp % 2
+    return tp, tp + 1 - 2 * core, (tp + 2) % 8, (tp + 6) % 8, (tp + 4) % 8, 1 - 2 * core
+
+
+def ring_gather(chunk_ref, slots_ref, send, recv, meanwhile, use):
+    tp, partner, right, left, across, twist = lanes()
+    half = chunk_ref.shape[0] // 2
+    top, low = slice(0, half), slice(half, 2 * half)
+
+    def copy(n, src, dst, target):
+        return pltpu.make_async_remote_copy(
+            src_ref=src, dst_ref=dst, send_sem=send.at[n], recv_sem=recv.at[n],
+            device_id={"tp": target}, device_id_type=MESH,
+        )
+
+    def relay(n, source, part, target):
+        return copy(n, slots_ref.at[source, part], slots_ref.at[source, part], target)
+
+    barrier = pltpu.get_barrier_semaphore()
+    for peer in (partner, right, left):
+        pl.semaphore_signal(barrier, inc=1, device_id={"tp": peer}, device_id_type=MESH)
+    pl.semaphore_wait(barrier, 3)
+    copies = [
+        copy(0, chunk_ref, slots_ref.at[tp], partner),
+        copy(1, chunk_ref.at[top], slots_ref.at[tp, top], right),
+        copy(2, chunk_ref.at[low], slots_ref.at[tp, low], left),
+        copy(3, chunk_ref.at[low], slots_ref.at[tp, low], right),
+        copy(4, chunk_ref.at[top], slots_ref.at[tp, top], left),
+        relay(5, left, top, right),
+        relay(6, right, low, left),
+        relay(7, left, top, partner),
+        relay(8, right, low, partner),
+        relay(9, left, low, partner),
+        relay(10, right, top, partner),
+        relay(11, across, top, partner),
+        relay(12, across, low, partner),
+    ]
+    for n in range(5):
+        copies[n].start()
+    meanwhile()
+    use(tp, chunk_ref)
+    copies[1].wait_recv()
+    copies[5].start()
+    copies[7].start()
+    copies[2].wait_recv()
+    copies[6].start()
+    copies[8].start()
+    copies[0].wait_recv()
+    use(partner, slots_ref.at[partner])
+    copies[3].wait_recv()
+    copies[9].start()
+    copies[4].wait_recv()
+    copies[10].start()
+    use(left, slots_ref.at[left])
+    use(right, slots_ref.at[right])
+    copies[7].wait_recv()
+    copies[9].wait_recv()
+    use(left + twist, slots_ref.at[left + twist])
+    copies[8].wait_recv()
+    copies[10].wait_recv()
+    use(right + twist, slots_ref.at[right + twist])
+    copies[5].wait_recv()
+    copies[11].start()
+    copies[6].wait_recv()
+    copies[12].start()
+    use(across, slots_ref.at[across])
+    copies[11].wait_recv()
+    copies[12].wait_recv()
+    use(across + twist, slots_ref.at[across + twist])
+    for one in copies:
+        one.wait_send()
+
+
+def project_kernel(
+    token_ref, gain_ref, query_w, key_w, value_w, rec_w, forget_w, input_w, gate_w,
+    kv_ref, query_ref, rec_ref, forget_ref, input_ref, gate_ref,
+    slots_ref, raw_ref, weight_ref, acc_ref, square_ref, send, recv, load,
+):
+    narrow = (key_w, value_w, input_w, gate_w, query_w)
+    loads = [pltpu.make_async_copy(w, raw_ref.at[n], load.at[n]) for n, w in enumerate(narrow)]
+    loads += [
+        pltpu.make_async_copy(rec_w, weight_ref.at[:, 128:256], load.at[5]),
+        pltpu.make_async_copy(forget_w, weight_ref.at[:, 256:384], load.at[6]),
+    ]
+    for one in loads:
+        one.start()
+    acc_ref[...] = jnp.zeros_like(acc_ref)
+    square_ref[...] = jnp.zeros_like(square_ref)
+
+    def meanwhile():
+        for one in loads:
+            one.wait()
+
+        def assemble(n, _):
+            at = pl.ds(pl.multiple_of(n * 256, 256), 256)
+            weight_ref[at, 0:128] = jnp.concatenate([raw_ref[0, at, :], raw_ref[1, at, :]], axis=1)
+            weight_ref[at, 384:512] = jnp.concatenate([raw_ref[2, at, :], raw_ref[3, at, :]], axis=1)
+            weight_ref[at, 512:576] = raw_ref[4, at, :]
+            return 0
+
+        lax.fori_loop(0, 8, assemble, 0)
+
+    def use(source, ref):
+        values = ref[...].astype(F32)
+        squares = values * values
+        square_ref[...] += squares[:, 0:128] + squares[:, 128:256]
+        scaled = (values * gain_ref[pl.ds(source, 1), :]).astype(BF16)
+        at = pl.ds(pl.multiple_of(source * 256, 256), 256)
+        acc_ref[...] += dot(scaled, weight_ref[at, :])
+
+    ring_gather(token_ref, slots_ref, send, recv, meanwhile, use)
+    inverse = lax.rsqrt(jnp.sum(square_ref[...], axis=1, keepdims=True) / D + epsilon)
+    kv_ref[...] = (acc_ref[:, 0:128] * inverse).astype(BF16)
+    rec_ref[...] = (acc_ref[:, 128:256] * inverse).astype(BF16)
+    forget_ref[...] = (acc_ref[:, 256:384] * inverse).astype(BF16)
+    input_ref[...] = (acc_ref[:, 384:448] * inverse).astype(BF16)
+    gate_ref[...] = (acc_ref[:, 448:512] * inverse).astype(BF16)
+    query = (acc_ref[:, 512:576] * inverse).astype(BF16)
+    query_ref[...] = jnp.concatenate([query[0:128], query[128:256]], axis=1)
+
+
+def project(tokens, gain, *weights):
+    dma = pltpu.SemaphoreType.DMA
+    wide, narrow = jax.ShapeDtypeStruct((TOK, 128), BF16), jax.ShapeDtypeStruct((TOK, 64), BF16)
+    return pl.pallas_call(
+        project_kernel,
+        out_shape=(wide, jax.ShapeDtypeStruct((128, 128), BF16), wide, wide, narrow, narrow),
+        in_specs=[VMEM, VMEM] + [ANY] * 7,
+        out_specs=(VMEM,) * 6,
+        scratch_shapes=[
+            pltpu.VMEM((8, TOK, 256), BF16),
+            pltpu.VMEM((5, D, 64), BF16),
+            pltpu.VMEM((D, 576), BF16),
+            pltpu.VMEM((TOK, 576), F32),
+            pltpu.VMEM((TOK, 128), F32),
+            dma((13,)), dma((13,)), dma((7,)),
+        ],
+        compiler_params=pltpu.CompilerParams(collective_id=2, has_side_effects=True),
+        name="project",
+    )(tokens, gain, *weights)
+
+
+def output_kernel(heads_ref, weight_ref, out_ref, slots_ref, acc_ref, send, recv):
+    acc_ref[...] = jnp.zeros_like(acc_ref)
+
+    def use(source, ref):
+        acc_ref[...] += dot(ref[...], weight_ref[source])
+
+    ring_gather(heads_ref, slots_ref, send, recv, lambda: None, use)
+    out_ref[...] = acc_ref[...].astype(BF16)
+
+
+def output(heads, weight):
+    dma = pltpu.SemaphoreType.DMA
+    return pl.pallas_call(
+        output_kernel,
+        out_shape=jax.ShapeDtypeStruct((TOK, 256), BF16),
+        in_specs=[VMEM, VMEM],
+        out_specs=VMEM,
+        scratch_shapes=[
+            pltpu.VMEM((8, TOK, 128), BF16),
+            pltpu.VMEM((TOK, 256), F32),
+            dma((13,)), dma((13,)),
+        ],
+        compiler_params=pltpu.CompilerParams(collective_id=3, has_side_effects=True),
+        name="output",
+    )(heads, weight)
+
+
+def local_scan(query_ref, forget_ref, input_ref, low_ref, spike_ref, out_ref, lift_ref, state_ref):
+    span = REC_SPAN
+    rows = lax.broadcasted_iota(jnp.int32, (span, span), 0)
+    cols = lax.broadcasted_iota(jnp.int32, (span, span), 1)
+    causal = cols <= rows
+    ones = jnp.where(causal, 1.0, 0.0)
+    state = jnp.zeros((REC_VAL, REC_KEY), F32)
+    offset = jnp.zeros((1, REC_KEY), F32)
+    for n in range(query_ref.shape[0] // span):
+        at = slice(n * span, (n + 1) * span)
+        query = query_ref[at, :].astype(F32)
+        lifted = query * jax.nn.sigmoid(query)
+        intake = (1.0 - low_ref[...]) * jax.nn.sigmoid(-forget_ref[at, :].astype(F32))
+        log_forget = jnp.log1p(-intake) + spike_ref[at, :]
+        running = lax.dot_general(
+            ones, log_forget, (((1,), (0,)), ((), ())),
+            precision=lax.Precision.HIGHEST, preferred_element_type=F32,
+        )
+        total = running[span - 1 : span, :]
+        middle = running[span // 2 - 1 : span // 2, :]
+        value = input_ref[at, :]
+        grown = (lifted * jnp.exp(running - middle)).astype(BF16)
+        shrunk = (intake * jnp.exp(middle - running)).astype(BF16)
+        inner = jnp.where(causal, dot(grown, shrunk, tb=True), 0.0)
+        faded = (lifted * jnp.exp(running)).astype(BF16)
+        out_ref[at, :] = dot(inner.astype(BF16), value) + dot(faded, state.astype(BF16), tb=True)
+        lift_ref[at, :] = (lifted * jnp.exp(running + offset)).astype(BF16)
+        kept = (intake * jnp.exp(total - running)).astype(BF16)
+        state = state * jnp.exp(total) + dot(value, kept, ta=True)
+        offset = offset + total
+    state_ref[0:REC_VAL, :] = state
+    state_ref[REC_VAL:STATE_ROWS, :] = jnp.broadcast_to(offset, (8, REC_KEY))
 
 
 def share_kernel(
-    kv_ref, kv_hbm, query_ref, state_ref,
-    early_ref, late_ref, queries_ref, before_ref, group_ref,
-    rows_ref, planes_ref, send, recv, query_send, query_recv, own_sem,
+    kv_ref, kv_hbm, query_ref, rec_ref, forget_ref, input_ref, low_ref, spike_ref, rec_out_w, att_out_w,
+    early_ref, late_ref, queries_ref, before_ref, group_ref, local_ref, faded_ref, columns_ref,
+    state_ref, rows_ref, planes_ref, send, recv, query_send, query_recv, column_send, column_recv, own_sem,
 ):
     sp, c, zl, y = place()
     base = c * 16
@@ -62,8 +270,33 @@
     own_late = pltpu.make_async_copy(kv_hbm.at[EARLY:TOK], late_ref.at[zl, y], own_sem.at[1])
     own_early.start()
     own_late.start()
-    rows_ref[y] = state_ref[...]
-    greet(in_row + in_line + far)
+    tp = lax.axis_index("tp")
+    lane_peers = [(tp + d) % 8 for d in range(1, 8)]
+
+    def columns(w, there):
+        return w.at[:, pl.ds(pl.multiple_of(there * 256, 256), 256)]
+
+    own_columns = [
+        pltpu.make_async_copy(columns(w, tp), columns_ref.at[tp, n * 64 : n * 64 + 64], own_sem.at[2 + n])
+        for n, w in enumerate((rec_out_w, att_out_w))
+    ]
+    column_copies = [
+        pltpu.make_async_remote_copy(
+            src_ref=columns(w, there), dst_ref=columns_ref.at[tp, n * 64 : n * 64 + 64],
+            send_sem=column_send.at[n, d], recv_sem=column_recv.at[n, d],
+            device_id={"tp": there}, device_id_type=MESH,
+        )
+        for n, w in enumerate((rec_out_w, att_out_w))
+        for d, there in enumerate(lane_peers)
+    ]
+
+    def scan():
+        local_scan(
+            rec_ref, forget_ref, input_ref, low_ref, spike_ref, local_ref, faded_ref, state_ref
+        )
+        rows_ref[y] = state_ref[...]
+
+    greet(in_row + in_line + far, lane_peers, scan)
 
     def step(n, src, dst, peers):
         return [to(src, dst, send.at[n, d], recv.at[n, d], peers[d]) for d in range(3)]
@@ -83,6 +316,8 @@
                 query_ref, queries_ref.at[c - 1], query_send.at[d - 1], query_recv.at[c - 1], sp - 16 * d
             ).start()
 
+    for copy in own_columns + column_copies:
+        copy.start()
     own_early.wait()
     own_late.wait()
     for copy in first:
@@ -133,7 +368,11 @@
                 query_ref, queries_ref.at[n - 1], query_send.at[0], query_recv.at[n - 1], sp
             ).wait_recv()
 
-    for copy in first + second + third:
+    for copy in own_columns:
+        copy.wait()
+    for copy in column_copies:
+        copy.wait_recv()
+    for copy in first + second + third + column_copies:
         copy.wait_send()
     for d in (1, 2, 3):
 
@@ -144,7 +383,7 @@
             ).wait_send()
 
 
-def share(kv, query, state):
+def share(kv, query, *operands):
     dma = pltpu.SemaphoreType.DMA
     return pl.pallas_call(
         share_kernel,
@@ -154,17 +393,21 @@
             jax.ShapeDtypeStruct((3, 128, 128), BF16),
             jax.ShapeDtypeStruct((STATE_ROWS, REC_KEY), F32),
             jax.ShapeDtypeStruct((STATE_ROWS, REC_KEY), F32),
+            jax.ShapeDtypeStruct((TOK, REC_VAL), F32),
+            jax.ShapeDtypeStruct((TOK, REC_KEY), BF16),
+            jax.ShapeDtypeStruct((8, 128, 256), BF16),
         ),
-        in_specs=[VMEM, ANY, VMEM, VMEM],
-        out_specs=(VMEM,) * 5,
+        in_specs=[VMEM, ANY] + [VMEM] * 6 + [ANY] * 2,
+        out_specs=(VMEM,) * 8,
         scratch_shapes=[
+            pltpu.VMEM((STATE_ROWS, REC_KEY), F32),
             pltpu.VMEM((4, STATE_ROWS, REC_KEY), F32),
             pltpu.VMEM((4, STATE_ROWS, REC_KEY), F32),
-            dma((6, 3)), dma((6, 3)), dma((3,)), dma((3,)), dma((2,)),
+            dma((6, 3)), dma((6, 3)), dma((3,)), dma((3,)), dma((2, 7)), dma((2, 7)), dma((4,)),
         ],
         compiler_params=pltpu.CompilerParams(collective_id=0, has_side_effects=True),
         name="share",
-    )(kv, kv, query, state)
+    )(kv, kv, query, *operands)
 
 
 def stick_tile(q, kv, tri, bias2, keep=None):
@@ -355,71 +598,6 @@
     )(*operands)
 
 
-def scan_kernel(query_ref, forget_ref, input_ref, low_ref, spike_ref, out_ref, lift_ref, state_ref):
-    span = REC_SPAN
-    rows = lax.broadcasted_iota(jnp.int32, (span, span), 0)
-    cols = lax.broadcasted_iota(jnp.int32, (span, span), 1)
-    causal = cols <= rows
-    ones = jnp.where(causal, 1.0, 0.0)
-    state = jnp.zeros((REC_VAL, REC_KEY), F32)
-    offset = jnp.zeros((1, REC_KEY), F32)
-    for n in range(query_ref.shape[0] // span):
-        at = slice(n * span, (n + 1) * span)
-        query = query_ref[at, :].astype(F32)
-        lifted = query * jax.nn.sigmoid(query)
-        intake = (1.0 - low_ref[...]) * jax.nn.sigmoid(-forget_ref[at, :].astype(F32))
-        log_forget = jnp.log1p(-intake) + spike_ref[at, :]
-        running = lax.dot_general(
-            ones, log_forget, (((1,), (0,)), ((), ())),
-            precision=lax.Precision.HIGHEST, preferred_element_type=F32,
-        )
-        total = running[span - 1 : span, :]
-        middle = running[span // 2 - 1 : span // 2, :]
-        value = input_ref[at, :]
-        grown = (lifted * jnp.exp(running - middle)).astype(BF16)
-        shrunk = (intake * jnp.exp(middle - running)).astype(BF16)
-        inner = jnp.where(causal, dot(grown, shrunk, tb=True), 0.0)
-        faded = (lifted * jnp.exp(running)).astype(BF16)
-        out_ref[at, :] = dot(inner.astype(BF16), value) + dot(faded, state.astype(BF16), tb=True)
-        lift_ref[at, :] = (lifted * jnp.exp(running + offset)).astype(BF16)
-        kept = (intake * jnp.exp(total - running)).astype(BF16)
-        state = state * jnp.exp(total) + dot(value, kept, ta=True)
-        offset = offset + total
-    state_ref[0:REC_VAL, :] = state
-    state_ref[REC_VAL:STATE_ROWS, :] = jnp.broadcast_to(offset, (8, REC_KEY))
-
-
-def local_scan(query, forget, inputs, low, spikes):
-    n = query.shape[0]
-    return pl.pallas_call(
-        scan_kernel,
-        out_shape=(
-            jax.ShapeDtypeStruct((n, REC_VAL), F32),
-            jax.ShapeDtypeStruct((n, REC_KEY), BF16),
-            jax.ShapeDtypeStruct((STATE_ROWS, REC_KEY), F32),
-        ),
-        in_specs=[VMEM] * 5,
-        out_specs=(VMEM,) * 3,
-        name="local_scan",
-    )(query, forget, inputs, low, spikes)
-
-
-def gathered_copies(array, axis, dim):
-    copies = jnp.broadcast_to(array, (lax.axis_size(axis), *array.shape))
-    pieces = lax.all_to_all(copies, axis, split_axis=0, concat_axis=0, tiled=True)
-    lengths = list(array.shape)
-    lengths[dim] *= pieces.shape[0]
-    return jnp.moveaxis(pieces, 0, dim).reshape(lengths)
-
-
-def summed_on_arrival(array, axis, dim):
-    size, lengths = lax.axis_size(axis), array.shape
-    pieces = array.reshape(*lengths[:dim], size, lengths[dim] // size, *lengths[dim + 1 :])
-    pieces = jnp.moveaxis(pieces, dim, 0)
-    arrived = lax.all_to_all(pieces, axis, split_axis=0, concat_axis=0, tiled=True)
-    return arrived.astype(F32).sum(axis=0)
-
-
 def shards(
     tokens,
     input_norm_gain,
@@ -437,9 +615,9 @@
     attention_output_weight,
     recurrence_output_weight,
 ):
-    values = gathered_copies(tokens, "tp", 1).astype(F32)
-    scaled = (values * input_norm_gain[None, :]).astype(BF16)
-    weights = (
+    kv, query, rec, forget, inputs, gate = project(
+        tokens,
+        input_norm_gain.reshape(8, 256),
         attention_query_weight,
         attention_key_weight,
         attention_value_weight,
@@ -448,24 +626,15 @@
         input_weight,
         output_gate_weight,
     )
-    inverse = lax.rsqrt(jnp.sum(values * values, axis=1) / D + epsilon)[:, None]
-    query_stick, key_stick, value_stick, query_rows, forget_rows, input_rows, gate_rows = (
-        (jnp.dot(scaled, weight, preferred_element_type=F32) * inverse).astype(BF16)
-        for weight in weights
-    )
-    kv = jnp.concatenate([key_stick, value_stick], axis=1)
-    query = jnp.concatenate([query_stick[0:128], query_stick[128:256]], axis=1)
-    local_out, faded, state = local_scan(
-        query_rows, forget_rows, input_rows, forget_minimum, decay_spikes
-    )
-    early, late, queries, before, group = share(kv, query, state)
+    early, late, queries, before, group, local_out, faded, columns = share(
+        kv, query, rec, forget, inputs, forget_minimum, decay_spikes,
+        recurrence_output_weight, attention_output_weight,
+    )
     own, own_left, far, far_left = stick(attention_score_bias, query, queries, early, late)
     heads = finish(
-        own, own_left, far, far_left, before, group, local_out, faded, gate_rows, head_norm_gain[None, :]
-    )
-    output_weight = jnp.concatenate([recurrence_output_weight, attention_output_weight], axis=0)
-    partial_out = jnp.dot(heads, output_weight, preferred_element_type=F32)
-    return summed_on_arrival(partial_out.astype(BF16), "tp", 1).astype(BF16)
+        own, own_left, far, far_left, before, group, local_out, faded, gate, head_norm_gain[None, :]
+    )
+    return output(heads, columns)
 
 
 def solution(mesh):

time: 126 us -> 110 us (0.87)
  Pallas kernels: 58.2 us -> 99.6 us
  blocking collectives: 29.5 us -> 0 us
  waiting for transfers between devices: 13.5 us -> 0 us
  starting transfers between devices: 10.4 us -> 0 us
  matrix products: 7.15 us -> 0 us
  local copies, waits for them, and re-layouts: 3.47 us -> 9.72 us
  other arithmetic: 2.86 us -> 0 us
    all_to_all x1 -> x0, blocking collectives: 29.5 us -> none  [summed_on_arrival(): lax.all_to_all(pieces, axis, split_axis=0, concat_axis=0, tiled=True)]
    pallas_call x1 -> x2, Pallas kernels: 2.85 us -> 30.4 us  [the longest x1 18.1 us: project(): pl.pallas_call(project_kernel, out_shape=(wide, jax.ShapeDtypeStruct((128...]
    all_to_all x1 -> x0, waiting for transfers between devices: 13.5 us -> none  [gathered_copies(): lax.all_to_all(copies, axis, split_axis=0, concat_axis=0, tiled=True)]
    all_to_all x1 -> x0, starting transfers between devices: 10.4 us -> none  [gathered_copies(): lax.all_to_all(copies, axis, split_axis=0, concat_axis=0, tiled=True)]
    pallas_call x1, Pallas kernels: 11 us -> 20.2 us  [finish(): pl.pallas_call(finish_kernel, out_shape=jax.ShapeDtypeStruct((TOK, 128),...]
    dot_general x8 -> x0, matrix products: 7.15 us -> none  [the longest x7 5.89 us: shards(): jnp.dot(scaled, weight, preferred_element_type=F32) * inverse]
    unnamed x24 -> x19, local copies, waits for them, and re-layouts: 2.36 us -> 9.12 us
    pallas_call x1, Pallas kernels: 27.6 us -> 32.3 us  [share(): pl.pallas_call(share_kernel, out_shape=(jax.ShapeDtypeStruct((4, 4, EARLY...]
  transfers between devices with their start and end apart: 1 -> 0, of which waited for: 1 -> 0; matrix products, arithmetic and copies ran while one was open for 1% -> 0% of each run, Pallas kernels for 0% -> 0%
where the time goes in v3:
time: 110 us
  Pallas kernels  99.6 us (91%)
  local copies, waits for them, and re-layouts  9.72 us (9%)
    pallas_call x1, Pallas kernels, share(): pl.pallas_call(share_kernel, out_shape=(jax.ShapeDtypeStruct((4, 4, EARLY...  32.3 us
    pallas_call x1, Pallas kernels, finish(): pl.pallas_call(finish_kernel, out_shape=jax.ShapeDtypeStruct((TOK, 128),...  20.2 us
    pallas_call x1, Pallas kernels, project(): pl.pallas_call(project_kernel, out_shape=(wide, jax.ShapeDtypeStruct((128...  18.1 us
    pallas_call x1, Pallas kernels, stick(): pl.pallas_call(stick_kernel, out_shape=(jax.ShapeDtypeStruct((TOK, 128),...  16.7 us
    pallas_call x1, Pallas kernels, output(): pl.pallas_call(output_kernel, out_shape=jax.ShapeDtypeStruct((TOK, 256),...  12.3 us
    unnamed x19, local copies, waits for them, and re-layouts  9.12 us

profile of v3, /device:TPU:1, one launch (start us, length us, event | category | flops | bytes accessed | tf_op | source)
XLA Modules:
  0.0 110.0 jit_solution(6437410450575908397)
XLA Ops:
  0.0 0.0 copy-start
  0.0 2.0 %copy.16.query_w = bf16[2048,64]{1,0:T(8,128)(2,1)} copy(bf16[2048,64]{0,1:T(8,128)(2,1)} %param.17) | data formatting | bytes 524288 | tf_op args[2]
  2.0 0.0 copy-done
  2.0 0.0 copy-start.1
  2.0 1.0 copy.17.key_w
  3.0 0.0 copy-done.1
  3.0 0.0 copy-start.2
  3.0 1.0 copy.18.value_w
  4.0 0.0 copy-done.2
  4.0 0.0 copy-start.3
  4.1 1.0 copy.19.input_w
  5.1 0.0 copy-done.3
  5.1 0.0 copy-start.4
  5.1 1.0 copy.20.gate_w
  6.1 0.0 copy-done.4
  6.1 0.6 reshape.3.gain_ref
  6.7 18.1 %project.1 = (bf16[256,128]{1,0:T(8,128)(2,1)}, bf16[128,128]{1,0:T(8,128)(2,1)}, bf16[256,128]{1,0:T(8,128)(2,1)}, bf16[256,128]{1,0:T(8,128)(2,1)}, bf16[256,64]{1,0:T(8,128)(2,1)}, /*index=5*/bf16[256,64]{1,0:T(8,128)(2,1)}) custom-call(bf16[256,256]{1,0:T(8,128)(2,1)} %token_ref.1, f32[8,256]{1,0:T(8,128)} %reshape.3.gain_ref, ...), custom_call_target="tpu_custom_call" | custom-call | tf_op jit(solution)/shard_map/project/pallas_call | solution.py:180
  24.8 0.0 copy-start.5
  24.9 0.7 copy-done.5
  25.5 0.8 copy.21.spike_ref
  26.3 32.3 %share.1 = (bf16[4,4,192,128]{3,2,1,0:T(8,128)(2,1)}, bf16[4,4,64,128]{3,2,1,0:T(8,128)(2,1)}, bf16[3,128,128]{2,1,0:T(8,128)(2,1)}, f32[72,128]{1,0:T(8,128)}, ...) custom-call(bf16[256,128]{1,0:T(8,128)(2,1)} %get-tuple-element.24.kv_ref.kv_hbm, ...), custom_call_target="tpu_custom_call" | custom-call | tf_op jit(solution)/shard_map/share/pallas_call | solution.py:388
  59.3 16.7 %stick.1 = (f32[256,128]{1,0:T(8,128)}, f32[256,128]{1,0:T(8,128)}, bf16[3,128,128]{2,1,0:T(8,128)(2,1)}, f32[3,8,256]{2,1,0:T(8,128)}) custom-call(f32[1]{0:T(128)S(6)} %copy.23.bias_ref, bf16[128,128]{1,0:T(8,128)(2,1)} %get-tuple-element.23.query_ref, bf16[3,128,128]{2,1,0:T(8,128)(2,1)} %get-tuple-element.28.queries_ref, ...), custom_call_target="tpu_custom_call" | custom-call | tf_op jit(solution)/shard_map/stick/pallas_call | solution.py:485
  76.0 20.2 %finish.1.heads_ref = bf16[256,128]{1,0:T(8,128)(2,1)} custom-call(f32[256,128]{1,0:T(8,128)} %get-tuple-element.31.own_ref, f32[256,128]{1,0:T(8,128)} %get-tuple-element.32.own_left_ref, bf16[3,128,128]{2,1,0:T(8,128)(2,1)} %get-tuple-element.33.far_ref, f32[3,8,256]{2,1,0:T(8,128)} %get-tuple-element.34.far_left_ref, ...), custom_call_target="tpu_custom_call" | custom-call | tf_op jit(solution)/shard_map/finish/pallas_call | solution.py:582
  96.2 12.3 %output.1 = bf16[256,256]{1,0:T(8,128)(2,1)} custom-call(bf16[256,128]{1,0:T(8,128)(2,1)} %finish.1.heads_ref, bf16[8,128,256]{2,1,0:T(8,128)(2,1)} %get-tuple-element.40.weight_ref), custom_call_target="tpu_custom_call" | custom-call | tf_op jit(solution)/shard_map/output/pallas_call | solution.py:210
  108.4 1.6 %copy.24 = bf16[256,256]{1,0:T(8,128)(2,1)} copy(bf16[256,256]{1,0:T(8,128)(2,1)} %output.1) | data formatting | bytes 262144
Async XLA Ops:
  0.0 2.0 %copy-start = (bf16[2048,64]{0,1:T(8,128)(2,1)S(1)}, bf16[2048,64]{0,1:T(8,128)(2,1)}, u32[]{:S(2)}) copy-start(bf16[2048,64]{0,1:T(8,128)(2,1)} %param.18) | copy-start | bytes 786436
  2.0 1.0 copy-start.1
  3.0 1.0 copy-start.2
  4.0 1.0 copy-start.3
  5.1 1.0 copy-start.4
  24.8 0.7 copy-start.5

commit v4 on v3

v4 whole, which is shorter than its diff:
```python
import functools

import jax
import jax.numpy as jnp
from jax import lax
from jax.experimental import pallas as pl
from jax.experimental.pallas import tpu as pltpu
from jax.sharding import PartitionSpec as P

D = 2048
HEAD = 64
REC_KEY = 128
REC_VAL = 64
REC_SPAN = 64
TOK = 256
LOG2E = 1.4426950408889634
STATE_ROWS = REC_VAL + 8
epsilon = 1e-06
F32, BF16 = jnp.float32, jnp.bfloat16
VMEM = pl.BlockSpec(memory_space=pltpu.VMEM)
SMEM = pl.BlockSpec(memory_space=pltpu.SMEM)
ANY = pl.BlockSpec(memory_space=pl.ANY)
MESH = pl.DeviceIdType.MESH


def dot(a, b, ta=False, tb=False):
    dims = (((0 if ta else 1,), (1 if tb else 0,)), ((), ()))
    return lax.dot_general(a, b, dims, preferred_element_type=F32)


def to(src, dst, send, recv, sp):
    return pltpu.make_async_remote_copy(
        src_ref=src, dst_ref=dst, send_sem=send, recv_sem=recv,
        device_id={"sp": sp}, device_id_type=MESH,
    )


def place():
    sp = lax.axis_index("sp")
    return sp, sp // 16, (sp // 4) % 4, sp % 4


def greet(peers, lane_peers=(), meanwhile=lambda: None):
    barrier = pltpu.get_barrier_semaphore()
    for peer in peers:
        pl.semaphore_signal(barrier, inc=1, device_id={"sp": peer}, device_id_type=MESH)
    for peer in lane_peers:
        pl.semaphore_signal(barrier, inc=1, device_id={"tp": peer}, device_id_type=MESH)
    meanwhile()
    pl.semaphore_wait(barrier, len(peers) + len(lane_peers))


def lanes():
    tp = lax.axis_index("tp")
    x, core = tp // 2, tp % 2
    return tp, tp + 1 - 2 * core, (tp + 2) % 8, (tp + 6) % 8, (tp + 4) % 8, 1 - 2 * core


def ring_gather(chunk_ref, slots_ref, send, recv, meanwhile, use):
    tp, partner, right, left, across, twist = lanes()
    half = chunk_ref.shape[0] // 2
    top, low = slice(0, half), slice(half, 2 * half)

    def copy(n, src, dst, target):
        return pltpu.make_async_remote_copy(
            src_ref=src, dst_ref=dst, send_sem=send.at[n], recv_sem=recv.at[n],
            device_id={"tp": target}, device_id_type=MESH,
        )

    def relay(n, source, part, target):
        return copy(n, slots_ref.at[source, part], slots_ref.at[source, part], target)

    barrier = pltpu.get_barrier_semaphore()
    for peer in (partner, right, left):
        pl.semaphore_signal(barrier, inc=1, device_id={"tp": peer}, device_id_type=MESH)
    pl.semaphore_wait(barrier, 3)
    copies = [
        copy(0, chunk_ref, slots_ref.at[tp], partner),
        copy(1, chunk_ref.at[top], slots_ref.at[tp, top], right),
        copy(2, chunk_ref.at[low], slots_ref.at[tp, low], left),
        copy(3, chunk_ref.at[low], slots_ref.at[tp, low], right),
        copy(4, chunk_ref.at[top], slots_ref.at[tp, top], left),
        relay(5, left, top, right),
        relay(6, right, low, left),
        relay(7, left, top, partner),
        relay(8, right, low, partner),
        relay(9, left, low, partner),
        relay(10, right, top, partner),
        relay(11, across, top, partner),
        relay(12, across, low, partner),
    ]
    for n in range(5):
        copies[n].start()
    meanwhile()
    use(tp, chunk_ref)
    copies[1].wait_recv()
    copies[5].start()
    copies[7].start()
    copies[2].wait_recv()
    copies[6].start()
    copies[8].start()
    copies[0].wait_recv()
    use(partner, slots_ref.at[partner])
    copies[3].wait_recv()
    copies[9].start()
    copies[4].wait_recv()
    copies[10].start()
    use(left, slots_ref.at[left])
    use(right, slots_ref.at[right])
    copies[7].wait_recv()
    copies[9].wait_recv()
    use(left + twist, slots_ref.at[left + twist])
    copies[8].wait_recv()
    copies[10].wait_recv()
    use(right + twist, slots_ref.at[right + twist])
    copies[5].wait_recv()
    copies[11].start()
    copies[6].wait_recv()
    copies[12].start()
    use(across, slots_ref.at[across])
    copies[11].wait_recv()
    copies[12].wait_recv()
    use(across + twist, slots_ref.at[across + twist])
    for one in copies:
        one.wait_send()


def project_kernel(
    token_ref, gain_ref, key_w, value_w, input_w, gate_w, query_w, rec_w, forget_w,
    kv_ref, query_ref, rec_ref, forget_ref, input_ref, gate_ref,
    slots_ref, narrow_ref, wide_ref, first_ref, second_ref, square_ref, send, recv, load,
):
    narrow = (key_w, value_w, input_w, gate_w, query_w)
    loads = [
        pltpu.make_async_copy(w, narrow_ref.at[n * 64 : n * 64 + 64], load.at[n])
        for n, w in enumerate(narrow)
    ]
    loads += [
        pltpu.make_async_copy(w, wide_ref.at[:, n * 128 : n * 128 + 128], load.at[5 + n])
        for n, w in enumerate((rec_w, forget_w))
    ]
    for one in loads:
        one.start()
    first_ref[...] = jnp.zeros_like(first_ref)
    second_ref[...] = jnp.zeros_like(second_ref)
    square_ref[...] = jnp.zeros_like(square_ref)

    def meanwhile():
        for one in loads:
            one.wait()

    def use(source, ref):
        at = pl.ds(pl.multiple_of(source * 256, 256), 256)
        values = ref[...].astype(F32)
        squares = values * values
        square_ref[...] += squares[:, 0:128] + squares[:, 128:256]
        scaled = (values * gain_ref[:, at]).astype(BF16)
        first_ref[...] += dot(scaled, narrow_ref[:, at], tb=True)
        second_ref[...] += dot(scaled, wide_ref[at, :])

    ring_gather(token_ref, slots_ref, send, recv, meanwhile, use)
    inverse = lax.rsqrt(jnp.sum(square_ref[...], axis=1, keepdims=True) / D + epsilon)
    kv_ref[...] = (first_ref[:, 0:128] * inverse).astype(BF16)
    input_ref[...] = (first_ref[:, 128:192] * inverse).astype(BF16)
    gate_ref[...] = (first_ref[:, 192:256] * inverse).astype(BF16)
    query = (first_ref[:, 256:320] * inverse).astype(BF16)
    query_ref[...] = jnp.concatenate([query[0:128], query[128:256]], axis=1)
    rec_ref[...] = (second_ref[:, 0:128] * inverse).astype(BF16)
    forget_ref[...] = (second_ref[:, 128:256] * inverse).astype(BF16)


def project(tokens, gain, *weights):
    dma = pltpu.SemaphoreType.DMA
    wide, narrow = jax.ShapeDtypeStruct((TOK, 128), BF16), jax.ShapeDtypeStruct((TOK, 64), BF16)
    return pl.pallas_call(
        project_kernel,
        out_shape=(wide, jax.ShapeDtypeStruct((128, 128), BF16), wide, wide, narrow, narrow),
        in_specs=[VMEM, VMEM] + [ANY] * 7,
        out_specs=(VMEM,) * 6,
        scratch_shapes=[
            pltpu.VMEM((8, TOK, 256), BF16),
            pltpu.VMEM((320, D), BF16),
            pltpu.VMEM((D, 256), BF16),
            pltpu.VMEM((TOK, 320), F32),
            pltpu.VMEM((TOK, 256), F32),
            pltpu.VMEM((TOK, 128), F32),
            dma((13,)), dma((13,)), dma((7,)),
        ],
        compiler_params=pltpu.CompilerParams(collective_id=2, has_side_effects=True),
        name="project",
    )(tokens, gain, *weights)


def output_kernel(heads_ref, weight_ref, out_ref, slots_ref, acc_ref, send, recv):
    acc_ref[...] = jnp.zeros_like(acc_ref)

    def use(source, ref):
        acc_ref[...] += dot(ref[...], weight_ref[source])

    ring_gather(heads_ref, slots_ref, send, recv, lambda: None, use)
    out_ref[...] = acc_ref[...].astype(BF16)


def output(heads, weight):
    dma = pltpu.SemaphoreType.DMA
    return pl.pallas_call(
        output_kernel,
        out_shape=jax.ShapeDtypeStruct((TOK, 256), BF16),
        in_specs=[VMEM, VMEM],
        out_specs=VMEM,
        scratch_shapes=[
            pltpu.VMEM((8, TOK, 128), BF16),
            pltpu.VMEM((TOK, 256), F32),
            dma((13,)), dma((13,)),
        ],
        compiler_params=pltpu.CompilerParams(collective_id=3, has_side_effects=True),
        name="output",
    )(heads, weight)


def column(row):
    return jnp.transpose(jnp.broadcast_to(row, (128, 128)))


def local_scan(query_ref, forget_ref, input_ref, low_ref, spike_ref, out_ref, lift_ref, state_ref):
    span = REC_SPAN
    rows = lax.broadcasted_iota(jnp.int32, (span, span), 0)
    cols = lax.broadcasted_iota(jnp.int32, (span, span), 1)
    causal = cols <= rows
    ones = jnp.where(causal, 1.0, 0.0)
    spikes = jnp.concatenate([column(spike_ref[:, n : n + 128]) for n in (0, 128)], axis=0)
    state = jnp.zeros((REC_VAL, REC_KEY), F32)
    offset = jnp.zeros((1, REC_KEY), F32)
    for n in range(query_ref.shape[0] // span):
        at = slice(n * span, (n + 1) * span)
        query = query_ref[at, :].astype(F32)
        lifted = query * jax.nn.sigmoid(query)
        intake = (1.0 - low_ref[...]) * jax.nn.sigmoid(-forget_ref[at, :].astype(F32))
        log_forget = jnp.log1p(-intake) + spikes[at, :]
        running = lax.dot_general(
            ones, log_forget, (((1,), (0,)), ((), ())),
            precision=lax.Precision.HIGHEST, preferred_element_type=F32,
        )
        total = running[span - 1 : span, :]
        middle = running[span // 2 - 1 : span // 2, :]
        value = input_ref[at, :]
        grown = (lifted * jnp.exp(running - middle)).astype(BF16)
        shrunk = (intake * jnp.exp(middle - running)).astype(BF16)
        inner = jnp.where(causal, dot(grown, shrunk, tb=True), 0.0)
        faded = (lifted * jnp.exp(running)).astype(BF16)
        out_ref[at, :] = dot(inner.astype(BF16), value) + dot(faded, state.astype(BF16), tb=True)
        lift_ref[at, :] = (lifted * jnp.exp(running + offset)).astype(BF16)
        kept = (intake * jnp.exp(total - running)).astype(BF16)
        state = state * jnp.exp(total) + dot(value, kept, ta=True)
        offset = offset + total
    state_ref[0:REC_VAL, :] = state
    state_ref[REC_VAL:STATE_ROWS, :] = jnp.broadcast_to(offset, (8, REC_KEY))


def stick_tile(q, kv, tri, bias2, keep=None):
    z = dot(q, kv, tb=True) * (LOG2E / 8.0) + bias2
    soft = jnp.maximum(z, jnp.log(1.0 + jnp.exp2(jnp.minimum(z, 30.0))) * LOG2E)
    if keep is not None:
        soft = jnp.where(keep, soft, 0.0)
    later = dot(soft.astype(BF16), tri)
    return z, soft, later


def attend(here, bias2, q_ref, kvs_ref, tri_ref, acc_ref, left_ref):
    rows = lax.broadcasted_iota(jnp.int32, (TOK, TOK), 0)
    cols = lax.broadcasted_iota(jnp.int32, (TOK, TOK), 1)
    tri_ref[...] = jnp.where(rows > cols, -1.0, 0.0).astype(BF16)
    acc_ref[...] = jnp.zeros_like(acc_ref)
    left_ref[...] = jnp.zeros_like(left_ref)

    def pair(i, _):
        tri = tri_ref[...]
        q_own, q_far = q_ref[0:TOK, :], q_ref[TOK:, :]
        kvs, own, far = [], [], []
        for u in range(2):
            m = 15 - 2 * i - u
            kv = kvs_ref[m // 4, m % 4]
            keep = cols - rows < (here - m) * TOK
            kvs.append(kv)
            own.append(stick_tile(q_own, kv, tri, bias2, keep) + (keep,))
            far.append(stick_tile(q_far, kv, tri, bias2))
        left_own, left_far = left_ref[0:TOK, 0:1], left_ref[TOK:, 0:1]
        acc_own, acc_far = acc_ref[0:TOK, :], acc_ref[TOK:, :]
        for u in range(2):
            z, soft, later, keep = own[u]
            weight = jnp.where(keep, jnp.exp2((z - soft) + (later + left_own)), 0.0)
            acc_own = acc_own + dot(weight.astype(BF16), kvs[u])
            left_own = left_own + (later[:, 0:1] - soft[:, 0:1])
            z, soft, later = far[u]
            weight = jnp.exp2((z - soft) + (later + left_far))
            acc_far = acc_far + dot(weight.astype(BF16), kvs[u])
            left_far = left_far + (later[:, 0:1] - soft[:, 0:1])
        acc_ref[0:TOK, :] = acc_own
        acc_ref[TOK:, :] = acc_far
        left_ref[0:TOK, :] = jnp.broadcast_to(left_own, (TOK, 128))
        left_ref[TOK:, :] = jnp.broadcast_to(left_far, (3 * TOK, 128))
        return 0

    lax.fori_loop(0, 8, pair, 0)


def chain(states_ref, here):
    state = states_ref[0, 0:REC_VAL, :]
    total = states_ref[0, REC_VAL : REC_VAL + 1, :]
    ahead, ahead_total = jnp.zeros_like(state), jnp.zeros_like(total)
    for n in range(1, 4):
        ahead = jnp.where(n <= here, state, ahead)
        ahead_total = jnp.where(n <= here, total, ahead_total)
        more = states_ref[n, REC_VAL : REC_VAL + 1, :]
        state = state * jnp.exp(more) + states_ref[n, 0:REC_VAL, :]
        total = total + more
    return state, total, ahead, ahead_total


def mix_kernel(
    bias_ref, kv_ref, query_ref, rec_ref, forget_ref, input_ref, gate_ref, low_ref, spike_ref, gain_ref,
    rec_out_w, att_out_w,
    heads_ref, columns_ref,
    kvs_ref, queries_ref, state_ref, rows_ref, planes_ref, group_ref, groups_ref,
    local_ref, faded_ref, q_ref, tri_ref, acc_ref, left_ref,
    far_ref, far_left_ref, part_ref, part_left_ref, in_ref,
    line_send, line_recv, row_send, row_recv, half_send, half_recv, state_send, state_recv,
    query_send, query_recv, column_send, column_recv, back_send, back_recv, own_sem,
):
    sp, c, zl, y = place()
    tp = lax.axis_index("tp")
    base = c * 16
    row = [base + zl * 4 + (y + d) % 4 for d in range(4)]
    line = [base + ((zl + d) % 4) * 4 + y for d in range(4)]
    far = [(sp + 16 * d) % 64 for d in range(4)]
    lane_peers = [(tp + d) % 8 for d in range(1, 8)]

    def columns(w, there):
        return w.at[:, pl.ds(pl.multiple_of(there * 256, 256), 256)]

    out_w = ((0, rec_out_w), (1, att_out_w))
    own_columns = [
        pltpu.make_async_copy(columns(w, tp), columns_ref.at[tp, n * 64 : n * 64 + 64], own_sem.at[n])
        for n, w in out_w
    ]
    column_copies = [
        pltpu.make_async_remote_copy(
            src_ref=columns(w, there), dst_ref=columns_ref.at[tp, n * 64 : n * 64 + 64],
            send_sem=column_send.at[n, d], recv_sem=column_recv.at[n, d],
            device_id={"tp": there}, device_id_type=MESH,
        )
        for n, w in out_w
        for d, there in enumerate(lane_peers)
    ]
    for copy in own_columns:
        copy.start()

    def scan():
        local_scan(
            rec_ref, forget_ref, input_ref, low_ref, spike_ref, local_ref, faded_ref, state_ref
        )
        rows_ref[y] = state_ref[...]
        kvs_ref[zl, y] = kv_ref[...]
        for n in (1, 2, 3):

            @pl.when(c >= n)
            def _():
                queries_ref[n - 1] = jnp.zeros((128, 128), BF16)

    greet(row[1:] + line[1:] + far[1:], lane_peers, scan)

    def query_copy(d):
        slot = (c + 3) % 4
        return to(query_ref, queries_ref.at[slot], query_send.at[d - 1], query_recv.at[slot], far[4 - d])

    for d in (1, 2, 3):

        @pl.when(c >= d)
        def _():
            query_copy(d).start()

    along_line = [
        to(kv_ref, kvs_ref.at[zl, y], line_send.at[d - 1], line_recv.at[d - 1], line[d]) for d in (1, 2, 3)
    ]
    along_row = [
        [
            to(
                kv_ref if d == 0 else kvs_ref.at[(zl - d + 4) % 4, y],
                kvs_ref.at[(zl - d + 4) % 4, y], row_send.at[d, k], row_recv.at[d, k], row[1 if k == 0 else 3],
            )
            for k in range(2)
        ]
        for d in range(4)
    ]

    def onward(d, k):
        block = kvs_ref.at[(zl - d + 4) % 4, (y + 3) % 4 if k == 0 else (y + 1) % 4, k * 128 : k * 128 + 128]
        return to(block, block, half_send.at[d, k], half_recv.at[d, k], row[1 if k == 0 else 3])

    halves = [[onward(d, k) for k in range(2)] for d in range(4)]
    for copy in along_row[0] + along_line:
        copy.start()
    row_states = [
        to(state_ref, rows_ref.at[y], state_send.at[0, d - 1], state_recv.at[0, d - 1], row[d])
        for d in (1, 2, 3)
    ]
    for copy in row_states + column_copies:
        copy.start()
    for d in range(4):
        if d < 3:
            along_line[d].wait_recv()
            for copy in along_row[d + 1]:
                copy.start()
        for k in range(2):
            along_row[d][k].wait_recv()
            halves[d][k].start()
        if d == 0:
            for copy in row_states:
                copy.wait_recv()
            state, total, ahead, ahead_total = chain(rows_ref, y)
            planes_ref[zl, 0:REC_VAL, :] = state
            planes_ref[zl, REC_VAL:STATE_ROWS, :] = jnp.broadcast_to(total, (8, REC_KEY))
            line_states = [
                to(planes_ref.at[zl], planes_ref.at[zl], state_send.at[1, n - 1], state_recv.at[1, n - 1], line[n])
                for n in (1, 2, 3)
            ]
            for copy in line_states:
                copy.start()
    for copy in line_states:
        copy.wait_recv()
    state, total, low, low_total = chain(planes_ref, zl)
    group_ref[0:REC_VAL, :] = state
    group_ref[REC_VAL:STATE_ROWS, :] = jnp.broadcast_to(total, (8, REC_KEY))
    before = low * jnp.exp(ahead_total) + ahead
    before_total = low_total + ahead_total

    def back(k, d):
        slot = (c + d + 3) % 4
        src, dst = ((group_ref, groups_ref), (far_ref, part_ref), (far_left_ref, part_left_ref))[k]
        src = src if k == 0 else src.at[slot % 3]
        return to(src, dst.at[c % 3], back_send.at[k, d - 1], back_recv.at[k, c % 3], far[d])

    def arrival(k, g):
        src, dst = ((group_ref, groups_ref), (far_ref.at[0], part_ref), (far_left_ref.at[0], part_left_ref))[k]
        return to(src, dst.at[g], back_send.at[k, 0], back_recv.at[k, g], far[1])

    for d in (1, 2, 3):

        @pl.when(c + d < 4)
        def _():
            back(0, d).start()

    for pair in halves:
        for copy in pair:
            copy.wait_recv()
    for n in (1, 2, 3):

        @pl.when(c < n)
        def _():
            to(
                query_ref, queries_ref.at[n - 1], query_send.at[0], query_recv.at[n - 1], far[1]
            ).wait_recv()

    lane = lax.broadcasted_iota(jnp.int32, (128, 128), 1)
    for n in range(4):
        packed = (query_ref[...] if n == 0 else queries_ref[n - 1]).astype(F32)
        for half in range(2):
            part = packed if half == 0 else pltpu.roll(packed, 64, 1)
            at = n * TOK + half * 128
            q_ref[at : at + 128, :] = jnp.where(lane < HEAD, part, 0.0).astype(BF16)

    attend(zl * 4 + y, bias_ref[0] * LOG2E, q_ref, kvs_ref, tri_ref, acc_ref, left_ref)

    for n in range(3):
        at = (n + 1) * TOK
        top = acc_ref[at : at + 128, :]
        bottom = pltpu.roll(acc_ref[at + 128 : at + 256, :], 64, 1)
        far_ref[n] = jnp.where(lane < HEAD, bottom, top).astype(BF16)
        for half in range(2):
            turned = jnp.transpose(left_ref[at + half * 128 : at + half * 128 + 128, :])
            far_left_ref[n, :, half * 128 : half * 128 + 128] = turned[0:8, :]
    for d in (1, 2, 3):

        @pl.when(c + d < 4)
        def _():
            back(1, d).start()
            back(2, d).start()

    in_ref[...] = jnp.zeros_like(in_ref)
    for g in (0, 1, 2):

        @pl.when(g < c)
        def _():
            arrival(0, g).wait_recv()
            in_ref[...] = in_ref[...] * jnp.exp(groups_ref[g, REC_VAL : REC_VAL + 1, :]) + groups_ref[
                g, 0:REC_VAL, :
            ]

    entering = in_ref[...] * jnp.exp(before_total) + before
    raw = local_ref[...] + dot(faded_ref[...], entering.astype(BF16), tb=True)
    normed = raw * lax.rsqrt(jnp.mean(raw * raw, axis=1, keepdims=True) + epsilon) * gain_ref[...]
    gate = gate_ref[...].astype(F32)
    heads_ref[:, 0:REC_VAL] = (normed * (gate * jax.nn.sigmoid(gate))).astype(BF16)

    for g in (2, 1, 0):

        @pl.when(g < c)
        def _():
            arrival(1, g).wait_recv()
            arrival(2, g).wait_recv()
            packed = part_ref[g].astype(F32)
            scale = jnp.exp2(left_ref[0:TOK, :])
            acc_ref[0:128, :] += packed * scale[0:128, :]
            acc_ref[128:256, :] += pltpu.roll(packed, 64, 1) * scale[128:256, :]
            for at in (0, 128):
                left_ref[at : at + 128, :] += column(part_left_ref[g, 0:1, at : at + 128])

    heads_ref[:, REC_VAL:] = acc_ref[0:TOK, HEAD:].astype(BF16)

    for copy in own_columns:
        copy.wait()
    for copy in column_copies:
        copy.wait_recv()
    sent = along_line + row_states + line_states + column_copies
    for d in range(4):
        sent = sent + along_row[d] + halves[d]
    for copy in sent:
        copy.wait_send()
    for d in (1, 2, 3):

        @pl.when(c >= d)
        def _():
            query_copy(d).wait_send()

        @pl.when(c + d < 4)
        def _():
            for k in range(3):
                back(k, d).wait_send()


def mix(*operands):
    dma = pltpu.SemaphoreType.DMA
    return pl.pallas_call(
        mix_kernel,
        out_shape=(
            jax.ShapeDtypeStruct((TOK, 128), BF16),
            jax.ShapeDtypeStruct((8, 128, 256), BF16),
        ),
        in_specs=[SMEM] + [VMEM] * 9 + [ANY] * 2,
        out_specs=(VMEM,) * 2,
        scratch_shapes=[
            pltpu.VMEM((4, 4, TOK, 128), BF16),
            pltpu.VMEM((3, 128, 128), BF16),
            pltpu.VMEM((STATE_ROWS, REC_KEY), F32),
            pltpu.VMEM((4, STATE_ROWS, REC_KEY), F32),
            pltpu.VMEM((4, STATE_ROWS, REC_KEY), F32),
            pltpu.VMEM((STATE_ROWS, REC_KEY), F32),
            pltpu.VMEM((3, STATE_ROWS, REC_KEY), F32),
            pltpu.VMEM((TOK, REC_VAL), F32),
            pltpu.VMEM((TOK, REC_KEY), BF16),
            pltpu.VMEM((4 * TOK, 128), BF16),
            pltpu.VMEM((TOK, TOK), BF16),
            pltpu.VMEM((4 * TOK, 128), F32),
            pltpu.VMEM((4 * TOK, 128), F32),
            pltpu.VMEM((3, 128, 128), BF16),
            pltpu.VMEM((3, 8, TOK), F32),
            pltpu.VMEM((3, 128, 128), BF16),
            pltpu.VMEM((3, 8, TOK), F32),
            pltpu.VMEM((REC_VAL, REC_KEY), F32),
            dma((3,)), dma((3,)), dma((4, 2)), dma((4, 2)), dma((4, 2)), dma((4, 2)), dma((2, 3)), dma((2, 3)),
            dma((3,)), dma((3,)), dma((2, 7)), dma((2, 7)), dma((3, 3)), dma((3, 3)), dma((2,)),
        ],
        compiler_params=pltpu.CompilerParams(collective_id=0, has_side_effects=True),
        name="mix",
    )(*operands)


def shards(
    tokens,
    input_norm_gain,
    attention_query_weight,
    attention_key_weight,
    attention_value_weight,
    attention_score_bias,
    recurrence_query_weight,
    forget_weight,
    input_weight,
    output_gate_weight,
    forget_minimum,
    decay_spikes,
    head_norm_gain,
    attention_output_weight,
    recurrence_output_weight,
):
    narrow = (
        attention_key_weight, attention_value_weight, input_weight, output_gate_weight, attention_query_weight
    )
    kv, query, rec, forget, inputs, gate = project(
        tokens, input_norm_gain[None, :], *(w.T for w in narrow), recurrence_query_weight, forget_weight
    )
    heads, columns = mix(
        attention_score_bias, kv, query, rec, forget, inputs, gate,
        forget_minimum, decay_spikes.reshape(1, TOK), head_norm_gain[None, :],
        recurrence_output_weight, attention_output_weight,
    )
    return output(heads, columns)


def solution(mesh):
    placed = (
        P("sp", "tp"),
        P(),
        P(None, "tp"),
        P(None, "tp"),
        P(None, "tp"),
        P("tp"),
        P(None, "tp"),
        P(None, "tp"),
        P(None, "tp"),
        P(None, "tp"),
        P("tp", None),
        P("sp", "tp"),
        P(),
        P("tp", None),
        P("tp", None),
    )
    return jax.shard_map(
        shards, mesh=mesh, in_specs=placed, out_specs=P("sp", "tp"), check_vma=False
    )
```

time: 110 us -> 84 us (0.76)
  the two profiles are of different devices: /device:TPU:1 before, /device:TPU:33 now
where the time goes in v4:
time: 84 us; the launch traced here: 83.7 us
  Pallas kernels  81.5 us (97%)
  local copies, waits for them, and re-layouts  1.57 us (2%)
    pallas_call x1, Pallas kernels, mix(): pl.pallas_call(mix_kernel, out_shape=(jax.ShapeDtypeStruct((TOK, 128), BF...  48.4 us
    pallas_call x1, Pallas kernels, output(): pl.pallas_call(output_kernel, out_shape=jax.ShapeDtypeStruct((TOK, 256),...  18.9 us
    pallas_call x1, Pallas kernels, project(): pl.pallas_call(project_kernel, out_shape=(wide, jax.ShapeDtypeStruct((128...  14.2 us

profile of v4, /device:TPU:33, one launch (start us, length us, event | category | flops | bytes accessed | tf_op | source)
XLA Modules:
  0.0 83.7 jit_solution(1610441847983403339)
XLA Ops:
  0.7 14.2 %project.1 = (bf16[256,128]{1,0:T(8,128)(2,1)}, bf16[128,128]{1,0:T(8,128)(2,1)}, bf16[256,128]{1,0:T(8,128)(2,1)}, bf16[256,128]{1,0:T(8,128)(2,1)}, bf16[256,64]{1,0:T(8,128)(2,1)}, /*index=5*/bf16[256,64]{1,0:T(8,128)(2,1)}) custom-call(bf16[256,256]{1,0:T(8,128)(2,1)} %token_ref.1, f32[1,2048]{1,0:T(1,128)} %bitcast.13, bf16[64,2048]{1,0:T(8,128)(2,1)} %bitcast.8, ...), custom_call_target="tpu_custom_call" | custom-call | tf_op jit(solution)/shard_map/project/pallas_call | solution.py:175
  14.8 48.4 %mix.1 = (bf16[256,128]{1,0:T(8,128)(2,1)}, bf16[8,128,256]{2,1,0:T(8,128)(2,1)}) custom-call(f32[1]{0:T(128)S(6)} %copy.17.bias_ref, bf16[256,128]{1,0:T(8,128)(2,1)} %get-tuple-element.13.kv_ref, bf16[128,128]{1,0:T(8,128)(2,1)} %get-tuple-element.14.query_ref, bf16[256,128]{1,0:T(8,128)(2,1)} %get-tuple-element.15.rec_ref, ...), custom_call_target="tpu_custom_call" | custom-call | tf_op jit(solution)/shard_map/mix/pallas_call | solution.py:543
  63.3 18.9 %output.1 = bf16[256,256]{1,0:T(8,128)(2,1)} custom-call(bf16[256,128]{1,0:T(8,128)(2,1)} %get-tuple-element.19.heads_ref, bf16[8,128,256]{2,1,0:T(8,128)(2,1)} %get-tuple-element.20.weight_ref), custom_call_target="tpu_custom_call" | custom-call | tf_op jit(solution)/shard_map/output/pallas_call | solution.py:206
  82.2 1.6 %copy.18 = bf16[256,256]{1,0:T(8,128)(2,1)} copy(bf16[256,256]{1,0:T(8,128)(2,1)} %output.1) | data formatting | bytes 262144

commit v5 on v4

--- a/solution.py
+++ b/solution.py
@@ -40,16 +40,6 @@
     return sp, sp // 16, (sp // 4) % 4, sp % 4
 
 
-def greet(peers, lane_peers=(), meanwhile=lambda: None):
-    barrier = pltpu.get_barrier_semaphore()
-    for peer in peers:
-        pl.semaphore_signal(barrier, inc=1, device_id={"sp": peer}, device_id_type=MESH)
-    for peer in lane_peers:
-        pl.semaphore_signal(barrier, inc=1, device_id={"tp": peer}, device_id_type=MESH)
-    meanwhile()
-    pl.semaphore_wait(barrier, len(peers) + len(lane_peers))
-
-
 def lanes():
     tp = lax.axis_index("tp")
     x, core = tp // 2, tp % 2
@@ -70,10 +60,6 @@
     def relay(n, source, part, target):
         return copy(n, slots_ref.at[source, part], slots_ref.at[source, part], target)
 
-    barrier = pltpu.get_barrier_semaphore()
-    for peer in (partner, right, left):
-        pl.semaphore_signal(barrier, inc=1, device_id={"tp": peer}, device_id_type=MESH)
-    pl.semaphore_wait(barrier, 3)
     copies = [
         copy(0, chunk_ref, slots_ref.at[tp], partner),
         copy(1, chunk_ref.at[top], slots_ref.at[tp, top], right),
@@ -125,99 +111,6 @@
         one.wait_send()
 
 
-def project_kernel(
-    token_ref, gain_ref, key_w, value_w, input_w, gate_w, query_w, rec_w, forget_w,
-    kv_ref, query_ref, rec_ref, forget_ref, input_ref, gate_ref,
-    slots_ref, narrow_ref, wide_ref, first_ref, second_ref, square_ref, send, recv, load,
-):
-    narrow = (key_w, value_w, input_w, gate_w, query_w)
-    loads = [
-        pltpu.make_async_copy(w, narrow_ref.at[n * 64 : n * 64 + 64], load.at[n])
-        for n, w in enumerate(narrow)
-    ]
-    loads += [
-        pltpu.make_async_copy(w, wide_ref.at[:, n * 128 : n * 128 + 128], load.at[5 + n])
-        for n, w in enumerate((rec_w, forget_w))
-    ]
-    for one in loads:
-        one.start()
-    first_ref[...] = jnp.zeros_like(first_ref)
-    second_ref[...] = jnp.zeros_like(second_ref)
-    square_ref[...] = jnp.zeros_like(square_ref)
-
-    def meanwhile():
-        for one in loads:
-            one.wait()
-
-    def use(source, ref):
-        at = pl.ds(pl.multiple_of(source * 256, 256), 256)
-        values = ref[...].astype(F32)
-        squares = values * values
-        square_ref[...] += squares[:, 0:128] + squares[:, 128:256]
-        scaled = (values * gain_ref[:, at]).astype(BF16)
-        first_ref[...] += dot(scaled, narrow_ref[:, at], tb=True)
-        second_ref[...] += dot(scaled, wide_ref[at, :])
-
-    ring_gather(token_ref, slots_ref, send, recv, meanwhile, use)
-    inverse = lax.rsqrt(jnp.sum(square_ref[...], axis=1, keepdims=True) / D + epsilon)
-    kv_ref[...] = (first_ref[:, 0:128] * inverse).astype(BF16)
-    input_ref[...] = (first_ref[:, 128:192] * inverse).astype(BF16)
-    gate_ref[...] = (first_ref[:, 192:256] * inverse).astype(BF16)
-    query = (first_ref[:, 256:320] * inverse).astype(BF16)
-    query_ref[...] = jnp.concatenate([query[0:128], query[128:256]], axis=1)
-    rec_ref[...] = (second_ref[:, 0:128] * inverse).astype(BF16)
-    forget_ref[...] = (second_ref[:, 128:256] * inverse).astype(BF16)
-
-
-def project(tokens, gain, *weights):
-    dma = pltpu.SemaphoreType.DMA
-    wide, narrow = jax.ShapeDtypeStruct((TOK, 128), BF16), jax.ShapeDtypeStruct((TOK, 64), BF16)
-    return pl.pallas_call(
-        project_kernel,
-        out_shape=(wide, jax.ShapeDtypeStruct((128, 128), BF16), wide, wide, narrow, narrow),
-        in_specs=[VMEM, VMEM] + [ANY] * 7,
-        out_specs=(VMEM,) * 6,
-        scratch_shapes=[
-            pltpu.VMEM((8, TOK, 256), BF16),
-            pltpu.VMEM((320, D), BF16),
-            pltpu.VMEM((D, 256), BF16),
-            pltpu.VMEM((TOK, 320), F32),
-            pltpu.VMEM((TOK, 256), F32),
-            pltpu.VMEM((TOK, 128), F32),
-            dma((13,)), dma((13,)), dma((7,)),
-        ],
-        compiler_params=pltpu.CompilerParams(collective_id=2, has_side_effects=True),
-        name="project",
-    )(tokens, gain, *weights)
-
-
-def output_kernel(heads_ref, weight_ref, out_ref, slots_ref, acc_ref, send, recv):
-    acc_ref[...] = jnp.zeros_like(acc_ref)
-
-    def use(source, ref):
-        acc_ref[...] += dot(ref[...], weight_ref[source])
-
-    ring_gather(heads_ref, slots_ref, send, recv, lambda: None, use)
-    out_ref[...] = acc_ref[...].astype(BF16)
-
-
-def output(heads, weight):
-    dma = pltpu.SemaphoreType.DMA
-    return pl.pallas_call(
-        output_kernel,
-        out_shape=jax.ShapeDtypeStruct((TOK, 256), BF16),
-        in_specs=[VMEM, VMEM],
-        out_specs=VMEM,
-        scratch_shapes=[
-            pltpu.VMEM((8, TOK, 128), BF16),
-            pltpu.VMEM((TOK, 256), F32),
-            dma((13,)), dma((13,)),
-        ],
-        compiler_params=pltpu.CompilerParams(collective_id=3, has_side_effects=True),
-        name="output",
-    )(heads, weight)
-
-
 def column(row):
     return jnp.transpose(jnp.broadcast_to(row, (128, 128)))
 
@@ -266,10 +159,9 @@
     return z, soft, later
 
 
-def attend(here, bias2, q_ref, kvs_ref, tri_ref, acc_ref, left_ref):
+def attend(here, plane, bias2, q_ref, kvs_ref, tri_ref, acc_ref, left_ref):
     rows = lax.broadcasted_iota(jnp.int32, (TOK, TOK), 0)
     cols = lax.broadcasted_iota(jnp.int32, (TOK, TOK), 1)
-    tri_ref[...] = jnp.where(rows > cols, -1.0, 0.0).astype(BF16)
     acc_ref[...] = jnp.zeros_like(acc_ref)
     left_ref[...] = jnp.zeros_like(left_ref)
 
@@ -278,9 +170,9 @@
         q_own, q_far = q_ref[0:TOK, :], q_ref[TOK:, :]
         kvs, own, far = [], [], []
         for u in range(2):
-            m = 15 - 2 * i - u
-            kv = kvs_ref[m // 4, m % 4]
-            keep = cols - rows < (here - m) * TOK
+            n = 3 - 2 * i - u
+            kv = kvs_ref[plane, n]
+            keep = cols - rows < (here - plane * 4 - n) * TOK
             kvs.append(kv)
             own.append(stick_tile(q_own, kv, tri, bias2, keep) + (keep,))
             far.append(stick_tile(q_far, kv, tri, bias2))
@@ -301,7 +193,7 @@
         left_ref[TOK:, :] = jnp.broadcast_to(left_far, (3 * TOK, 128))
         return 0
 
-    lax.fori_loop(0, 8, pair, 0)
+    lax.fori_loop(0, 2, pair, 0)
 
 
 def chain(states_ref, here):
@@ -317,15 +209,19 @@
     return state, total, ahead, ahead_total
 
 
-def mix_kernel(
-    bias_ref, kv_ref, query_ref, rec_ref, forget_ref, input_ref, gate_ref, low_ref, spike_ref, gain_ref,
-    rec_out_w, att_out_w,
-    heads_ref, columns_ref,
+def layer_kernel(
+    bias_ref, token_ref, feature_gain_ref, low_ref, spike_ref, gain_ref,
+    key_w, value_w, input_w, gate_w, query_w, rec_w, forget_w, rec_out_w, att_out_w,
+    out_ref,
+    slots_ref, narrow_ref, wide_ref, first_ref, second_ref, square_ref,
+    kv_ref, query_ref, rec_ref, forget_ref, input_ref, gate_ref,
     kvs_ref, queries_ref, state_ref, rows_ref, planes_ref, group_ref, groups_ref,
     local_ref, faded_ref, q_ref, tri_ref, acc_ref, left_ref,
     far_ref, far_left_ref, part_ref, part_left_ref, in_ref,
+    heads_ref, columns_ref, head_slots_ref, sum_ref,
+    load, token_send, token_recv, head_send, head_recv,
     line_send, line_recv, row_send, row_recv, half_send, half_recv, state_send, state_recv,
-    query_send, query_recv, column_send, column_recv, back_send, back_recv, own_sem,
+    query_send, query_recv, column_send, column_recv, back_send, back_recv, own_sem, near_sem,
 ):
     sp, c, zl, y = place()
     tp = lax.axis_index("tp")
@@ -335,6 +231,16 @@
     far = [(sp + 16 * d) % 64 for d in range(4)]
     lane_peers = [(tp + d) % 8 for d in range(1, 8)]
 
+    narrow = (key_w, value_w, input_w, gate_w, query_w)
+    loads = [
+        pltpu.make_async_copy(w, narrow_ref.at[n * 64 : n * 64 + 64], load.at[n])
+        for n, w in enumerate(narrow)
+    ]
+    loads += [
+        pltpu.make_async_copy(w, wide_ref.at[:, n * 128 : n * 128 + 128], load.at[5 + n])
+        for n, w in enumerate((rec_w, forget_w))
+    ]
+
     def columns(w, there):
         return w.at[:, pl.ds(pl.multiple_of(there * 256, 256), 256)]
 
@@ -352,27 +258,61 @@
         for n, w in out_w
         for d, there in enumerate(lane_peers)
     ]
-    for copy in own_columns:
+
+    barrier = pltpu.get_barrier_semaphore()
+    near = row[1:] + line[1:] + [far[1], far[3]]
+    for peer in lane_peers:
+        pl.semaphore_signal(barrier, inc=1, device_id={"tp": peer}, device_id_type=MESH)
+    for peer in near:
+        pl.semaphore_signal(barrier, inc=1, device_id={"sp": peer}, device_id_type=MESH)
+    for copy in loads + own_columns:
         copy.start()
-
-    def scan():
-        local_scan(
-            rec_ref, forget_ref, input_ref, low_ref, spike_ref, local_ref, faded_ref, state_ref
-        )
-        rows_ref[y] = state_ref[...]
-        kvs_ref[zl, y] = kv_ref[...]
-        for n in (1, 2, 3):
-
-            @pl.when(c >= n)
-            def _():
-                queries_ref[n - 1] = jnp.zeros((128, 128), BF16)
-
-    greet(row[1:] + line[1:] + far[1:], lane_peers, scan)
+    first_ref[...] = jnp.zeros_like(first_ref)
+    second_ref[...] = jnp.zeros_like(second_ref)
+    square_ref[...] = jnp.zeros_like(square_ref)
+    rows = lax.broadcasted_iota(jnp.int32, (TOK, TOK), 0)
+    cols = lax.broadcasted_iota(jnp.int32, (TOK, TOK), 1)
+    tri_ref[...] = jnp.where(rows > cols, -1.0, 0.0).astype(BF16)
+    pl.semaphore_wait(barrier, len(lane_peers) + len(near))
+    for peer in (far[1], far[3]):
+        pl.semaphore_signal(near_sem, inc=1, device_id={"sp": peer}, device_id_type=MESH)
+
+    def meanwhile():
+        for one in loads:
+            one.wait()
+
+    def use(source, ref):
+        at = pl.ds(pl.multiple_of(source * 256, 256), 256)
+        values = ref[...].astype(F32)
+        squares = values * values
+        square_ref[...] += squares[:, 0:128] + squares[:, 128:256]
+        scaled = (values * feature_gain_ref[:, at]).astype(BF16)
+        first_ref[...] += dot(scaled, narrow_ref[:, at], tb=True)
+        second_ref[...] += dot(scaled, wide_ref[at, :])
+
+    ring_gather(token_ref, slots_ref, token_send, token_recv, meanwhile, use)
+    inverse = lax.rsqrt(jnp.sum(square_ref[...], axis=1, keepdims=True) / D + epsilon)
+    query = (first_ref[:, 256:320] * inverse).astype(BF16)
+    query_ref[...] = jnp.concatenate([query[0:128], query[128:256]], axis=1)
+    kv = (first_ref[:, 0:128] * inverse).astype(BF16)
+    kv_ref[...] = kv
+    kvs_ref[zl, y] = kv
+    for n in (1, 2, 3):
+
+        @pl.when(c >= n)
+        def _():
+            queries_ref[n - 1] = jnp.zeros((128, 128), BF16)
+
+    input_ref[...] = (first_ref[:, 128:192] * inverse).astype(BF16)
+    gate_ref[...] = (first_ref[:, 192:256] * inverse).astype(BF16)
+    rec_ref[...] = (second_ref[:, 0:128] * inverse).astype(BF16)
+    forget_ref[...] = (second_ref[:, 128:256] * inverse).astype(BF16)
 
     def query_copy(d):
         slot = (c + 3) % 4
         return to(query_ref, queries_ref.at[slot], query_send.at[d - 1], query_recv.at[slot], far[4 - d])
 
+    pl.semaphore_wait(near_sem, 2)
     for d in (1, 2, 3):
 
         @pl.when(c >= d)
@@ -400,32 +340,68 @@
     halves = [[onward(d, k) for k in range(2)] for d in range(4)]
     for copy in along_row[0] + along_line:
         copy.start()
+    local_scan(rec_ref, forget_ref, input_ref, low_ref, spike_ref, local_ref, faded_ref, state_ref)
+    rows_ref[y] = state_ref[...]
     row_states = [
         to(state_ref, rows_ref.at[y], state_send.at[0, d - 1], state_recv.at[0, d - 1], row[d])
         for d in (1, 2, 3)
     ]
-    for copy in row_states + column_copies:
-        copy.start()
-    for d in range(4):
-        if d < 3:
-            along_line[d].wait_recv()
-            for copy in along_row[d + 1]:
-                copy.start()
+
+    def pass_on(d):
         for k in range(2):
             along_row[d][k].wait_recv()
             halves[d][k].start()
-        if d == 0:
-            for copy in row_states:
-                copy.wait_recv()
-            state, total, ahead, ahead_total = chain(rows_ref, y)
-            planes_ref[zl, 0:REC_VAL, :] = state
-            planes_ref[zl, REC_VAL:STATE_ROWS, :] = jnp.broadcast_to(total, (8, REC_KEY))
-            line_states = [
-                to(planes_ref.at[zl], planes_ref.at[zl], state_send.at[1, n - 1], state_recv.at[1, n - 1], line[n])
-                for n in (1, 2, 3)
-            ]
-            for copy in line_states:
-                copy.start()
+
+    along_line[0].wait_recv()
+    for copy in along_row[1]:
+        copy.start()
+    pass_on(0)
+    along_line[1].wait_recv()
+    for copy in along_row[2] + row_states:
+        copy.start()
+    pass_on(1)
+    along_line[2].wait_recv()
+    for copy in along_row[3] + column_copies:
+        copy.start()
+    for copy in row_states:
+        copy.wait_recv()
+    state, total, ahead, ahead_total = chain(rows_ref, y)
+    planes_ref[zl, 0:REC_VAL, :] = state
+    planes_ref[zl, REC_VAL:STATE_ROWS, :] = jnp.broadcast_to(total, (8, REC_KEY))
+    line_states = [
+        to(planes_ref.at[zl], planes_ref.at[zl], state_send.at[1, n - 1], state_recv.at[1, n - 1], line[n])
+        for n in (1, 2, 3)
+    ]
+    for copy in line_states:
+        copy.start()
+    for n in (1, 2, 3):
+
+        @pl.when(c < n)
+        def _():
+            to(
+                query_ref, queries_ref.at[n - 1], query_send.at[0], query_recv.at[n - 1], far[1]
+            ).wait_recv()
+
+    lane = lax.broadcasted_iota(jnp.int32, (128, 128), 1)
+    for n in range(4):
+        packed = (query_ref[...] if n == 0 else queries_ref[n - 1]).astype(F32)
+        for half in range(2):
+            part = packed if half == 0 else pltpu.roll(packed, 64, 1)
+            at = n * TOK + half * 128
+            q_ref[at : at + 128, :] = jnp.where(lane < HEAD, part, 0.0).astype(BF16)
+
+    def attend_plane(d):
+        for k in range(2):
+            halves[d][k].wait_recv()
+        attend(
+            zl * 4 + y, (zl - d + 4) % 4, bias_ref[0] * LOG2E, q_ref, kvs_ref, tri_ref,
+            acc_ref.at[d], left_ref.at[d],
+        )
+
+    attend_plane(0)
+    pass_on(2)
+    attend_plane(1)
+    pass_on(3)
     for copy in line_states:
         copy.wait_recv()
     state, total, low, low_total = chain(planes_ref, zl)
@@ -450,41 +426,35 @@
         def _():
             back(0, d).start()
 
-    for pair in halves:
-        for copy in pair:
-            copy.wait_recv()
-    for n in (1, 2, 3):
-
-        @pl.when(c < n)
-        def _():
-            to(
-                query_ref, queries_ref.at[n - 1], query_send.at[0], query_recv.at[n - 1], far[1]
-            ).wait_recv()
-
-    lane = lax.broadcasted_iota(jnp.int32, (128, 128), 1)
-    for n in range(4):
-        packed = (query_ref[...] if n == 0 else queries_ref[n - 1]).astype(F32)
-        for half in range(2):
-            part = packed if half == 0 else pltpu.roll(packed, 64, 1)
-            at = n * TOK + half * 128
-            q_ref[at : at + 128, :] = jnp.where(lane < HEAD, part, 0.0).astype(BF16)
-
-    attend(zl * 4 + y, bias_ref[0] * LOG2E, q_ref, kvs_ref, tri_ref, acc_ref, left_ref)
+    attend_plane(2)
+    attend_plane(3)
+
+    def joined(at):
+        n = (zl + 1) % 4
+        acc, left = acc_ref[n, at, :], left_ref[n, at, :]
+        for p in (2, 1, 0):
+            n = (zl - p + 4) % 4
+            acc = acc + acc_ref[n, at, :] * jnp.exp2(left)
+            left = left + left_ref[n, at, :]
+        return acc, left
 
     for n in range(3):
         at = (n + 1) * TOK
-        top = acc_ref[at : at + 128, :]
-        bottom = pltpu.roll(acc_ref[at + 128 : at + 256, :], 64, 1)
-        far_ref[n] = jnp.where(lane < HEAD, bottom, top).astype(BF16)
-        for half in range(2):
-            turned = jnp.transpose(left_ref[at + half * 128 : at + half * 128 + 128, :])
-            far_left_ref[n, :, half * 128 : half * 128 + 128] = turned[0:8, :]
-    for d in (1, 2, 3):
+        top, top_left = joined(slice(at, at + 128))
+        bottom, bottom_left = joined(slice(at + 128, at + 256))
+        far_ref[n] = jnp.where(lane < HEAD, pltpu.roll(bottom, 64, 1), top).astype(BF16)
+        far_left_ref[n, :, 0:128] = jnp.transpose(top_left)[0:1, :]
+        far_left_ref[n, :, 128:256] = jnp.transpose(bottom_left)[0:1, :]
+    for d in (3, 2, 1):
 
         @pl.when(c + d < 4)
         def _():
             back(1, d).start()
             back(2, d).start()
+
+    own_acc, own_left = joined(slice(0, TOK))
+    acc_ref[0, 0:TOK, :] = own_acc
+    left_ref[0, 0:TOK, :] = own_left
 
     in_ref[...] = jnp.zeros_like(in_ref)
     for g in (0, 1, 2):
@@ -509,18 +479,27 @@
             arrival(1, g).wait_recv()
             arrival(2, g).wait_recv()
             packed = part_ref[g].astype(F32)
-            scale = jnp.exp2(left_ref[0:TOK, :])
-            acc_ref[0:128, :] += packed * scale[0:128, :]
-            acc_ref[128:256, :] += pltpu.roll(packed, 64, 1) * scale[128:256, :]
+            scale = jnp.exp2(left_ref[0, 0:TOK, :])
+            acc_ref[0, 0:128, :] += packed * scale[0:128, :]
+            acc_ref[0, 128:256, :] += pltpu.roll(packed, 64, 1) * scale[128:256, :]
             for at in (0, 128):
-                left_ref[at : at + 128, :] += column(part_left_ref[g, 0:1, at : at + 128])
-
-    heads_ref[:, REC_VAL:] = acc_ref[0:TOK, HEAD:].astype(BF16)
-
-    for copy in own_columns:
-        copy.wait()
-    for copy in column_copies:
-        copy.wait_recv()
+                left_ref[0, at : at + 128, :] += column(part_left_ref[g, 0:1, at : at + 128])
+
+    heads_ref[:, REC_VAL:] = acc_ref[0, 0:TOK, HEAD:].astype(BF16)
+
+    def columns_here():
+        for copy in own_columns:
+            copy.wait()
+        for copy in column_copies:
+            copy.wait_recv()
+
+    sum_ref[...] = jnp.zeros_like(sum_ref)
+
+    def add(source, ref):
+        sum_ref[...] += dot(ref[...], columns_ref[source])
+
+    ring_gather(heads_ref, head_slots_ref, head_send, head_recv, columns_here, add)
+    out_ref[...] = sum_ref[...].astype(BF16)
     sent = along_line + row_states + line_states + column_copies
     for d in range(4):
         sent = sent + along_row[d] + halves[d]
@@ -538,17 +517,30 @@
                 back(k, d).wait_send()
 
 
-def mix(*operands):
+def layer(*operands):
     dma = pltpu.SemaphoreType.DMA
+
+    def both(*shape):
+        return [dma(shape), dma(shape)]
+
     return pl.pallas_call(
-        mix_kernel,
-        out_shape=(
-            jax.ShapeDtypeStruct((TOK, 128), BF16),
-            jax.ShapeDtypeStruct((8, 128, 256), BF16),
-        ),
-        in_specs=[SMEM] + [VMEM] * 9 + [ANY] * 2,
-        out_specs=(VMEM,) * 2,
+        layer_kernel,
+        out_shape=jax.ShapeDtypeStruct((TOK, 256), BF16),
+        in_specs=[SMEM] + [VMEM] * 5 + [ANY] * 9,
+        out_specs=VMEM,
         scratch_shapes=[
+            pltpu.VMEM((8, TOK, 256), BF16),
+            pltpu.VMEM((320, D), BF16),
+            pltpu.VMEM((D, 256), BF16),
+            pltpu.VMEM((TOK, 320), F32),
+            pltpu.VMEM((TOK, 256), F32),
+            pltpu.VMEM((TOK, 128), F32),
+            pltpu.VMEM((TOK, 128), BF16),
+            pltpu.VMEM((128, 128), BF16),
+            pltpu.VMEM((TOK, 128), BF16),
+            pltpu.VMEM((TOK, 128), BF16),
+            pltpu.VMEM((TOK, 64), BF16),
+            pltpu.VMEM((TOK, 64), BF16),
             pltpu.VMEM((4, 4, TOK, 128), BF16),
             pltpu.VMEM((3, 128, 128), BF16),
             pltpu.VMEM((STATE_ROWS, REC_KEY), F32),
@@ -560,18 +552,23 @@
             pltpu.VMEM((TOK, REC_KEY), BF16),
             pltpu.VMEM((4 * TOK, 128), BF16),
             pltpu.VMEM((TOK, TOK), BF16),
-            pltpu.VMEM((4 * TOK, 128), F32),
-            pltpu.VMEM((4 * TOK, 128), F32),
+            pltpu.VMEM((4, 4 * TOK, 128), F32),
+            pltpu.VMEM((4, 4 * TOK, 128), F32),
             pltpu.VMEM((3, 128, 128), BF16),
-            pltpu.VMEM((3, 8, TOK), F32),
+            pltpu.VMEM((3, 1, TOK), F32),
             pltpu.VMEM((3, 128, 128), BF16),
-            pltpu.VMEM((3, 8, TOK), F32),
+            pltpu.VMEM((3, 1, TOK), F32),
             pltpu.VMEM((REC_VAL, REC_KEY), F32),
-            dma((3,)), dma((3,)), dma((4, 2)), dma((4, 2)), dma((4, 2)), dma((4, 2)), dma((2, 3)), dma((2, 3)),
-            dma((3,)), dma((3,)), dma((2, 7)), dma((2, 7)), dma((3, 3)), dma((3, 3)), dma((2,)),
+            pltpu.VMEM((TOK, 128), BF16),
+            pltpu.VMEM((8, 128, 256), BF16),
+            pltpu.VMEM((8, TOK, 128), BF16),
+            pltpu.VMEM((TOK, 256), F32),
+            dma((7,)), *both(13), *both(13),
+            *both(3), *both(4, 2), *both(4, 2), *both(2, 3),
+            *both(3), *both(2, 7), *both(3, 3), dma((2,)), pltpu.SemaphoreType.REGULAR,
         ],
         compiler_params=pltpu.CompilerParams(collective_id=0, has_side_effects=True),
-        name="mix",
+        name="layer",
     )(*operands)
 
 
@@ -595,15 +592,12 @@
     narrow = (
         attention_key_weight, attention_value_weight, input_weight, output_gate_weight, attention_query_weight
     )
-    kv, query, rec, forget, inputs, gate = project(
-        tokens, input_norm_gain[None, :], *(w.T for w in narrow), recurrence_query_weight, forget_weight
-    )
-    heads, columns = mix(
-        attention_score_bias, kv, query, rec, forget, inputs, gate,
-        forget_minimum, decay_spikes.reshape(1, TOK), head_norm_gain[None, :],
+    return layer(
+        attention_score_bias, tokens, input_norm_gain[None, :], forget_minimum,
+        decay_spikes.reshape(1, TOK), head_norm_gain[None, :],
+        *(w.T for w in narrow), recurrence_query_weight, forget_weight,
         recurrence_output_weight, attention_output_weight,
     )
-    return output(heads, columns)
 
 
 def solution(mesh):

time: 84 us -> 70.2 us (0.84)
  the two profiles are of different devices: /device:TPU:33 before, /device:TPU:387 now
where the time goes in v5:
time: 70.2 us; the launch traced here: 70 us
  Pallas kernels  67.8 us (97%)
  local copies, waits for them, and re-layouts  1.57 us (2%)
    pallas_call x1, Pallas kernels, layer(): pl.pallas_call(layer_kernel, out_shape=jax.ShapeDtypeStruct((TOK, 256), B...  67.8 us
    unnamed x1, local copies, waits for them, and re-layouts  1.57 us

profile of v5, /device:TPU:387, one launch (start us, length us, event | category | flops | bytes accessed | tf_op | source)
XLA Modules:
  0.0 70.0 jit_solution(582786252381964720)
XLA Ops:
  0.7 67.8 %layer.1 = bf16[256,256]{1,0:T(8,128)(2,1)} custom-call(f32[1]{0:T(128)S(6)} %copy.17.bias_ref, bf16[256,256]{1,0:T(8,128)(2,1)} %token_ref.1, f32[1,2048]{1,0:T(1,128)} %bitcast.13, f32[1,128]{1,0:T(1,128)} %low_ref.1, f32[1,256]{1,0:T(1,128)} %bitcast.14, f32[1,64]{1,0:T(1,128)} %bitcast.15, bf16[64,2048]{1,0:T(8,128)(2,1)} %bitcast.8, ...), custom_call_target="tpu_custom_call" | custom-call | tf_op jit(solution)/shard_map/layer/pallas_call | solution.py:526
  68.5 1.6 %copy.18 = bf16[256,256]{1,0:T(8,128)(2,1)} copy(bf16[256,256]{1,0:T(8,128)(2,1)} %layer.1) | data formatting | bytes 262144

commit v6 on v5

--- a/solution.py
+++ b/solution.py
@@ -150,50 +150,42 @@
     state_ref[REC_VAL:STATE_ROWS, :] = jnp.broadcast_to(offset, (8, REC_KEY))
 
 
-def stick_tile(q, kv, tri, bias2, keep=None):
-    z = dot(q, kv, tb=True) * (LOG2E / 8.0) + bias2
-    soft = jnp.maximum(z, jnp.log(1.0 + jnp.exp2(jnp.minimum(z, 30.0))) * LOG2E)
-    if keep is not None:
-        soft = jnp.where(keep, soft, 0.0)
-    later = dot(soft.astype(BF16), tri)
-    return z, soft, later
-
-
-def attend(here, plane, bias2, q_ref, kvs_ref, tri_ref, acc_ref, left_ref):
-    rows = lax.broadcasted_iota(jnp.int32, (TOK, TOK), 0)
-    cols = lax.broadcasted_iota(jnp.int32, (TOK, TOK), 1)
-    acc_ref[...] = jnp.zeros_like(acc_ref)
-    left_ref[...] = jnp.zeros_like(left_ref)
-
-    def pair(i, _):
-        tri = tri_ref[...]
-        q_own, q_far = q_ref[0:TOK, :], q_ref[TOK:, :]
-        kvs, own, far = [], [], []
-        for u in range(2):
-            n = 3 - 2 * i - u
-            kv = kvs_ref[plane, n]
-            keep = cols - rows < (here - plane * 4 - n) * TOK
-            kvs.append(kv)
-            own.append(stick_tile(q_own, kv, tri, bias2, keep) + (keep,))
-            far.append(stick_tile(q_far, kv, tri, bias2))
-        left_own, left_far = left_ref[0:TOK, 0:1], left_ref[TOK:, 0:1]
-        acc_own, acc_far = acc_ref[0:TOK, :], acc_ref[TOK:, :]
-        for u in range(2):
-            z, soft, later, keep = own[u]
-            weight = jnp.where(keep, jnp.exp2((z - soft) + (later + left_own)), 0.0)
-            acc_own = acc_own + dot(weight.astype(BF16), kvs[u])
-            left_own = left_own + (later[:, 0:1] - soft[:, 0:1])
-            z, soft, later = far[u]
-            weight = jnp.exp2((z - soft) + (later + left_far))
-            acc_far = acc_far + dot(weight.astype(BF16), kvs[u])
-            left_far = left_far + (later[:, 0:1] - soft[:, 0:1])
-        acc_ref[0:TOK, :] = acc_own
-        acc_ref[TOK:, :] = acc_far
-        left_ref[0:TOK, :] = jnp.broadcast_to(left_own, (TOK, 128))
-        left_ref[TOK:, :] = jnp.broadcast_to(left_far, (3 * TOK, 128))
-        return 0
-
-    lax.fori_loop(0, 2, pair, 0)
+def attend(first, here, plane, bias2, q_ref, kvs_ref, tri_ref, acc_ref, left_ref):
+    at = slice(first, first + 2 * TOK)
+    ahead = lax.broadcasted_iota(jnp.int32, (TOK, TOK), 1) - lax.broadcasted_iota(jnp.int32, (TOK, TOK), 0)
+    q, tri = q_ref[at, :], tri_ref[...]
+    acc = jnp.zeros((2 * TOK, 128), F32)
+    left = jnp.zeros((2 * TOK, 1), F32)
+    for n in (3, 2, 1, 0):
+
+        def masked(x):
+            if first > 0:
+                return x
+            keep = ahead < (here - plane * 4 - n) * TOK
+            return jnp.concatenate([jnp.where(keep, x[0:TOK], 0.0), x[TOK:]], axis=0)
+
+        kv = kvs_ref[plane, n]
+        z = dot(q, kv, tb=True) * (LOG2E / 8.0) + bias2
+        soft = masked(jnp.maximum(z, jnp.log(1.0 + jnp.exp2(jnp.minimum(z, 30.0))) * LOG2E))
+        later = dot(soft.astype(BF16), tri)
+        weight = masked(jnp.exp2((z - soft) + (later + left)))
+        acc = acc + dot(weight.astype(BF16), kv)
+        left = left + (later[:, 0:1] - soft[:, 0:1])
+    acc_ref[at, :] = acc
+    left_ref[at, :] = jnp.broadcast_to(left, (2 * TOK, 128))
+
+
+def pack(top, low, natural):
+    lane = lax.broadcasted_iota(jnp.int32, (128, 128), 1)
+    return jnp.where((lane < HEAD) == (natural == 0), top, pltpu.roll(low, 64, 1)).astype(BF16)
+
+
+def unpack(packed, natural):
+    lane = lax.broadcasted_iota(jnp.int32, (128, 128), 1)
+    keep = (lane < HEAD) == (natural == 0)
+    packed = packed.astype(F32)
+    low = pltpu.roll(packed, 64, 1)
+    return jnp.concatenate([jnp.where(keep, packed, 0.0), jnp.where(keep, low, 0.0)], axis=0).astype(BF16)
 
 
 def chain(states_ref, here):
@@ -218,8 +210,8 @@
     kvs_ref, queries_ref, state_ref, rows_ref, planes_ref, group_ref, groups_ref,
     local_ref, faded_ref, q_ref, tri_ref, acc_ref, left_ref,
     far_ref, far_left_ref, part_ref, part_left_ref, in_ref,
-    heads_ref, columns_ref, head_slots_ref, sum_ref,
-    load, token_send, token_recv, head_send, head_recv,
+    heads_ref, columns_ref, head_slots_ref, early_ref, early_slots_ref,
+    load, early_send, early_recv, token_send, token_recv, head_send, head_recv,
     line_send, line_recv, row_send, row_recv, half_send, half_recv, state_send, state_recv,
     query_send, query_recv, column_send, column_recv, back_send, back_recv, own_sem, near_sem,
 ):
@@ -374,33 +366,35 @@
     ]
     for copy in line_states:
         copy.start()
-    for n in (1, 2, 3):
-
-        @pl.when(c < n)
-        def _():
-            to(
-                query_ref, queries_ref.at[n - 1], query_send.at[0], query_recv.at[n - 1], far[1]
-            ).wait_recv()
-
-    lane = lax.broadcasted_iota(jnp.int32, (128, 128), 1)
-    for n in range(4):
-        packed = (query_ref[...] if n == 0 else queries_ref[n - 1]).astype(F32)
-        for half in range(2):
-            part = packed if half == 0 else pltpu.roll(packed, 64, 1)
-            at = n * TOK + half * 128
-            q_ref[at : at + 128, :] = jnp.where(lane < HEAD, part, 0.0).astype(BF16)
-
-    def attend_plane(d):
-        for k in range(2):
-            halves[d][k].wait_recv()
+    def take(n):
+        if n > 0:
+
+            @pl.when(c < n)
+            def _():
+                to(
+                    query_ref, queries_ref.at[n - 1], query_send.at[0], query_recv.at[n - 1], far[1]
+                ).wait_recv()
+
+        packed = query_ref[...] if n == 0 else queries_ref[n - 1]
+        q_ref[n * TOK : (n + 1) * TOK, :] = unpack(packed, 0)
+
+    def attend_plane(d, first):
+        if first == (0 if d == 0 or d == 1 else 2 * TOK):
+            for k in range(2):
+                halves[d][k].wait_recv()
         attend(
-            zl * 4 + y, (zl - d + 4) % 4, bias_ref[0] * LOG2E, q_ref, kvs_ref, tri_ref,
+            first, zl * 4 + y, (zl - d + 4) % 4, bias_ref[0] * LOG2E, q_ref, kvs_ref, tri_ref,
             acc_ref.at[d], left_ref.at[d],
         )
 
-    attend_plane(0)
+    take(0)
+    take(1)
+    attend_plane(0, 0)
+    take(2)
+    take(3)
+    attend_plane(0, 2 * TOK)
     pass_on(2)
-    attend_plane(1)
+    attend_plane(1, 0)
     pass_on(3)
     for copy in line_states:
         copy.wait_recv()
@@ -426,8 +420,9 @@
         def _():
             back(0, d).start()
 
-    attend_plane(2)
-    attend_plane(3)
+    attend_plane(1, 2 * TOK)
+    attend_plane(2, 2 * TOK)
+    attend_plane(3, 2 * TOK)
 
     def joined(at):
         n = (zl + 1) % 4
@@ -438,23 +433,22 @@
             left = left + left_ref[n, at, :]
         return acc, left
 
-    for n in range(3):
+    def ready(n):
         at = (n + 1) * TOK
         top, top_left = joined(slice(at, at + 128))
-        bottom, bottom_left = joined(slice(at + 128, at + 256))
-        far_ref[n] = jnp.where(lane < HEAD, pltpu.roll(bottom, 64, 1), top).astype(BF16)
+        low, low_left = joined(slice(at + 128, at + 256))
+        far_ref[n] = pack(top, low, 1)
         far_left_ref[n, :, 0:128] = jnp.transpose(top_left)[0:1, :]
-        far_left_ref[n, :, 128:256] = jnp.transpose(bottom_left)[0:1, :]
-    for d in (3, 2, 1):
-
-        @pl.when(c + d < 4)
+        far_left_ref[n, :, 128:256] = jnp.transpose(low_left)[0:1, :]
+
+    ready(1)
+    ready(2)
+    for d in (2, 3, 1):
+
+        @pl.when((c + d < 4) & (c + d > 1))
         def _():
             back(1, d).start()
             back(2, d).start()
-
-    own_acc, own_left = joined(slice(0, TOK))
-    acc_ref[0, 0:TOK, :] = own_acc
-    left_ref[0, 0:TOK, :] = own_left
 
     in_ref[...] = jnp.zeros_like(in_ref)
     for g in (0, 1, 2):
@@ -470,7 +464,32 @@
     raw = local_ref[...] + dot(faded_ref[...], entering.astype(BF16), tb=True)
     normed = raw * lax.rsqrt(jnp.mean(raw * raw, axis=1, keepdims=True) + epsilon) * gain_ref[...]
     gate = gate_ref[...].astype(F32)
-    heads_ref[:, 0:REC_VAL] = (normed * (gate * jax.nn.sigmoid(gate))).astype(BF16)
+    state_heads = normed * (gate * jax.nn.sigmoid(gate))
+    state_heads = jnp.concatenate([state_heads, jnp.zeros_like(state_heads)], axis=1)
+    early_ref[...] = pack(state_heads[0:128], state_heads[128:256], 0)
+    early_copies = [
+        pltpu.make_async_remote_copy(
+            src_ref=early_ref, dst_ref=early_slots_ref.at[tp], send_sem=early_send.at[d],
+            recv_sem=early_recv.at[d], device_id={"tp": there}, device_id_type=MESH,
+        )
+        for d, there in enumerate(lane_peers)
+    ]
+    for copy in early_copies:
+        copy.start()
+    early_slots_ref[tp] = early_ref[...]
+
+    attend_plane(2, 0)
+    attend_plane(3, 0)
+    ready(0)
+
+    @pl.when(c == 0)
+    def _():
+        back(1, 1).start()
+        back(2, 1).start()
+
+    own_acc, own_left = joined(slice(0, TOK))
+    acc_ref[0, 0:TOK, :] = own_acc
+    left_ref[0, 0:TOK, :] = own_left
 
     for g in (2, 1, 0):
 
@@ -485,22 +504,22 @@
             for at in (0, 128):
                 left_ref[0, at : at + 128, :] += column(part_left_ref[g, 0:1, at : at + 128])
 
-    heads_ref[:, REC_VAL:] = acc_ref[0, 0:TOK, HEAD:].astype(BF16)
+    heads_ref[...] = pack(acc_ref[0, 0:128, :], acc_ref[0, 128:256, :], 1)
 
     def columns_here():
         for copy in own_columns:
             copy.wait()
-        for copy in column_copies:
+        for copy in column_copies + early_copies:
             copy.wait_recv()
-
-    sum_ref[...] = jnp.zeros_like(sum_ref)
-
-    def add(source, ref):
-        sum_ref[...] += dot(ref[...], columns_ref[source])
+        out_ref[...] = jnp.zeros_like(out_ref)
+        for n in range(8):
+            add(n, early_slots_ref.at[n], 0)
+
+    def add(source, ref, natural=1):
+        out_ref[...] += dot(unpack(ref[...], natural), columns_ref[source])
 
     ring_gather(heads_ref, head_slots_ref, head_send, head_recv, columns_here, add)
-    out_ref[...] = sum_ref[...].astype(BF16)
-    sent = along_line + row_states + line_states + column_copies
+    sent = early_copies + along_line + row_states + line_states + column_copies
     for d in range(4):
         sent = sent + along_row[d] + halves[d]
     for copy in sent:
@@ -525,7 +544,7 @@
 
     return pl.pallas_call(
         layer_kernel,
-        out_shape=jax.ShapeDtypeStruct((TOK, 256), BF16),
+        out_shape=jax.ShapeDtypeStruct((TOK, 256), F32),
         in_specs=[SMEM] + [VMEM] * 5 + [ANY] * 9,
         out_specs=VMEM,
         scratch_shapes=[
@@ -559,11 +578,12 @@
             pltpu.VMEM((3, 128, 128), BF16),
             pltpu.VMEM((3, 1, TOK), F32),
             pltpu.VMEM((REC_VAL, REC_KEY), F32),
-            pltpu.VMEM((TOK, 128), BF16),
+            pltpu.VMEM((128, 128), BF16),
             pltpu.VMEM((8, 128, 256), BF16),
-            pltpu.VMEM((8, TOK, 128), BF16),
-            pltpu.VMEM((TOK, 256), F32),
-            dma((7,)), *both(13), *both(13),
+            pltpu.VMEM((8, 128, 128), BF16),
+            pltpu.VMEM((128, 128), BF16),
+            pltpu.VMEM((8, 128, 128), BF16),
+            dma((7,)), *both(7), *both(13), *both(13),
             *both(3), *both(4, 2), *both(4, 2), *both(2, 3),
             *both(3), *both(2, 7), *both(3, 3), dma((2,)), pltpu.SemaphoreType.REGULAR,
         ],
@@ -597,7 +617,7 @@
         decay_spikes.reshape(1, TOK), head_norm_gain[None, :],
         *(w.T for w in narrow), recurrence_query_weight, forget_weight,
         recurrence_output_weight, attention_output_weight,
-    )
+    ).astype(BF16)
 
 
 def solution(mesh):

time: 70.2 us -> 70.4 us (level)
  the two profiles are of different devices: /device:TPU:387 before, /device:TPU:449 now
where the time goes in v6:
time: 70.4 us; the launch traced here: 70.3 us
  Pallas kernels  68 us (97%)
  other arithmetic  1.62 us (2%)
    pallas_call x1, Pallas kernels, layer(): pl.pallas_call(layer_kernel, out_shape=jax.ShapeDtypeStruct((TOK, 256), F...  68 us
    convert_element_type x1, other arithmetic, shards(): return layer(attention_score_bias, tokens, input_norm_gain[None, :], forg...  1.62 us

profile of v6, /device:TPU:449, one launch (start us, length us, event | category | flops | bytes accessed | tf_op | source)
XLA Modules:
  0.0 70.3 jit_solution(14541516767024653181)
XLA Ops:
  0.7 68.0 %layer.1 = f32[256,256]{1,0:T(8,128)} custom-call(f32[1]{0:T(128)S(6)} %copy.16.bias_ref, bf16[256,256]{1,0:T(8,128)(2,1)} %token_ref.1, f32[1,2048]{1,0:T(1,128)} %bitcast.13, f32[1,128]{1,0:T(1,128)} %low_ref.1, f32[1,256]{1,0:T(1,128)} %bitcast.14, f32[1,64]{1,0:T(1,128)} %bitcast.15, bf16[64,2048]{1,0:T(8,128)(2,1)} %bitcast.8, ...), custom_call_target="tpu_custom_call" | custom-call | tf_op jit(solution)/shard_map/layer/pallas_call | solution.py:545
  68.6 1.6 %convert_element_type.3 = bf16[256,256]{1,0:T(8,128)(2,1)} convert(f32[256,256]{1,0:T(8,128)} %layer.1) | non-fusion elementwise | flops 65536 | bytes 393216 | tf_op jit(solution)/shard_map/convert_element_type | solution.py:620

commit v7 on v6

--- a/solution.py
+++ b/solution.py
@@ -252,7 +252,8 @@
     ]
 
     barrier = pltpu.get_barrier_semaphore()
-    near = row[1:] + line[1:] + [far[1], far[3]]
+    planes = [[(sp + 4 * d) % 64, (sp + 64 - 4 * d) % 64] for d in (1, 2, 4)]
+    near = row[1:] + planes[0]
     for peer in lane_peers:
         pl.semaphore_signal(barrier, inc=1, device_id={"tp": peer}, device_id_type=MESH)
     for peer in near:
@@ -266,12 +267,20 @@
     cols = lax.broadcasted_iota(jnp.int32, (TOK, TOK), 1)
     tri_ref[...] = jnp.where(rows > cols, -1.0, 0.0).astype(BF16)
     pl.semaphore_wait(barrier, len(lane_peers) + len(near))
-    for peer in (far[1], far[3]):
-        pl.semaphore_signal(near_sem, inc=1, device_id={"sp": peer}, device_id_type=MESH)
+
+    def vouch(n):
+        for peer in planes[n]:
+            pl.semaphore_signal(near_sem.at[n], inc=1, device_id={"sp": peer}, device_id_type=MESH)
+
+    vouch(0)
 
     def meanwhile():
+        pl.semaphore_wait(near_sem.at[0], 2)
+        vouch(1)
         for one in loads:
             one.wait()
+        pl.semaphore_wait(near_sem.at[1], 2)
+        vouch(2)
 
     def use(source, ref):
         at = pl.ds(pl.multiple_of(source * 256, 256), 256)
@@ -304,13 +313,7 @@
         slot = (c + 3) % 4
         return to(query_ref, queries_ref.at[slot], query_send.at[d - 1], query_recv.at[slot], far[4 - d])
 
-    pl.semaphore_wait(near_sem, 2)
-    for d in (1, 2, 3):
-
-        @pl.when(c >= d)
-        def _():
-            query_copy(d).start()
-
+    pl.semaphore_wait(near_sem.at[2], 2)
     along_line = [
         to(kv_ref, kvs_ref.at[zl, y], line_send.at[d - 1], line_recv.at[d - 1], line[d]) for d in (1, 2, 3)
     ]
@@ -330,30 +333,64 @@
         return to(block, block, half_send.at[d, k], half_recv.at[d, k], row[1 if k == 0 else 3])
 
     halves = [[onward(d, k) for k in range(2)] for d in range(4)]
-    for copy in along_row[0] + along_line:
+    for copy in along_row[0]:
         copy.start()
+    for d, n in ((2, 1), (1, 2), (3, 3)):
+
+        @pl.when(c >= d)
+        def _():
+            query_copy(d).start()
+
+        along_line[n - 1].start()
     local_scan(rec_ref, forget_ref, input_ref, low_ref, spike_ref, local_ref, faded_ref, state_ref)
     rows_ref[y] = state_ref[...]
     row_states = [
         to(state_ref, rows_ref.at[y], state_send.at[0, d - 1], state_recv.at[0, d - 1], row[d])
         for d in (1, 2, 3)
     ]
+    for copy in row_states:
+        copy.start()
 
     def pass_on(d):
         for k in range(2):
             along_row[d][k].wait_recv()
             halves[d][k].start()
 
-    along_line[0].wait_recv()
-    for copy in along_row[1]:
-        copy.start()
+    def from_line(d):
+        along_line[d - 1].wait_recv()
+        for copy in along_row[d]:
+            copy.start()
+
+    def take(n):
+        if n > 0:
+
+            @pl.when(c < n)
+            def _():
+                to(
+                    query_ref, queries_ref.at[n - 1], query_send.at[0], query_recv.at[n - 1], far[1]
+                ).wait_recv()
+
+        packed = query_ref[...] if n == 0 else queries_ref[n - 1]
+        q_ref[n * TOK : (n + 1) * TOK, :] = unpack(packed, 0)
+
+    def attend_plane(d, first):
+        if first == (0 if d == 0 else 2 * TOK):
+            for k in range(2):
+                halves[d][k].wait_recv()
+        attend(
+            first, zl * 4 + y, (zl - d + 4) % 4, bias_ref[0] * LOG2E, q_ref, kvs_ref, tri_ref,
+            acc_ref.at[d], left_ref.at[d],
+        )
+
     pass_on(0)
-    along_line[1].wait_recv()
-    for copy in along_row[2] + row_states:
-        copy.start()
+    from_line(1)
+    take(0)
+    take(1)
+    attend_plane(0, 0)
+    from_line(2)
     pass_on(1)
-    along_line[2].wait_recv()
-    for copy in along_row[3] + column_copies:
+    from_line(3)
+    for copy in column_copies:
         copy.start()
     for copy in row_states:
         copy.wait_recv()
@@ -366,35 +403,11 @@
     ]
     for copy in line_states:
         copy.start()
-    def take(n):
-        if n > 0:
-
-            @pl.when(c < n)
-            def _():
-                to(
-                    query_ref, queries_ref.at[n - 1], query_send.at[0], query_recv.at[n - 1], far[1]
-                ).wait_recv()
-
-        packed = query_ref[...] if n == 0 else queries_ref[n - 1]
-        q_ref[n * TOK : (n + 1) * TOK, :] = unpack(packed, 0)
-
-    def attend_plane(d, first):
-        if first == (0 if d == 0 or d == 1 else 2 * TOK):
-            for k in range(2):
-                halves[d][k].wait_recv()
-        attend(
-            first, zl * 4 + y, (zl - d + 4) % 4, bias_ref[0] * LOG2E, q_ref, kvs_ref, tri_ref,
-            acc_ref.at[d], left_ref.at[d],
-        )
-
-    take(0)
-    take(1)
-    attend_plane(0, 0)
     take(2)
     take(3)
     attend_plane(0, 2 * TOK)
     pass_on(2)
-    attend_plane(1, 0)
+    attend_plane(1, 2 * TOK)
     pass_on(3)
     for copy in line_states:
         copy.wait_recv()
@@ -420,7 +433,6 @@
         def _():
             back(0, d).start()
 
-    attend_plane(1, 2 * TOK)
     attend_plane(2, 2 * TOK)
     attend_plane(3, 2 * TOK)
 
@@ -449,6 +461,8 @@
         def _():
             back(1, d).start()
             back(2, d).start()
+
+    attend_plane(1, 0)
 
     in_ref[...] = jnp.zeros_like(in_ref)
     for g in (0, 1, 2):
@@ -585,7 +599,7 @@
             pltpu.VMEM((8, 128, 128), BF16),
             dma((7,)), *both(7), *both(13), *both(13),
             *both(3), *both(4, 2), *both(4, 2), *both(2, 3),
-            *both(3), *both(2, 7), *both(3, 3), dma((2,)), pltpu.SemaphoreType.REGULAR,
+            *both(3), *both(2, 7), *both(3, 3), dma((2,)), pltpu.SemaphoreType.REGULAR((3,)),
         ],
         compiler_params=pltpu.CompilerParams(collective_id=0, has_side_effects=True),
         name="layer",

time: 70.4 us -> 65.1 us (0.925)
  the two profiles are of different devices: /device:TPU:449 before, /device:TPU:451 now
where the time goes in v7:
time: 65.1 us; the launch traced here: 65 us
  Pallas kernels  62.7 us (96%)
  other arithmetic  1.62 us (2%)
  between operations  0.66 us (1%)
    pallas_call x1, Pallas kernels, layer(): pl.pallas_call(layer_kernel, out_shape=jax.ShapeDtypeStruct((TOK, 256), F...  62.7 us
    convert_element_type x1, other arithmetic, shards(): return layer(attention_score_bias, tokens, input_norm_gain[None, :], forg...  1.62 us

profile of v7, /device:TPU:451, one launch (start us, length us, event | category | flops | bytes accessed | tf_op | source)
XLA Modules:
  0.0 65.0 jit_solution(8875584775251585476)
XLA Ops:
  0.7 62.7 %layer.1 = f32[256,256]{1,0:T(8,128)} custom-call(f32[1]{0:T(128)S(6)} %copy.16.bias_ref, bf16[256,256]{1,0:T(8,128)(2,1)} %token_ref.1, f32[1,2048]{1,0:T(1,128)} %bitcast.13, f32[1,128]{1,0:T(1,128)} %low_ref.1, f32[1,256]{1,0:T(1,128)} %bitcast.14, f32[1,64]{1,0:T(1,128)} %bitcast.15, bf16[64,2048]{1,0:T(8,128)(2,1)} %bitcast.8, ...), custom_call_target="tpu_custom_call" | custom-call | tf_op jit(solution)/shard_map/layer/pallas_call | solution.py:559
  63.4 1.6 %convert_element_type.3 = bf16[256,256]{1,0:T(8,128)(2,1)} convert(f32[256,256]{1,0:T(8,128)} %layer.1) | non-fusion elementwise | flops 65536 | bytes 393216 | tf_op jit(solution)/shard_map/convert_element_type | solution.py:634

commit v8 on v7

--- a/solution.py
+++ b/solution.py
@@ -19,7 +19,7 @@
 F32, BF16 = jnp.float32, jnp.bfloat16
 VMEM = pl.BlockSpec(memory_space=pltpu.VMEM)
 SMEM = pl.BlockSpec(memory_space=pltpu.SMEM)
-ANY = pl.BlockSpec(memory_space=pl.ANY)
+HBM = pl.BlockSpec(memory_space=pltpu.HBM)
 MESH = pl.DeviceIdType.MESH
 
 
@@ -46,7 +46,7 @@
     return tp, tp + 1 - 2 * core, (tp + 2) % 8, (tp + 6) % 8, (tp + 4) % 8, 1 - 2 * core
 
 
-def ring_gather(chunk_ref, slots_ref, send, recv, meanwhile, use):
+def ring_gather(chunk_ref, slots_ref, send, recv, meanwhile, use, small=False):
     tp, partner, right, left, across, twist = lanes()
     half = chunk_ref.shape[0] // 2
     top, low = slice(0, half), slice(half, 2 * half)
@@ -72,18 +72,24 @@
         relay(8, right, low, partner),
         relay(9, left, low, partner),
         relay(10, right, top, partner),
-        relay(11, across, top, partner),
-        relay(12, across, low, partner),
-    ]
+    ]
+    if small:
+        copies += [relay(11, left, top, right + twist), relay(12, right, low, left + twist)]
+    else:
+        copies += [relay(11, across, top, partner), relay(12, across, low, partner)]
     for n in range(5):
         copies[n].start()
     meanwhile()
     use(tp, chunk_ref)
     copies[1].wait_recv()
     copies[5].start()
+    if small:
+        copies[11].start()
     copies[7].start()
     copies[2].wait_recv()
     copies[6].start()
+    if small:
+        copies[12].start()
     copies[8].start()
     copies[0].wait_recv()
     use(partner, slots_ref.at[partner])
@@ -100,9 +106,11 @@
     copies[10].wait_recv()
     use(right + twist, slots_ref.at[right + twist])
     copies[5].wait_recv()
-    copies[11].start()
+    if not small:
+        copies[11].start()
     copies[6].wait_recv()
-    copies[12].start()
+    if not small:
+        copies[12].start()
     use(across, slots_ref.at[across])
     copies[11].wait_recv()
     copies[12].wait_recv()
@@ -202,9 +210,10 @@
 
 
 def layer_kernel(
-    bias_ref, token_ref, feature_gain_ref, low_ref, spike_ref, gain_ref,
+    bias_ref, token_hbm, feature_gain_hbm, low_hbm, spike_hbm, gain_hbm,
     key_w, value_w, input_w, gate_w, query_w, rec_w, forget_w, rec_out_w, att_out_w,
     out_ref,
+    token_ref, feature_gain_ref, low_ref, spike_ref, gain_ref,
     slots_ref, narrow_ref, wide_ref, first_ref, second_ref, square_ref,
     kv_ref, query_ref, rec_ref, forget_ref, input_ref, gate_ref,
     kvs_ref, queries_ref, state_ref, rows_ref, planes_ref, group_ref, groups_ref,
@@ -232,6 +241,11 @@
         pltpu.make_async_copy(w, wide_ref.at[:, n * 128 : n * 128 + 128], load.at[5 + n])
         for n, w in enumerate((rec_w, forget_w))
     ]
+    small = (
+        (token_hbm, token_ref), (feature_gain_hbm, feature_gain_ref), (low_hbm, low_ref),
+        (spike_hbm, spike_ref), (gain_hbm, gain_ref),
+    )
+    first_loads = [pltpu.make_async_copy(src, dst, load.at[7 + n]) for n, (src, dst) in enumerate(small)]
 
     def columns(w, there):
         return w.at[:, pl.ds(pl.multiple_of(there * 256, 256), 256)]
@@ -258,7 +272,7 @@
         pl.semaphore_signal(barrier, inc=1, device_id={"tp": peer}, device_id_type=MESH)
     for peer in near:
         pl.semaphore_signal(barrier, inc=1, device_id={"sp": peer}, device_id_type=MESH)
-    for copy in loads + own_columns:
+    for copy in first_loads + loads + own_columns:
         copy.start()
     first_ref[...] = jnp.zeros_like(first_ref)
     second_ref[...] = jnp.zeros_like(second_ref)
@@ -273,6 +287,8 @@
             pl.semaphore_signal(near_sem.at[n], inc=1, device_id={"sp": peer}, device_id_type=MESH)
 
     vouch(0)
+    for copy in first_loads:
+        copy.wait()
 
     def meanwhile():
         pl.semaphore_wait(near_sem.at[0], 2)
@@ -532,7 +548,7 @@
     def add(source, ref, natural=1):
         out_ref[...] += dot(unpack(ref[...], natural), columns_ref[source])
 
-    ring_gather(heads_ref, head_slots_ref, head_send, head_recv, columns_here, add)
+    ring_gather(heads_ref, head_slots_ref, head_send, head_recv, columns_here, add, small=True)
     sent = early_copies + along_line + row_states + line_states + column_copies
     for d in range(4):
         sent = sent + along_row[d] + halves[d]
@@ -559,9 +575,14 @@
     return pl.pallas_call(
         layer_kernel,
         out_shape=jax.ShapeDtypeStruct((TOK, 256), F32),
-        in_specs=[SMEM] + [VMEM] * 5 + [ANY] * 9,
+        in_specs=[SMEM] + [HBM] * 14,
         out_specs=VMEM,
         scratch_shapes=[
+            pltpu.VMEM((TOK, 256), BF16),
+            pltpu.VMEM((1, D), F32),
+            pltpu.VMEM((1, REC_KEY), F32),
+            pltpu.VMEM((1, TOK), F32),
+            pltpu.VMEM((1, REC_VAL), F32),
             pltpu.VMEM((8, TOK, 256), BF16),
             pltpu.VMEM((320, D), BF16),
             pltpu.VMEM((D, 256), BF16),
@@ -597,7 +618,7 @@
             pltpu.VMEM((8, 128, 128), BF16),
             pltpu.VMEM((128, 128), BF16),
             pltpu.VMEM((8, 128, 128), BF16),
-            dma((7,)), *both(7), *both(13), *both(13),
+            dma((12,)), *both(7), *both(13), *both(13),
             *both(3), *both(4, 2), *both(4, 2), *both(2, 3),
             *both(3), *both(2, 7), *both(3, 3), dma((2,)), pltpu.SemaphoreType.REGULAR((3,)),
         ],

time: 65.1 us -> 63.3 us (0.972)
  Pallas kernels: 62.7 us -> 60.9 us
    pallas_call x1, Pallas kernels: 62.7 us -> 60.9 us  [layer(): pl.pallas_call(layer_kernel, out_shape=jax.ShapeDtypeStruct((TOK, 256), F...]
where the time goes in v8:
time: 63.3 us; the launch traced here: 63.1 us
  Pallas kernels  60.9 us (96%)
  other arithmetic  1.62 us (3%)
  between operations  0.66 us (1%)
    pallas_call x1, Pallas kernels, layer(): pl.pallas_call(layer_kernel, out_shape=jax.ShapeDtypeStruct((TOK, 256), F...  60.9 us
    convert_element_type x1, other arithmetic, shards(): return layer(attention_score_bias, tokens, input_norm_gain[None, :], forg...  1.62 us

profile of v8, /device:TPU:451, one launch (start us, length us, event | category | flops | bytes accessed | tf_op | source)
XLA Modules:
  0.0 63.1 jit_solution(17550539496306410133)
XLA Ops:
  0.7 60.9 %layer.1 = f32[256,256]{1,0:T(8,128)} custom-call(f32[1]{0:T(128)S(6)} %copy.16.bias_ref, bf16[256,256]{1,0:T(8,128)(2,1)} %token_hbm.1, f32[1,2048]{1,0:T(1,128)} %bitcast.13, f32[1,128]{1,0:T(1,128)} %low_hbm.1, f32[1,256]{1,0:T(1,128)} %bitcast.14, f32[1,64]{1,0:T(1,128)} %bitcast.15, bf16[64,2048]{1,0:T(8,128)(2,1)} %bitcast.8, ...), custom_call_target="tpu_custom_call" | custom-call | tf_op jit(solution)/shard_map/layer/pallas_call | solution.py:575
  61.5 1.6 %convert_element_type.3 = bf16[256,256]{1,0:T(8,128)(2,1)} convert(f32[256,256]{1,0:T(8,128)} %layer.1) | non-fusion elementwise | flops 65536 | bytes 393216 | tf_op jit(solution)/shard_map/convert_element_type | solution.py:655

commit v9 on v8

--- a/solution.py
+++ b/solution.py
@@ -320,10 +320,6 @@
         def _():
             queries_ref[n - 1] = jnp.zeros((128, 128), BF16)
 
-    input_ref[...] = (first_ref[:, 128:192] * inverse).astype(BF16)
-    gate_ref[...] = (first_ref[:, 192:256] * inverse).astype(BF16)
-    rec_ref[...] = (second_ref[:, 0:128] * inverse).astype(BF16)
-    forget_ref[...] = (second_ref[:, 128:256] * inverse).astype(BF16)
 
     def query_copy(d):
         slot = (c + 3) % 4
@@ -358,6 +354,10 @@
             query_copy(d).start()
 
         along_line[n - 1].start()
+    input_ref[...] = (first_ref[:, 128:192] * inverse).astype(BF16)
+    gate_ref[...] = (first_ref[:, 192:256] * inverse).astype(BF16)
+    rec_ref[...] = (second_ref[:, 0:128] * inverse).astype(BF16)
+    forget_ref[...] = (second_ref[:, 128:256] * inverse).astype(BF16)
     local_scan(rec_ref, forget_ref, input_ref, low_ref, spike_ref, local_ref, faded_ref, state_ref)
     rows_ref[y] = state_ref[...]
     row_states = [
@@ -419,10 +419,10 @@
     ]
     for copy in line_states:
         copy.start()
+    pass_on(2)
     take(2)
     take(3)
     attend_plane(0, 2 * TOK)
-    pass_on(2)
     attend_plane(1, 2 * TOK)
     pass_on(3)
     for copy in line_states:
@@ -521,6 +521,17 @@
     acc_ref[0, 0:TOK, :] = own_acc
     left_ref[0, 0:TOK, :] = own_left
 
+    def add(source, ref, natural=1):
+        out_ref[...] += dot(unpack(ref[...], natural), columns_ref[source])
+
+    for copy in own_columns:
+        copy.wait()
+    for copy in column_copies + early_copies:
+        copy.wait_recv()
+    out_ref[...] = jnp.zeros_like(out_ref)
+    for n in range(8):
+        add(n, early_slots_ref.at[n], 0)
+
     for g in (2, 1, 0):
 
         @pl.when(g < c)
@@ -536,19 +547,7 @@
 
     heads_ref[...] = pack(acc_ref[0, 0:128, :], acc_ref[0, 128:256, :], 1)
 
-    def columns_here():
-        for copy in own_columns:
-            copy.wait()
-        for copy in column_copies + early_copies:
-            copy.wait_recv()
-        out_ref[...] = jnp.zeros_like(out_ref)
-        for n in range(8):
-            add(n, early_slots_ref.at[n], 0)
-
-    def add(source, ref, natural=1):
-        out_ref[...] += dot(unpack(ref[...], natural), columns_ref[source])
-
-    ring_gather(heads_ref, head_slots_ref, head_send, head_recv, columns_here, add, small=True)
+    ring_gather(heads_ref, head_slots_ref, head_send, head_recv, lambda: None, add, small=True)
     sent = early_copies + along_line + row_states + line_states + column_copies
     for d in range(4):
         sent = sent + along_row[d] + halves[d]

time: 63.3 us -> 64.9 us (1.025)
  the two profiles are of different devices: /device:TPU:451 before, /device:TPU:449 now
where the time goes in v9:
time: 64.9 us; the launch traced here: 64.7 us
  Pallas kernels  62.5 us (96%)
  other arithmetic  1.62 us (2%)
  between operations  0.66 us (1%)
    pallas_call x1, Pallas kernels, layer(): pl.pallas_call(layer_kernel, out_shape=jax.ShapeDtypeStruct((TOK, 256), F...  62.5 us
    convert_element_type x1, other arithmetic, shards(): return layer(attention_score_bias, tokens, input_norm_gain[None, :], forg...  1.62 us

profile of v9, /device:TPU:449, one launch (start us, length us, event | category | flops | bytes accessed | tf_op | source)
XLA Modules:
  0.0 64.7 jit_solution(12853922948625852550)
XLA Ops:
  0.7 62.5 %layer.1 = f32[256,256]{1,0:T(8,128)} custom-call(f32[1]{0:T(128)S(6)} %copy.16.bias_ref, bf16[256,256]{1,0:T(8,128)(2,1)} %token_hbm.1, f32[1,2048]{1,0:T(1,128)} %bitcast.13, f32[1,128]{1,0:T(1,128)} %low_hbm.1, f32[1,256]{1,0:T(1,128)} %bitcast.14, f32[1,64]{1,0:T(1,128)} %bitcast.15, bf16[64,2048]{1,0:T(8,128)(2,1)} %bitcast.8, ...), custom_call_target="tpu_custom_call" | custom-call | tf_op jit(solution)/shard_map/layer/pallas_call | solution.py:574
  63.1 1.6 %convert_element_type.3 = bf16[256,256]{1,0:T(8,128)(2,1)} convert(f32[256,256]{1,0:T(8,128)} %layer.1) | non-fusion elementwise | flops 65536 | bytes 393216 | tf_op jit(solution)/shard_map/convert_element_type | solution.py:654

commit v10 on v8

--- a/solution.py
+++ b/solution.py
@@ -79,8 +79,9 @@
         copies += [relay(11, across, top, partner), relay(12, across, low, partner)]
     for n in range(5):
         copies[n].start()
-    meanwhile()
-    use(tp, chunk_ref)
+    if not small:
+        meanwhile()
+        use(tp, chunk_ref)
     copies[1].wait_recv()
     copies[5].start()
     if small:
@@ -92,11 +93,16 @@
         copies[12].start()
     copies[8].start()
     copies[0].wait_recv()
-    use(partner, slots_ref.at[partner])
+    if not small:
+        use(partner, slots_ref.at[partner])
     copies[3].wait_recv()
     copies[9].start()
     copies[4].wait_recv()
     copies[10].start()
+    if small:
+        meanwhile()
+        use(tp, chunk_ref)
+        use(partner, slots_ref.at[partner])
     use(left, slots_ref.at[left])
     use(right, slots_ref.at[right])
     copies[7].wait_recv()
@@ -320,13 +326,9 @@
         def _():
             queries_ref[n - 1] = jnp.zeros((128, 128), BF16)
 
-    input_ref[...] = (first_ref[:, 128:192] * inverse).astype(BF16)
-    gate_ref[...] = (first_ref[:, 192:256] * inverse).astype(BF16)
-    rec_ref[...] = (second_ref[:, 0:128] * inverse).astype(BF16)
-    forget_ref[...] = (second_ref[:, 128:256] * inverse).astype(BF16)
 
     def query_copy(d):
-        slot = (c + 3) % 4
+        slot = (c + 2) % 3
         return to(query_ref, queries_ref.at[slot], query_send.at[d - 1], query_recv.at[slot], far[4 - d])
 
     pl.semaphore_wait(near_sem.at[2], 2)
@@ -358,6 +360,10 @@
             query_copy(d).start()
 
         along_line[n - 1].start()
+    input_ref[...] = (first_ref[:, 128:192] * inverse).astype(BF16)
+    gate_ref[...] = (first_ref[:, 192:256] * inverse).astype(BF16)
+    rec_ref[...] = (second_ref[:, 0:128] * inverse).astype(BF16)
+    forget_ref[...] = (second_ref[:, 128:256] * inverse).astype(BF16)
     local_scan(rec_ref, forget_ref, input_ref, low_ref, spike_ref, local_ref, faded_ref, state_ref)
     rows_ref[y] = state_ref[...]
     row_states = [

time: 63.3 us -> 63.2 us (level)
  no operation moved by 1% of the time
where the time goes in v10:
time: 63.2 us; the launch traced here: 63.1 us
  Pallas kernels  60.8 us (96%)
  other arithmetic  1.62 us (3%)
  between operations  0.66 us (1%)
    pallas_call x1, Pallas kernels, layer(): pl.pallas_call(layer_kernel, out_shape=jax.ShapeDtypeStruct((TOK, 256), F...  60.8 us
    convert_element_type x1, other arithmetic, shards(): return layer(attention_score_bias, tokens, input_norm_gain[None, :], forg...  1.62 us

profile of v10, /device:TPU:451, one launch (start us, length us, event | category | flops | bytes accessed | tf_op | source)
XLA Modules:
  0.0 63.1 jit_solution(8362563207661109462)
XLA Ops:
  0.7 60.8 %layer.1 = f32[256,256]{1,0:T(8,128)} custom-call(f32[1]{0:T(128)S(6)} %copy.16.bias_ref, bf16[256,256]{1,0:T(8,128)(2,1)} %token_hbm.1, f32[1,2048]{1,0:T(1,128)} %bitcast.13, f32[1,128]{1,0:T(1,128)} %low_hbm.1, f32[1,256]{1,0:T(1,128)} %bitcast.14, f32[1,64]{1,0:T(1,128)} %bitcast.15, bf16[64,2048]{1,0:T(8,128)(2,1)} %bitcast.8, ...), custom_call_target="tpu_custom_call" | custom-call | tf_op jit(solution)/shard_map/layer/pallas_call | solution.py:581
  61.4 1.6 %convert_element_type.3 = bf16[256,256]{1,0:T(8,128)(2,1)} convert(f32[256,256]{1,0:T(8,128)} %layer.1) | non-fusion elementwise | flops 65536 | bytes 393216 | tf_op jit(solution)/shard_map/convert_element_type | solution.py:661
